TPU v7x, 256 devices: a whole 4x4x8 slice. The times are simulated.
256 devices in a mesh: sp: 64 (over z, x, core), tp: 4 (over y).
Axes of the slice: x: 4, y: 4, z: 8, core: 2. Of those that a mesh axis runs over, the one named last changes fastest.
Arguments:
- wide_query: bfloat16 [32768, 1536], P('sp', 'tp'), may hold values from -6 to 6
- wide_key: bfloat16 [32768, 1536], P('sp', 'tp'), may hold values from -6 to 6
- wide_value: bfloat16 [32768, 1536], P('sp', 'tp'), may hold values from -6 to 6
- wide_gate: bfloat16 [32768, 1536], P('sp', 'tp'), may hold values from -6 to 6
- narrow_query: bfloat16 [32768, 512], P('sp', 'tp'), may hold values from -6 to 6
- narrow_key: bfloat16 [32768, 512], P('sp', 'tp'), may hold values from -6 to 6
- narrow_value: bfloat16 [32768, 512], P('sp', 'tp'), may hold values from -6 to 6
- narrow_gate: bfloat16 [32768, 512], P('sp', 'tp'), may hold values from -6 to 6
- wide_decay: float32 [12, 32768], P('tp', 'sp'), may hold values from -1 to 0
- narrow_decay: float32 [8, 32768], P('tp', 'sp'), may hold values from -1 to 0
- residual: bfloat16 [32768, 2048], P(('sp', 'tp')), may hold values from -6 to 6
- wide_out: bfloat16 [1536, 2048], P('tp'), may hold values from -0.125 to 0.125
- narrow_out: bfloat16 [512, 2048], P('tp'), may hold values from -0.125 to 0.125
- up_weight: bfloat16 [2048, 8192], P('sp', 'tp'), may hold values from -0.125 to 0.125
- down_weight: bfloat16 [8192, 2048], P('tp', 'sp'), may hold values from -0.0625 to 0.0625
- gain_mix: float32 [2048], replicated, may hold values from 0.1 to 1.9
- gain_pre: float32 [2048], replicated, may hold values from 0.1 to 1.9
- gain_mlp: float32 [2048], replicated, may hold values from 0.1 to 1.9
Outputs:
- result: bfloat16 [32768, 2048], P(('sp', 'tp'))
All inputs are finite; a program needn't handle non-finite values.
Results may differ from a plain program's by a relative error of at most 0.02.
Values may be sent and summed in bfloat16 or wider, within the bound.
No kernel may reach another device: no remote copies, remote signals or barrier semaphores. Data moves between devices by JAX's collectives and lax.ppermute only.
A program may use at most 128 MiB of HBM per device.

v0:
```python
import jax
import jax.numpy as jnp
from jax import lax
from jax.sharding import Mesh
from jax.sharding import PartitionSpec as P

WIDE_DIM = 128
NARROW_DIM = 64
SPAN = 128
SP = ("sp_0", "sp_1", "sp_2")
SP_TP = ("sp_0", "sp_1", "sp_2", "tp")


epsilon = 1e-06


def filled_with(array, identity):
    return jax.tree.map(
        lambda a, e: jnp.broadcast_to(jnp.asarray(e, a.dtype), a.shape), array, identity
    )


def gathered_once(array, axis):
    leaves = jax.tree.leaves(array)
    turns = sorted(range(len(leaves)), key=lambda k: -leaves[k].size)
    width = (1, *leaves[turns[0]].shape)[-1]
    lines = [
        jnp.pad(leaves[k].reshape(-1), (0, -leaves[k].size % width)).reshape(-1, width)
        for k in turns
    ]
    both, at, found = (lax.all_gather(jnp.concatenate(lines), axis), 0, {})
    for k, line in zip(turns, lines):
        section = both[:, at : at + len(line)].reshape(len(both), -1)
        found[k] = section[:, : leaves[k].size].reshape(-1, *leaves[k].shape)
        at += len(line)
    numbers = iter(range(len(leaves)))
    return jax.tree.map(lambda _: found[next(numbers)], array)


def entering_2(array, axes, combine, identity):
    before = start = filled_with(array, identity)
    total = array
    for axis in reversed(axes):
        devices, position = (lax.axis_size(axis), lax.axis_index(axis))
        pieces = gathered_once(
            jax.tree.map(
                lambda part, kind: part.astype(kind),
                total,
                (jnp.bfloat16, jnp.bfloat16, jnp.bfloat16, jnp.bfloat16),
            ),
            axis,
        )
        inside, total = (start, start)
        for k in range(devices):
            passed = k < position
            total = combine(
                total, jax.tree.map(lambda part, own: part[k].astype(own.dtype), pieces, array)
            )
            inside = jax.tree.map(lambda new, old: jnp.where(passed, new, old), total, inside)
        before = combine(inside, before)
    return before


def in_blocks(array, dim, devices):
    dims = array.shape
    tiles = array.reshape(*dims[:dim], devices, dims[dim] // devices, *dims[dim + 1 :])
    return jnp.moveaxis(tiles, dim, 0)


def sent_and_summed(array, axis, dim):
    devices = lax.axis_size(axis)
    tiles = lax.all_to_all(in_blocks(array, dim, devices), axis, 0, 0, tiled=True)
    return jnp.sum(tiles.astype(jnp.float32), axis=0)


def from_everyone(array, axis):
    devices = lax.axis_size(axis)
    return lax.all_to_all(
        jnp.broadcast_to(array[None], (devices, *array.shape)), axis, 0, 0, tiled=True
    )


def joined_along(tiles, dim):
    tiles = jnp.moveaxis(tiles, 0, dim)
    dims = tiles.shape
    return tiles.reshape(*dims[:dim], dims[dim] * dims[dim + 1], *dims[dim + 2 :])


def collect(array, axis, dim):
    tiles = from_everyone(array, axis)
    return joined_along(tiles, dim)


def rotate(packed, head_dim, positions):
    length = packed.shape[0]
    grouped = packed.astype(jnp.float32).reshape(length, -1, head_dim)
    halfway = head_dim // 2
    inverse = 10000.0 ** (-jnp.arange(0, head_dim, 2, dtype=jnp.float32) / head_dim)
    angles = positions.astype(jnp.float32)[:, None] * inverse[None, :]
    cosine_table = jnp.cos(angles)[:, None, :]
    sine_table = jnp.sin(angles)[:, None, :]
    leading = grouped[..., :halfway]
    trailing = grouped[..., halfway:]
    return jnp.concatenate(
        [
            leading * cosine_table - trailing * sine_table,
            leading * sine_table + trailing * cosine_table,
        ],
        axis=-1,
    )


def rms_scale(values, gain_vector):
    return (
        values
        * lax.rsqrt(jnp.mean(values * values, axis=-1, keepdims=True) + epsilon)
        * gain_vector
    )


def span_terms(query, key, value, log_decay, head_dim, offset):
    length = query.shape[0]
    count_of_heads = query.shape[1] // head_dim
    span_count = length // SPAN
    shaped = (span_count, SPAN, count_of_heads, head_dim)
    positions = offset + jnp.arange(length, dtype=jnp.int32)
    queries = rotate(query, head_dim, positions).astype(jnp.bfloat16).reshape(shaped)
    keys_full = (rotate(key, head_dim, positions) * head_dim ** (-0.5)).reshape(shaped)
    keys_half = keys_full.astype(jnp.bfloat16)
    values_all = value.reshape(shaped)
    cumulative = jnp.cumsum(log_decay.T.reshape(span_count, SPAN, count_of_heads), axis=1)
    causal = jnp.arange(SPAN)[:, None] >= jnp.arange(SPAN)[None, :]
    scores = jnp.einsum("nihd,njhd->nhij", queries, keys_half, preferred_element_type=jnp.float32)
    decay_rows = cumulative.transpose(0, 2, 1)
    log_gaps = jnp.where(causal, decay_rows[..., :, None] - decay_rows[..., None, :], -jnp.inf)
    weights = (scores * jnp.exp(log_gaps)).astype(jnp.bfloat16)
    within = jnp.einsum("nhij,njhd->nihd", weights, values_all, preferred_element_type=jnp.float32)
    span_total = cumulative[:, -1, :]
    scaled = (keys_full * jnp.exp(span_total[:, None, :] - cumulative)[..., None]).astype(
        jnp.bfloat16
    )
    own_state = jnp.einsum(
        "njhd,njhe->nhde", scaled, values_all, preferred_element_type=jnp.float32
    )

    def advance(carried, inputs):
        decay_sum, contribution = inputs
        return (carried * jnp.exp(decay_sum)[:, None, None] + contribution, carried)

    initial = jnp.zeros((count_of_heads, head_dim, head_dim), jnp.float32)
    closing, before = lax.scan(advance, initial, (span_total, own_state))
    device_decay = jnp.exp(jnp.sum(span_total, axis=0))
    return (queries, cumulative, within, span_total, before, closing, device_decay)


def finish(parts, prefix, gate, head_dim):
    queries, cumulative, within, span_total, before, closing, device_decay = parts
    length = gate.shape[0]
    earlier = jnp.cumsum(span_total, axis=0) - span_total
    entering = (prefix[None] * jnp.exp(earlier)[:, :, None, None] + before).astype(jnp.bfloat16)
    across = (
        jnp.einsum("nihd,nhde->nihe", queries, entering, preferred_element_type=jnp.float32)
        * jnp.exp(cumulative)[..., None]
    )
    output = (within + across).reshape(length, -1, head_dim)
    normed = output * lax.rsqrt(jnp.mean(output * output, axis=-1, keepdims=True) + epsilon)
    return (normed.reshape(length, -1) * jax.nn.silu(gate.astype(jnp.float32))).astype(jnp.bfloat16)


def combine_states(former, latter):
    return (
        former[0] * latter[0],
        former[1] * latter[0][:, None, None] + latter[1],
        former[2] * latter[2],
        former[3] * latter[2][:, None, None] + latter[3],
    )


def local(
    wide_query,
    wide_key,
    wide_value,
    wide_gate,
    narrow_query,
    narrow_key,
    narrow_value,
    narrow_gate,
    wide_decay,
    narrow_decay,
    residual,
    wide_out,
    narrow_out,
    up_weight,
    down_weight,
    gain_mix,
    gain_pre,
    gain_mlp,
):
    length = wide_query.shape[0]
    offset = lax.axis_index(SP) * length
    wide_parts = span_terms(wide_query, wide_key, wide_value, wide_decay, WIDE_DIM, offset)
    narrow_parts = span_terms(
        narrow_query, narrow_key, narrow_value, narrow_decay, NARROW_DIM, offset
    )
    identity = (
        jnp.ones_like(wide_parts[6]),
        jnp.zeros_like(wide_parts[5]),
        jnp.ones_like(narrow_parts[6]),
        jnp.zeros_like(narrow_parts[5]),
    )
    prefixes = entering_2(
        (wide_parts[6], wide_parts[5], narrow_parts[6], narrow_parts[5]),
        SP,
        combine_states,
        identity,
    )
    wide_mixed = finish(wide_parts, prefixes[1], wide_gate, WIDE_DIM)
    narrow_mixed = finish(narrow_parts, prefixes[3], narrow_gate, NARROW_DIM)
    projected = sent_and_summed(
        (
            jnp.dot(wide_mixed, wide_out, preferred_element_type=jnp.float32)
            + jnp.dot(narrow_mixed, narrow_out, preferred_element_type=jnp.float32)
        ).astype(jnp.bfloat16),
        "tp",
        0,
    )
    updated = (residual.astype(jnp.float32) + rms_scale(projected, gain_mix)).astype(jnp.bfloat16)
    normed = rms_scale(updated.astype(jnp.float32), gain_pre).astype(jnp.bfloat16)
    block_rows = collect(normed, "tp", 0)
    rectified = jax.nn.relu(
        jnp.dot(
            block_rows,
            lax.all_gather(up_weight, SP, axis=0, tiled=True),
            preferred_element_type=jnp.float32,
        )
    )
    hidden = (rectified * rectified).astype(jnp.bfloat16)
    partial_terms = jnp.dot(
        hidden,
        lax.all_gather(down_weight, SP, axis=1, tiled=True),
        preferred_element_type=jnp.float32,
    )
    lowered = sent_and_summed(partial_terms.astype(jnp.bfloat16), "tp", 0)
    return (updated.astype(jnp.float32) + rms_scale(lowered, gain_mlp)).astype(jnp.bfloat16)


def solution(mesh):
    finer = Mesh(mesh.devices.reshape(8, 4, 2, mesh.shape["tp"]), ("sp_0", "sp_1", "sp_2", "tp"))
    in_specs = (
        P(SP, "tp"),
        P(SP, "tp"),
        P(SP, "tp"),
        P(SP, "tp"),
        P(SP, "tp"),
        P(SP, "tp"),
        P(SP, "tp"),
        P(SP, "tp"),
        P("tp", SP),
        P("tp", SP),
        P(SP_TP, None),
        P("tp", None),
        P("tp", None),
        P(SP, "tp"),
        P("tp", SP),
        P(),
        P(),
        P(),
    )
    out_specs = P(SP_TP, None)
    return jax.shard_map(local, mesh=finer, in_specs=in_specs, out_specs=out_specs, check_vma=False)
```

profile of v0, /device:TPU:32, one launch (start us, length us, event | category | flops | bytes accessed | tf_op | source)
XLA Modules:
  0.0 278.3 jit_solution(16099406056745294829)
XLA Ops:
  20.7 2.1 reshape.1134
  22.7 2.8 fusion.27
  25.5 6.9 %while.26 = (s32[]{:T(128)}, f32[3,128,128]{2,1,0:T(8,128)S(1)}, f32[4,3,128,128]{3,2,1,0:T(8,128)}, f32[4,3]{1,0:T(4,128)S(1)}, f32[4,3,128,128]{3,2,1,0:T(8,128)}, /*index=5*/s32[]{:T(128)}, s32[]{:T(128)}) while((s32[]{:T(128)}, f32[3,128,128]{2,1,0:T(8,128)S(1)}, f32[4,3,128,128]{3,2,1,0:T(8,128)}, f32[4,3]{1,0:T(4,128)S(1)}, ...), condition=%wide.region_2.3_spmd.clone, body=%wide.region_1.2_spmd.clone.sunk | while | flops 196611 | bytes 983684 | solution.py:151
  34.1 1.7 copy.143
  36.6 1.7 copy.130
  39.2 1.6 add_bitcast_fusion
  41.5 1.7 fusion.106
  45.2 1.6 bitcast_dynamic-update-slice_fusion.2
  48.0 2.9 %while.27 = (s32[]{:T(128)}, f32[2,64,64]{2,1,0:T(8,128)S(1)}, f32[4,2,64,64]{3,2,1,0:T(8,128)}, f32[4,2]{1,0:T(4,128)S(1)}, f32[4,2,64,64]{3,2,1,0:T(8,128)S(1)}, /*index=5*/s32[]{:T(128)}, s32[]{:T(128)}) while((s32[]{:T(128)}, f32[2,64,64]{2,1,0:T(8,128)S(1)}, f32[4,2,64,64]{3,2,1,0:T(8,128)}, f32[4,2]{1,0:T(4,128)S(1)}, ...), condition=%wide.region_5.6_spmd.clone, body=%wide.region_4.5_spmd.clone.sunk | while | flops 32771 | bytes 197240 | solution.py:151
  51.9 2.0 all-gather.3
  55.1 14.5 %all-gather.4 = bf16[4,450,128]{2,1,0:T(8,128)(2,1)S(1)} all-gather(bf16[1,450,128]{2,1,0:T(8,128)(2,1)S(1)} %maximum_bitcast_fusion.1), channel_id=3, replica_groups=mesh['sp_0'=8,'sp_1'=4,'sp_2'=2,'tp'=4] {'sp_1'}, dimensions={0}, use_global_device_ids=true | all-gather | bytes 576000 | tf_op jit(solution)/shard_map/all_gather | solution.py:31
  76.8 31.4 %all-gather.5 = bf16[8,450,128]{2,1,0:T(8,128)(2,1)S(1)} all-gather(bf16[1,450,128]{2,1,0:T(8,128)(2,1)S(1)} %maximum_bitcast_fusion.2), channel_id=4, replica_groups=mesh['sp_0'=8,'sp_1'=4,'sp_2'=2,'tp'=4] {'sp_0'}, dimensions={0}, use_global_device_ids=true | all-gather | bytes 1036800 | tf_op jit(solution)/shard_map/all_gather | solution.py:31
  110.4 1.7 concatenate.43
  113.2 1.7 concatenate.44
  114.9 1.9 copy.116
  128.1 3.9 %multiply_reduce_fusion.2 = (f32[4,128,3]{1,2,0:T(4,128)}, f32[4,128,3,128]{1,3,2,0:T(8,128)}) fusion(f32[4,128,3,128]{1,3,2,0:T(8,128)} %fusion.4, bf16[4,128,3,128]{3,2,1,0:T(4,128)(2,1)} %reshape.1134, f32[4,3,128]{2,1,0:T(4,128)S(1)} %copy.121, pred[128,128]{1,0:T(8,128)(4,1)} %iota_compare_fusion, f32[4,128,3,64]{3,1,2,0:T(8,128)S(1)} %copy.119, ...), kind=kOutput, calls=%fused_computation.46 | convolution fusion | flops 103414272 | bytes 3174400 | tf_op jit(solution)/shard_map/nhij,njhd->nihd/dot_general | solution.py:137
  132.0 1.7 copy.141
  167.9 2.0 fusion.11
  169.9 2.1 multiply_reduce_fusion.3
  175.0 1.8 fusion.108
  178.1 26.0 %all_to_all.15 = bf16[4,128,2048]{2,1,0:T(8,128)(2,1)S(1)} all-to-all(bf16[4,128,2048]{2,1,0:T(8,128)(2,1)S(1)} %bitcast.416), channel_id=1, replica_groups=mesh['sp_0'=8,'sp_1'=4,'sp_2'=2,'tp'=4] {'tp'}, dimensions={0} | all-to-all | bytes 4194304 | tf_op jit(solution)/shard_map/all_to_all | solution.py:72
  205.5 24.3 %all_to_all.16 = bf16[4,128,2048]{2,1,0:T(8,128)(2,1)} all-to-all(bf16[4,128,2048]{2,1,0:T(8,128)(2,1)S(1)} %broadcast_in_dim.34), channel_id=1, replica_groups=mesh['sp_0'=8,'sp_1'=4,'sp_2'=2,'tp'=4] {'tp'}, dimensions={0} | all-to-all | bytes 4194304 | tf_op jit(solution)/shard_map/all_to_all | solution.py:78
  229.8 16.5 %convolution_convert_fusion = bf16[512,2048]{1,0:T(8,128)(2,1)} fusion(bf16[2048,2048]{0,1:T(8,128)(2,1)} %all-gather.11.cloned.1.call-done, bf16[512,2048]{1,0:T(8,128)(2,1)} %bitcast.420, bf16[2048,2048]{1,0:T(8,128)(2,1)} %all-gather.9.cloned.1.call-done), kind=kOutput, calls=%fused_computation.14 | convolution fusion | flops 8594128896 | bytes 20971520 | tf_op jit(solution)/shard_map/dot_general | solution.py:238
  246.3 23.5 %all_to_all.17 = bf16[4,128,2048]{2,1,0:T(8,128)(2,1)S(1)} all-to-all(bf16[4,128,2048]{2,1,0:T(8,128)(2,1)} %bitcast.421), channel_id=1, replica_groups=mesh['sp_0'=8,'sp_1'=4,'sp_2'=2,'tp'=4] {'tp'}, dimensions={0} | all-to-all | bytes 4194304 | tf_op jit(solution)/shard_map/all_to_all | solution.py:72
  (240 shorter events, 96.2 us)
Async XLA Ops:
  6.5 170.2 %copy-start = (bf16[384,2048]{1,0:T(8,128)(2,1)S(1)}, bf16[384,2048]{1,0:T(8,128)(2,1)}, u32[]{:S(2)}) copy-start(bf16[384,2048]{1,0:T(8,128)(2,1)} %param.33) | copy-start | bytes 4718596
  6.5 7.5 %copy-start.13 = (bf16[512,384]{1,0:T(8,128)(2,1)S(1)}, bf16[512,384]{1,0:T(8,128)(2,1)}, u32[]{:S(2)}) copy-start(bf16[512,384]{1,0:T(8,128)(2,1)} %param.23) | copy-start | bytes 1179652
  6.5 223.3 %all-gather.11.cloned.1.call-start = ((), (), s32[]{:S(2)}) async-start(), calls=%async_computation.4 | async-start | bytes 8519680 | tf_op jit(solution)/shard_map/all_gather | solution.py:240
  7.3 222.5 %all-gather.9.cloned.1.call-start = ((), (), s32[]{:S(2)}) async-start(), calls=%async_computation.3 | async-start | bytes 8519680 | tf_op jit(solution)/shard_map/all_gather | solution.py:233
  9.2 2.4 copy-start.7
  11.8 2.1 copy-start.5
  12.0 5.5 %copy-start.16 = (f32[4,1,2]{0,2,1:T(2,128)}, f32[4,1,2]{0,2,1:T(2,128)S(1)}, u32[]{:S(2)}) copy-start(f32[4,1,2]{0,2,1:T(2,128)S(1)} %copy.129) | copy-start | bytes 100
  32.4 3.3 %copy-start.15 = (f32[4,3]{1,0:T(4,128)}, f32[4,3]{1,0:T(4,128)S(1)}, u32[]{:S(2)}) copy-start(f32[4,3]{1,0:T(4,128)S(1)} %get-tuple-element.357) | copy-start | bytes 148
  53.9 56.5 %copy-start.8 = (bf16[2,450,128]{2,1,0:T(8,128)(2,1)}, bf16[2,450,128]{2,1,0:T(8,128)(2,1)S(1)}, u32[]{:S(2)}) copy-start(bf16[2,450,128]{2,1,0:T(8,128)(2,1)S(1)} %all-gather.3) | copy-start | bytes 691204
  53.9 17.8 %copy-start.21 = (f32[2]{0:T(128)}, f32[2]{0:T(128)S(1)}, u32[]{:S(2)}) copy-start(f32[2]{0:T(128)S(1)} %get-tuple-element.231) | copy-start | bytes 28
  54.1 17.0 %copy-start.30 = (f32[2]{0:T(128)}, f32[2]{0:T(128)S(1)}, u32[]{:S(2)}) copy-start(f32[2]{0:T(128)S(1)} %bitcast_convert_fusion.20) | copy-start | bytes 28
  71.2 45.6 %copy-start.23 = (f32[2]{0:T(128)}, f32[2]{0:T(128)S(1)}, u32[]{:S(2)}) copy-start(f32[2]{0:T(128)S(1)} %get-tuple-element.227) | copy-start | bytes 28
  74.0 42.8 %copy-start.27 = (f32[3]{0:T(128)}, f32[3]{0:T(128)S(1)}, u32[]{:S(2)}) copy-start(f32[3]{0:T(128)S(1)} %get-tuple-element.222) | copy-start | bytes 40
  108.2 1.0 copy-start.3
  119.0 7.6 %copy-start.4 = (bf16[4,128,3,64]{3,1,2,0:T(8,128)(2,1)S(1)}, bf16[4,128,3,64]{3,1,2,0:T(8,128)(2,1)}, u32[]{:S(2)}) copy-start(bf16[4,128,3,64]{3,1,2,0:T(8,128)(2,1)} %copy.116) | copy-start | bytes 589828
  119.0 7.6 %copy-start.10 = (f32[4,3,128,128]{3,2,1,0:T(8,128)S(1)}, f32[4,3,128,128]{3,2,1,0:T(8,128)}, u32[]{:S(2)}) copy-start(f32[4,3,128,128]{3,2,1,0:T(8,128)} %get-tuple-element.63) | copy-start | bytes 2359300
  132.0 28.9 %copy-start.9 = (f32[4,128,2]{2,1,0:T(8,128)S(1)}, f32[4,128,2]{2,1,0:T(8,128)}, u32[]{:S(2)}) copy-start(f32[4,128,2]{2,1,0:T(8,128)} %get-tuple-element.193) | copy-start | bytes 12292
  132.0 30.4 %copy-start.6 = (f32[4,128,2]{2,1,0:T(8,128)S(1)}, f32[4,128,2]{2,1,0:T(8,128)}, u32[]{:S(2)}) copy-start(f32[4,128,2]{2,1,0:T(8,128)} %copy-done.5) | copy-start | bytes 12292
  132.0 37.9 %copy-start.11 = (f32[4,128,2,64]{1,3,2,0:T(8,128)S(1)}, f32[4,128,2,64]{1,3,2,0:T(8,128)}, u32[]{:S(2)}) copy-start(f32[4,128,2,64]{1,3,2,0:T(8,128)} %bitcast_dynamic-update-slice_fusion.2) | copy-start | bytes 786436
  132.0 37.9 %copy-start.14 = (pred[128,128]{1,0:T(8,128)(4,1)S(1)}, pred[128,128]{1,0:T(8,128)(4,1)}, u32[]{:S(2)}) copy-start(pred[128,128]{1,0:T(8,128)(4,1)} %iota_compare_fusion) | copy-start | bytes 49156
  178.1 26.6 %copy-start.12 = (bf16[128,2048]{1,0:T(8,128)(2,1)S(1)}, bf16[128,2048]{1,0:T(8,128)(2,1)}, u32[]{:S(2)}) copy-start(bf16[128,2048]{1,0:T(8,128)(2,1)} %param.32) | copy-start | bytes 1572868
  178.1 26.6 %copy-start.17 = (f32[2048]{0:T(1024)S(1)}, f32[2048]{0:T(1024)}, u32[]{:S(2)}) copy-start(f32[2048]{0:T(1024)} %param.37) | copy-start | bytes 24580
  246.3 24.1 %copy-start.19 = (f32[2048]{0:T(1024)S(1)}, f32[2048]{0:T(1024)}, u32[]{:S(2)}) copy-start(f32[2048]{0:T(1024)} %param.39) | copy-start | bytes 24580
  246.3 25.1 %copy-start.1 = (bf16[384,2048]{1,0:T(8,128)(2,1)S(1)}, bf16[384,2048]{1,0:T(8,128)(2,1)}, u32[]{:S(2)}) copy-start(bf16[384,2048]{1,0:T(8,128)(2,1)} %param.33) | copy-start | bytes 4718596
  (10 other events, 6.7 us)
Sparse Core Ops, SparseCore 0:
  10.1 90.0 all-gather.10
  103.0 79.5 all-gather.8
where the time goes:
time: 281 us; the launch traced here: 278 us
  blocking collectives  122 us (43%)
  local copies, waits for them, and re-layouts  63.5 us (23%)
  other arithmetic  44.5 us (16%)
  matrix products  33 us (12%)
  between operations  14 us (5%)
    all_to_all x2, blocking collectives, sent_and_summed(): lax.all_to_all(in_blocks(array, dim, devices), axis, 0, 0, tiled=True)  49.5 us
    all_gather x3, blocking collectives, gathered_once(): both, at, found = (lax.all_gather(jnp.concatenate(lines), axis), 0, {})  47.9 us
    all_to_all x1, blocking collectives, from_everyone(): lax.all_to_all(jnp.broadcast_to(array[None], (devices, *array.shape)), ax...  24.3 us
    convert_element_type x14, local copies, waits for them, and re-layouts, entering_2(): part[k].astype(own.dtype)  20.4 us
    dot_general x1, matrix products, local(): jnp.dot(hidden, lax.all_gather(down_weight, SP, axis=1, tiled=True), pref...  16.5 us
    unnamed x79, local copies, waits for them, and re-layouts  13.4 us
    concatenate x10, local copies, waits for them, and re-layouts, rotate(): jnp.concatenate([leading * cosine_table - trailing * sine_table, leading...  12.4 us
    convert_element_type x11, other arithmetic, entering_2(): part[k].astype(own.dtype)  8.29 us
  transfers between devices with their start and end apart: 2, of which 0 were waited for; matrix products, arithmetic and copies ran while one was open for 43% of the time, Pallas kernels for 0%

commit v1 on v0

v1 whole, which is shorter than its diff:
```python
import functools

import jax
import jax.numpy as jnp
import numpy as np
from jax import lax
from jax.experimental import pallas as pl
from jax.experimental.pallas import tpu as pltpu
from jax.sharding import Mesh
from jax.sharding import PartitionSpec as P

SPAN = 128
LANES = 128
SPANS = 4
SP = ("sp_0", "sp_1", "sp_2")
SP_TP = ("sp_0", "sp_1", "sp_2", "tp")
EPS = 1e-06
WIDE_SCALE = 128 ** (-0.5)
NARROW_SCALE = 64 ** (-0.5)
F32 = jnp.float32
BF16 = jnp.bfloat16


def position_tables(devices):
    lane = np.arange(LANES)

    def inverse(head_dim):
        half = head_dim // 2
        return 10000.0 ** (-2.0 * (lane % half) / head_dim), np.where(
            lane % head_dim < half, -1.0, 1.0
        )

    row = np.arange(SPAN)[:, None]
    first = (np.arange(devices * SPANS) * SPAN)[:, None]
    inside, starts = [], []
    for head_dim in (128, 64):
        rate, sign = inverse(head_dim)
        inside += [np.cos(row * rate), np.sin(row * rate) * sign]
        starts += [
            np.cos(first * rate).reshape(devices, SPANS, LANES),
            (np.sin(first * rate) * sign).reshape(devices, SPANS, LANES),
        ]
    return (
        np.stack(inside).astype(np.float32),
        np.concatenate(starts, axis=1).astype(np.float32),
    )


def span_tables(inside_ref, start_ref, span, group):
    cos_row, sin_row = inside_ref[2 * group], inside_ref[2 * group + 1]
    cos_start = start_ref[0, pl.ds(2 * group * SPANS + span, 1), :]
    sin_start = start_ref[0, pl.ds((2 * group + 1) * SPANS + span, 1), :]
    return (
        cos_row * cos_start - sin_row * sin_start,
        sin_row * cos_start + cos_row * sin_start,
    )


def rotated_wide(x, tables):
    x = x.astype(F32)
    return x * tables[0] + pltpu.roll(x, 64, 1) * tables[1]


def rotated_narrow(x, tables):
    x = x.astype(F32)
    lane = lax.broadcasted_iota(jnp.int32, x.shape, 1)
    partner = jnp.where((lane & 32) == 0, pltpu.roll(x, 96, 1), pltpu.roll(x, 32, 1))
    return x * tables[0] + partner * tables[1]


def running_decay(wide_decay_ref, narrow_decay_ref, rows_ref):
    rows_ref[...] = jnp.zeros_like(rows_ref)
    rows_ref[0:3, :] = wide_decay_ref[...]
    rows_ref[3:5, :] = narrow_decay_ref[...]
    x = rows_ref[...]
    lane = lax.broadcasted_iota(jnp.int32, x.shape, 1)
    step = 1
    while step < SPAN:
        x = x + jnp.where(lane >= step, pltpu.roll(x, step, 1), 0.0)
        step *= 2
    return x


def low_rows(shape):
    return lax.broadcasted_iota(jnp.int32, shape, 0) < 64


def low_lanes(shape):
    return lax.broadcasted_iota(jnp.int32, shape, 1) < 64


def mm(a, b):
    return jnp.dot(a, b, preferred_element_type=F32)


def mm_nt(a, b):
    return lax.dot_general(a, b, (((1,), (1,)), ((), ())), preferred_element_type=F32)


def mm_tn(a, b):
    return lax.dot_general(a, b, (((0,), (0,)), ((), ())), preferred_element_type=F32)


def states_kernel(
    _, wk_ref, wv_ref, nk_ref, nv_ref, wd_ref, nd_ref, inside_ref, start_ref,
    before_ref, message_ref, rows_ref, state_ref, decay_ref,
):
    span = pl.program_id(0)

    @pl.when(span == 0)
    def _():
        state_ref[...] = jnp.zeros_like(state_ref)
        decay_ref[...] = jnp.zeros_like(decay_ref)

    total = running_decay(wd_ref, nd_ref, rows_ref)
    last = total[:, SPAN - 1 : SPAN]
    tail = jnp.exp(last - total).T
    kept = jnp.exp(last)
    before_ref[0] = state_ref[...]
    tables = span_tables(inside_ref, start_ref, span, 0)
    for head in range(3):
        cut = slice(head * 128, head * 128 + 128)
        keys = rotated_wide(wk_ref[:, cut], tables) * WIDE_SCALE
        scaled = (keys * tail[:, head : head + 1]).astype(BF16)
        state_ref[cut, :] = state_ref[cut, :] * kept[head : head + 1, :] + mm_tn(scaled, wv_ref[:, cut])
    tables = span_tables(inside_ref, start_ref, span, 1)
    keys = rotated_narrow(nk_ref[...], tables) * NARROW_SCALE
    tails = jnp.where(low_lanes((SPAN, LANES)), tail[:, 3:4], tail[:, 4:5])
    own = mm_tn((keys * tails).astype(BF16), nv_ref[...])
    square = (LANES, LANES)
    own = jnp.where(low_rows(square) == low_lanes(square), own, 0.0)
    keeps = jnp.where(low_rows(square), kept[3:4, :], kept[4:5, :])
    state_ref[384:512, :] = state_ref[384:512, :] * keeps + own
    decay_ref[...] += jnp.broadcast_to(last, decay_ref.shape)

    @pl.when(span == SPANS - 1)
    def _():
        sums = decay_ref[...]
        high = sums.astype(BF16).astype(F32)
        low = sums - high
        sub = lax.broadcasted_iota(jnp.int32, (8, LANES), 0)
        at = 0
        for head, count in enumerate((16, 16, 16, 8, 8)):
            pair = jnp.where(
                sub == 0,
                high[head : head + 1, :],
                jnp.where(sub == 1, low[head : head + 1, :], 0.0),
            )
            body = state_ref[at * 8 : (at + count) * 8, :].reshape(count, 8, LANES)
            ends = jnp.broadcast_to(pair[None], (count, 8, LANES))
            message_ref[at : at + count] = jnp.concatenate([body, ends], axis=1).astype(BF16)
            at += count


def prefix_kernel(message_ref, out_ref):
    devices = message_ref.shape[0]
    carried = jnp.zeros((8, LANES), F32)
    for k in range(devices):
        out_ref[k] = carried.astype(BF16)
        if k + 1 < devices:
            piece = message_ref[k].astype(F32)
            kept = jnp.exp(piece[8:9, :] + piece[9:10, :])
            carried = carried * kept + piece[0:8, :]


def gated(output, gate, scale):
    gate = gate.astype(F32)
    return (output * scale * (gate / (1.0 + jnp.exp(-gate)))).astype(BF16)


def finish_kernel(
    _, wq_ref, wk_ref, wv_ref, wg_ref, nq_ref, nk_ref, nv_ref, ng_ref, wd_ref, nd_ref,
    inside_ref, start_ref, before_ref, prefix_ref, wide_out_ref, narrow_out_ref,
    out_ref, rows_ref, decay_ref, mixed_ref,
):
    span = pl.program_id(0)

    @pl.when(span == 0)
    def _():
        decay_ref[...] = jnp.zeros_like(decay_ref)

    total = running_decay(wd_ref, nd_ref, rows_ref)
    columns = total.T
    grown = jnp.exp(columns)
    earlier = jnp.exp(decay_ref[...])
    square = (SPAN, SPAN)
    causal = lax.broadcasted_iota(jnp.int32, square, 0) >= lax.broadcasted_iota(jnp.int32, square, 1)

    def weights(scores, head):
        gaps = columns[:, head : head + 1] - total[head : head + 1, :]
        return (scores * jnp.exp(jnp.where(causal, gaps, -jnp.inf))).astype(BF16)

    tables = span_tables(inside_ref, start_ref, span, 0)
    for head in range(3):
        cut = slice(head * 128, head * 128 + 128)
        queries = rotated_wide(wq_ref[:, cut], tables).astype(BF16)
        keys = (rotated_wide(wk_ref[:, cut], tables) * WIDE_SCALE).astype(BF16)
        within = mm(weights(mm_nt(queries, keys), head), wv_ref[:, cut])
        entering = (
            prefix_ref[cut, :].astype(F32) * earlier[head : head + 1, :] + before_ref[0, cut, :]
        ).astype(BF16)
        output = within + mm(queries, entering) * grown[:, head : head + 1]
        scale = lax.rsqrt(jnp.mean(output * output, axis=-1, keepdims=True) + EPS)
        mixed_ref[:, cut] = gated(output, wg_ref[:, cut], scale)

    tables = span_tables(inside_ref, start_ref, span, 1)
    queries = rotated_narrow(nq_ref[...], tables).astype(BF16)
    keys = (rotated_narrow(nk_ref[...], tables) * NARROW_SCALE).astype(BF16)
    values = nv_ref[...]
    low = low_lanes(square)
    none = jnp.zeros_like(queries)
    within = jnp.where(
        low,
        mm(weights(mm_nt(jnp.where(low, queries, none), keys), 3), values),
        mm(weights(mm_nt(jnp.where(low, none, queries), keys), 4), values),
    )
    fades = jnp.where(low_rows(square), earlier[3:4, :], earlier[4:5, :])
    entering = (prefix_ref[384:512, :].astype(F32) * fades + before_ref[0, 384:512, :]).astype(BF16)
    output = within + mm(queries, entering) * jnp.where(low, grown[:, 3:4], grown[:, 4:5])
    squares = output * output
    first = jnp.sum(jnp.where(low, squares, 0.0), axis=-1, keepdims=True)
    second = jnp.sum(jnp.where(low, 0.0, squares), axis=-1, keepdims=True)
    scale = lax.rsqrt(jnp.where(low, first, second) * (1.0 / 64.0) + EPS)
    mixed_ref[:, 384:512] = gated(output, ng_ref[...], scale)
    decay_ref[...] += jnp.broadcast_to(total[:, SPAN - 1 : SPAN], decay_ref.shape)

    out_ref[0] = (
        mm(mixed_ref[:, 0:384], wide_out_ref[...]) + mm(mixed_ref[:, 384:512], narrow_out_ref[...])
    ).astype(BF16)


def rms(values, gain):
    return values * lax.rsqrt(jnp.mean(values * values, axis=-1, keepdims=True) + EPS) * gain


def norms_kernel(tiles_ref, residual_ref, mix_ref, pre_ref, updated_ref, normed_ref):
    projected = tiles_ref[0].astype(F32)
    for k in range(1, tiles_ref.shape[0]):
        projected = projected + tiles_ref[k].astype(F32)
    updated = (residual_ref[...].astype(F32) + rms(projected, mix_ref[...])).astype(BF16)
    updated_ref[...] = updated
    normed = rms(updated.astype(F32), pre_ref[...]).astype(BF16)
    for k in range(normed_ref.shape[0]):
        normed_ref[k] = normed


def mixer_kernel(x_ref, up_ref, down_ref, out_ref, hidden_ref, *, steps, block):
    step = pl.program_id(0)

    @pl.when(step < steps)
    def _():
        weight = up_ref[...].reshape(x_ref.shape[1], block)
        rectified = jnp.maximum(mm(x_ref[...], weight), 0.0)
        at = pl.multiple_of(step * block, block)
        hidden_ref[:, pl.ds(at, block)] = (rectified * rectified).astype(BF16)

    @pl.when(step >= steps)
    def _():
        weight = down_ref[...].reshape(block, hidden_ref.shape[1])
        out_ref[...] = mm_nt(hidden_ref[...], weight).astype(BF16)


def local(
    wide_query, wide_key, wide_value, wide_gate,
    narrow_query, narrow_key, narrow_value, narrow_gate,
    wide_decay, narrow_decay, residual, wide_out, narrow_out,
    up_weight, down_weight, gain_mix, gain_pre, gain_mlp,
):
    devices = lax.axis_size(SP)
    ranks = lax.axis_size("tp")
    length, width = wide_query.shape[0], residual.shape[1]
    rows = residual.shape[0]
    share = up_weight.shape[0]
    units = up_weight.shape[1]

    both = lax.all_gather(
        jnp.concatenate([up_weight, down_weight.T], axis=0), SP, axis=0, tiled=True
    ).reshape(devices, 2, share, units)

    inside, starts = (jnp.asarray(t) for t in position_tables(devices))
    index = lax.axis_index(SP).astype(jnp.int32).reshape(1)
    wide_block = pl.BlockSpec((SPAN, 384), lambda s, i: (s, 0))
    narrow_block = pl.BlockSpec((SPAN, 128), lambda s, i: (s, 0))
    decay_blocks = [
        pl.BlockSpec((3, SPAN), lambda s, i: (0, s)),
        pl.BlockSpec((2, SPAN), lambda s, i: (0, s)),
    ]
    table_blocks = [
        pl.BlockSpec((4, SPAN, LANES), lambda s, i: (0, 0, 0)),
        pl.BlockSpec((1, 4 * SPANS, LANES), lambda s, i: (i[0], 0, 0)),
    ]
    before_block = pl.BlockSpec((1, 512, LANES), lambda s, i: (s, 0, 0))
    before, message = pl.pallas_call(
        states_kernel,
        out_shape=(
            jax.ShapeDtypeStruct((SPANS, 512, LANES), F32),
            jax.ShapeDtypeStruct((devices, 16, LANES), BF16),
        ),
        grid_spec=pltpu.PrefetchScalarGridSpec(
            num_scalar_prefetch=1,
            grid=(SPANS,),
            in_specs=[wide_block, wide_block, narrow_block, narrow_block, *decay_blocks, *table_blocks],
            out_specs=[
                before_block,
                pl.BlockSpec((devices, 16, LANES), lambda s, i: (0, 0, 0)),
            ],
            scratch_shapes=[
                pltpu.VMEM((8, LANES), F32),
                pltpu.VMEM((512, LANES), F32),
                pltpu.VMEM((8, LANES), F32),
            ],
        ),
        name="states",
        cost_estimate=pl.CostEstimate(flops=60_000_000, bytes_accessed=2_500_000, transcendentals=20_000),
    )(index, wide_key, wide_value, narrow_key, narrow_value, wide_decay, narrow_decay, inside, starts)

    arrived = lax.all_to_all(message, SP, 0, 0, tiled=True)
    prefixes = pl.pallas_call(
        prefix_kernel,
        out_shape=jax.ShapeDtypeStruct((devices, 8, LANES), BF16),
        name="prefix",
        cost_estimate=pl.CostEstimate(flops=2_000_000, bytes_accessed=400_000, transcendentals=8_000),
    )(arrived)
    prefix = lax.all_to_all(prefixes, SP, 0, 0, tiled=True).reshape(512, LANES)

    partial = pl.pallas_call(
        finish_kernel,
        out_shape=jax.ShapeDtypeStruct((SPANS, SPAN, width), BF16),
        grid_spec=pltpu.PrefetchScalarGridSpec(
            num_scalar_prefetch=1,
            grid=(SPANS,),
            in_specs=[
                wide_block, wide_block, wide_block, wide_block,
                narrow_block, narrow_block, narrow_block, narrow_block,
                *decay_blocks, *table_blocks, before_block,
                pl.BlockSpec((512, LANES), lambda s, i: (0, 0)),
                pl.BlockSpec((384, width), lambda s, i: (0, 0)),
                pl.BlockSpec((128, width), lambda s, i: (0, 0)),
            ],
            out_specs=pl.BlockSpec((1, SPAN, width), lambda s, i: (s, 0, 0)),
            scratch_shapes=[
                pltpu.VMEM((8, LANES), F32),
                pltpu.VMEM((8, LANES), F32),
                pltpu.VMEM((SPAN, 512), BF16),
            ],
        ),
        name="finish",
        cost_estimate=pl.CostEstimate(flops=1_400_000_000, bytes_accessed=9_000_000, transcendentals=600_000),
    )(
        index, wide_query, wide_key, wide_value, wide_gate,
        narrow_query, narrow_key, narrow_value, narrow_gate,
        wide_decay, narrow_decay, inside, starts, before, prefix, wide_out, narrow_out,
    )

    tiles = lax.all_to_all(partial.reshape(ranks, rows, width), "tp", 0, 0, tiled=True)
    updated, normed = pl.pallas_call(
        norms_kernel,
        out_shape=(
            jax.ShapeDtypeStruct((rows, width), BF16),
            jax.ShapeDtypeStruct((ranks, rows, width), BF16),
        ),
        name="norms",
        cost_estimate=pl.CostEstimate(flops=4_000_000, bytes_accessed=6_000_000, transcendentals=300),
    )(tiles, residual, gain_mix.reshape(1, width), gain_pre.reshape(1, width))
    block_rows = lax.all_to_all(normed, "tp", 0, 0, tiled=True).reshape(length, width)

    block = 256
    steps = units // block
    lowered = pl.pallas_call(
        functools.partial(mixer_kernel, steps=steps, block=block),
        out_shape=jax.ShapeDtypeStruct((length, width), BF16),
        grid=(2 * steps,),
        in_specs=[
            pl.BlockSpec((length, width), lambda i: (0, 0)),
            pl.BlockSpec((devices, 1, share, block), lambda i: (0, 0, 0, jnp.minimum(i, steps - 1))),
            pl.BlockSpec(
                (block // share, 1, share, units), lambda i: (jnp.maximum(i - steps, 0), 1, 0, 0)
            ),
        ],
        out_specs=pl.BlockSpec((length, block), lambda i: (0, jnp.maximum(i - steps, 0))),
        scratch_shapes=[pltpu.VMEM((length, units), BF16)],
        compiler_params=pltpu.CompilerParams(vmem_limit_bytes=32 * 1024 * 1024),
        name="mixer",
        cost_estimate=pl.CostEstimate(
            flops=4 * length * width * units, bytes_accessed=22_000_000, transcendentals=0
        ),
    )(block_rows, both, both)
    lowered = lax.all_to_all(lowered.reshape(ranks, rows, width), "tp", 0, 0, tiled=True)
    lowered = jnp.sum(lowered.astype(F32), axis=0)
    return (updated.astype(F32) + rms(lowered, gain_mlp)).astype(BF16)


def solution(mesh):
    finer = Mesh(mesh.devices.reshape(8, 4, 2, mesh.shape["tp"]), ("sp_0", "sp_1", "sp_2", "tp"))
    in_specs = (
        *([P(SP, "tp")] * 8),
        P("tp", SP),
        P("tp", SP),
        P(SP_TP, None),
        P("tp", None),
        P("tp", None),
        P(SP, "tp"),
        P("tp", SP),
        P(),
        P(),
        P(),
    )
    return jax.shard_map(
        local, mesh=finer, in_specs=in_specs, out_specs=P(SP_TP, None), check_vma=False
    )
```

time: 281 us -> 192 us (0.68)
  local copies, waits for them, and re-layouts: 63.5 us -> 6.26 us
  other arithmetic: 44.5 us -> 3.25 us
  Pallas kernels: 0 us -> 36.7 us
  matrix products: 33 us -> 0 us
  blocking collectives: 122 us -> 131 us
    all_to_all x3 -> x5, blocking collectives: 73.8 us -> 131 us  [the longest x1 31.3 us: local(): lax.all_to_all(partial.reshape(ranks, rows, width), 'tp', 0, 0, tiled=True)]
    all_gather x3 -> x0, blocking collectives: 47.9 us -> none  [gathered_once(): both, at, found = (lax.all_gather(jnp.concatenate(lines), axis), 0, {})]
    pallas_call x0 -> x5, Pallas kernels: none -> 36.7 us  [the longest x1 14.1 us: local(): pl.pallas_call(functools.partial(mixer_kernel, steps=steps, block=block),...]
    dot_general x9 -> x0, matrix products: 33 us -> none  [the longest x1 16.5 us: local(): jnp.dot(hidden, lax.all_gather(down_weight, SP, axis=1, tiled=True), pref...]
    convert_element_type x14 -> x0, local copies, waits for them, and re-layouts: 20.4 us -> none  [entering_2(): part[k].astype(own.dtype)]
    concatenate x10 -> x0, local copies, waits for them, and re-layouts: 12.4 us -> none  [rotate(): jnp.concatenate([leading * cosine_table - trailing * sine_table, leading...]
    convert_element_type x24 -> x1, other arithmetic: 12.9 us -> 1.02 us  [local(): return (updated.astype(F32) + rms(lowered, gain_mlp)).astype(BF16)]
    add x10 -> x0, other arithmetic: 7.19 us -> none  [the longest x8 4.39 us: advance(): return (carried * jnp.exp(decay_sum)[:, None, None] + contribution, carried)]
  transfers between devices with their start and end apart: 2 -> 1, of which waited for: 0 -> 0; matrix products, arithmetic and copies ran while one was open for 43% -> 0% of each run, Pallas kernels for 0% -> 12%
where the time goes in v1:
time: 192 us; the launch traced here: 191 us
  blocking collectives  131 us (68%)
  Pallas kernels  36.7 us (19%)
  between operations  13.4 us (7%)
  local copies, waits for them, and re-layouts  6.26 us (3%)
  other arithmetic  3.25 us (2%)
    all_to_all x1, blocking collectives, local(): lax.all_to_all(partial.reshape(ranks, rows, width), 'tp', 0, 0, tiled=True)  31.3 us
    all_to_all x1, blocking collectives, local(): lax.all_to_all(normed, 'tp', 0, 0, tiled=True).reshape(length, width)  29.6 us
    all_to_all x1, blocking collectives, local(): lax.all_to_all(lowered.reshape(ranks, rows, width), 'tp', 0, 0, tiled=True)  27.6 us
    all_to_all x1, blocking collectives, local(): arrived = lax.all_to_all(message, SP, 0, 0, tiled=True)  26.1 us
    all_to_all x1, blocking collectives, local(): prefix = lax.all_to_all(prefixes, SP, 0, 0, tiled=True).reshape(512, LANES)  16.8 us
    pallas_call x1, Pallas kernels, local(): pl.pallas_call(functools.partial(mixer_kernel, steps=steps, block=block),...  14.1 us
    pallas_call x1, Pallas kernels, local(): pl.pallas_call(finish_kernel, out_shape=jax.ShapeDtypeStruct((SPANS, SPAN...  10.6 us
    pallas_call x1, Pallas kernels, local(): pl.pallas_call(states_kernel, out_shape=(jax.ShapeDtypeStruct((SPANS, 512...  6.41 us
  transfers between devices with their start and end apart: 1, of which 0 were waited for; matrix products, arithmetic and copies ran while one was open for 0% of the time, Pallas kernels for 12%

profile of v1, /device:TPU:32, one launch (start us, length us, event | category | flops | bytes accessed | tf_op | source)
XLA Modules:
  0.0 191.1 jit_solution(1613369341573040832)
XLA Ops:
  6.5 0.0 all-gather.2.cloned.1.call-start
  6.5 1.7 pad_maximum_fusion
  8.2 0.0 all-gather.2.cloned.1.call-update
  8.2 6.4 %states.1 = (f32[4,512,128]{2,1,0:T(8,128)}, bf16[64,16,128]{2,1,0:T(8,128)(2,1)}) custom-call(s32[1]{0:T(128)} %bitcast._, bf16[512,384]{1,0:T(8,128)(2,1)} %wk_ref.3, bf16[512,384]{1,0:T(8,128)(2,1)} %wv_ref.3, bf16[512,128]{1,0:T(8,128)(2,1)} %nk_ref.3, bf16[512,128]{1,0:T(8,128)(2,1)} %nv_ref.3, f32[3,512]{1,0:T(4,128)} %wd_ref.3, f32[2,512]{1,0:T(2,128)} %nd_ref.3, ...), custom_call_target="tpu_custom_call" | custom-call | flops 60000000 | bytes 2500000 | tf_op jit(solution)/shard_map/states/pallas_call | solution.py:293
  14.7 26.1 %all_to_all.25.message_ref = bf16[64,16,128]{2,1,0:T(8,128)(2,1)} all-to-all(bf16[64,16,128]{2,1,0:T(8,128)(2,1)} %get-tuple-element.10), channel_id=1, replica_groups=mesh['sp_0'=8,'sp_1'=4,'sp_2'=2,'tp'=4] {'sp_0','sp_1','sp_2'}, dimensions={0} | all-to-all | bytes 524288 | tf_op jit(solution)/shard_map/all_to_all | solution.py:317
  40.8 1.8 prefix.1
  42.5 16.8 %all_to_all.26 = bf16[64,8,128]{2,1,0:T(8,128)(2,1)} all-to-all(bf16[64,8,128]{2,1,0:T(8,128)(2,1)} %prefix.1), channel_id=1, replica_groups=mesh['sp_0'=8,'sp_1'=4,'sp_2'=2,'tp'=4] {'sp_0','sp_1','sp_2'}, dimensions={0} | all-to-all | bytes 262144 | tf_op jit(solution)/shard_map/all_to_all | solution.py:324
  59.3 10.6 %finish.1 = bf16[4,128,2048]{2,1,0:T(8,128)(2,1)} custom-call(s32[1]{0:T(128)} %bitcast._, bf16[512,384]{1,0:T(8,128)(2,1)} %wq_ref.1, bf16[512,384]{1,0:T(8,128)(2,1)} %wk_ref.3, bf16[512,384]{1,0:T(8,128)(2,1)} %wv_ref.3, bf16[512,384]{1,0:T(8,128)(2,1)} %wg_ref.1, bf16[512,128]{1,0:T(8,128)(2,1)} %nq_ref.1, bf16[512,128]{1,0:T(8,128)(2,1)} %nk_ref.3, ...), custom_call_target="tpu_custom_call" | custom-call | flops 1400000000 | bytes 9000000 | tf_op jit(solution)/shard_map/finish/pallas_call | solution.py:326
  69.9 31.3 %all_to_all.27.tiles_ref = bf16[4,128,2048]{2,1,0:T(8,128)(2,1)} all-to-all(bf16[4,128,2048]{2,1,0:T(8,128)(2,1)} %finish.1), channel_id=1, replica_groups=mesh['sp_0'=8,'sp_1'=4,'sp_2'=2,'tp'=4] {'tp'}, dimensions={0} | all-to-all | bytes 4194304 | tf_op jit(solution)/shard_map/all_to_all | solution.py:355
  101.2 3.9 %norms.1 = (bf16[128,2048]{1,0:T(8,128)(2,1)}, bf16[4,128,2048]{2,1,0:T(8,128)(2,1)}) custom-call(bf16[4,128,2048]{2,1,0:T(8,128)(2,1)} %all_to_all.27.tiles_ref, bf16[128,2048]{1,0:T(8,128)(2,1)} %residual_ref.1, f32[1,2048]{1,0:T(1,128)} %bitcast.14, f32[1,2048]{1,0:T(1,128)} %bitcast.15), custom_call_target="tpu_custom_call" | custom-call | flops 4000000 | bytes 6000000 | tf_op jit(solution)/shard_map/norms/pallas_call | solution.py:356
  105.1 29.6 %all_to_all.28 = bf16[4,128,2048]{2,1,0:T(8,128)(2,1)S(1)} all-to-all(bf16[4,128,2048]{2,1,0:T(8,128)(2,1)} %get-tuple-element.12), channel_id=1, replica_groups=mesh['sp_0'=8,'sp_1'=4,'sp_2'=2,'tp'=4] {'tp'}, dimensions={0} | all-to-all | bytes 4194304 | tf_op jit(solution)/shard_map/all_to_all | solution.py:365
  134.7 0.0 all-gather.2.cloned.1.call-done
  134.7 0.0 copy-start
  134.7 5.8 %copy-done = bf16[4096,2048]{1,0:T(8,128)(2,1)S(1)} copy-done((bf16[4096,2048]{1,0:T(8,128)(2,1)S(1)}, bf16[4096,2048]{1,0:T(8,128)(2,1)}, u32[]{:S(2)}) %copy-start) | copy-done | bytes 16777240
  140.5 14.1 %mixer.1 = bf16[512,2048]{1,0:T(8,128)(2,1)S(1)} custom-call(bf16[512,2048]{1,0:T(8,128)(2,1)S(1)} %bitcast.10, bf16[64,2,32,2048]{3,2,1,0:T(8,128)(2,1)S(1)} %bitcast.8, bf16[64,2,32,2048]{3,2,1,0:T(8,128)(2,1)S(1)} %bitcast.9), custom_call_target="tpu_custom_call" | custom-call | flops 8589934592 | bytes 22000000 | tf_op jit(solution)/shard_map/mixer/pallas_call | solution.py:369
  154.6 27.6 %all_to_all.29 = bf16[4,128,2048]{2,1,0:T(8,128)(2,1)S(1)} all-to-all(bf16[4,128,2048]{2,1,0:T(8,128)(2,1)S(1)} %bitcast.11), channel_id=1, replica_groups=mesh['sp_0'=8,'sp_1'=4,'sp_2'=2,'tp'=4] {'tp'}, dimensions={0} | all-to-all | bytes 4194304 | tf_op jit(solution)/shard_map/all_to_all | solution.py:388
  182.2 0.0 copy-start.1
  182.2 0.0 copy-start.2
  182.2 0.4 convert_reduce_fusion
  182.6 0.2 multiply_reduce_fusion
  182.8 0.5 copy-done.1
  183.2 0.0 copy-done.2
  183.2 1.0 add_convert_fusion
  (1 shorter events, 0.0 us)
Async XLA Ops:
  6.5 128.2 %all-gather.2.cloned.1.call-start = ((), (), s32[]{:S(2)}) async-start(), calls=%async_computation.5 | async-start | bytes 17039360 | tf_op jit(solution)/shard_map/all_gather | solution.py:276
  134.7 5.8 %copy-start = (bf16[4096,2048]{1,0:T(8,128)(2,1)S(1)}, bf16[4096,2048]{1,0:T(8,128)(2,1)}, u32[]{:S(2)}) copy-start(bf16[4096,2048]{1,0:T(8,128)(2,1)} %all-gather.2.cloned.1.call-done) | copy-start | bytes 50331652
  182.2 1.0 copy-start.1
  182.2 1.0 copy-start.2
Sparse Core Ops, SparseCore 0:
  10.1 103.4 all-gather.1

commit v2 on v1

--- a/solution.py
+++ b/solution.py
@@ -103,7 +103,7 @@
 
 def states_kernel(
     _, wk_ref, wv_ref, nk_ref, nv_ref, wd_ref, nd_ref, inside_ref, start_ref,
-    before_ref, message_ref, rows_ref, state_ref, decay_ref,
+    before_ref, earlier_ref, message_ref, rows_ref, state_ref, decay_ref,
 ):
     span = pl.program_id(0)
 
@@ -117,6 +117,7 @@
     tail = jnp.exp(last - total).T
     kept = jnp.exp(last)
     before_ref[0] = state_ref[...]
+    earlier_ref[0] = decay_ref[...]
     tables = span_tables(inside_ref, start_ref, span, 0)
     for head in range(3):
         cut = slice(head * 128, head * 128 + 128)
@@ -169,20 +170,16 @@
 
 
 def finish_kernel(
-    _, wq_ref, wk_ref, wv_ref, wg_ref, nq_ref, nk_ref, nv_ref, ng_ref, wd_ref, nd_ref,
-    inside_ref, start_ref, before_ref, prefix_ref, wide_out_ref, narrow_out_ref,
-    out_ref, rows_ref, decay_ref, mixed_ref,
+    order_ref, wq_ref, wk_ref, wv_ref, wg_ref, nq_ref, nk_ref, nv_ref, ng_ref, wd_ref, nd_ref,
+    inside_ref, start_ref, before_ref, earlier_ref, prefix_ref, wide_out_ref, narrow_out_ref,
+    *out_refs, first,
 ):
-    span = pl.program_id(0)
-
-    @pl.when(span == 0)
-    def _():
-        decay_ref[...] = jnp.zeros_like(decay_ref)
-
+    *out_refs, rows_ref, mixed_ref = out_refs
+    span = order_ref[1 + first + pl.program_id(0)]
     total = running_decay(wd_ref, nd_ref, rows_ref)
     columns = total.T
     grown = jnp.exp(columns)
-    earlier = jnp.exp(decay_ref[...])
+    earlier = jnp.exp(earlier_ref[0])
     square = (SPAN, SPAN)
     causal = lax.broadcasted_iota(jnp.int32, square, 0) >= lax.broadcasted_iota(jnp.int32, square, 1)
 
@@ -218,46 +215,126 @@
     entering = (prefix_ref[384:512, :].astype(F32) * fades + before_ref[0, 384:512, :]).astype(BF16)
     output = within + mm(queries, entering) * jnp.where(low, grown[:, 3:4], grown[:, 4:5])
     squares = output * output
-    first = jnp.sum(jnp.where(low, squares, 0.0), axis=-1, keepdims=True)
-    second = jnp.sum(jnp.where(low, 0.0, squares), axis=-1, keepdims=True)
-    scale = lax.rsqrt(jnp.where(low, first, second) * (1.0 / 64.0) + EPS)
+    left = jnp.sum(jnp.where(low, squares, 0.0), axis=-1, keepdims=True)
+    right = jnp.sum(jnp.where(low, 0.0, squares), axis=-1, keepdims=True)
+    scale = lax.rsqrt(jnp.where(low, left, right) * (1.0 / 64.0) + EPS)
     mixed_ref[:, 384:512] = gated(output, ng_ref[...], scale)
-    decay_ref[...] += jnp.broadcast_to(total[:, SPAN - 1 : SPAN], decay_ref.shape)
-
-    out_ref[0] = (
+
+    projected = (
         mm(mixed_ref[:, 0:384], wide_out_ref[...]) + mm(mixed_ref[:, 384:512], narrow_out_ref[...])
     ).astype(BF16)
+    if len(out_refs) == 2:
+        half = SPAN // 2
+        out_refs[0][...] = projected[:half]
+        out_refs[1][...] = projected[half:]
+    else:
+        out_refs[0][0] = projected
+
+
+def join_kernel(minus_ref, plus_ref, from_below_ref, from_above_ref, minus_out_ref, plus_out_ref):
+    part = pl.program_id(0)
+
+    @pl.when(part == 0)
+    def _():
+        minus_out_ref[...] = minus_ref[...]
+        plus_out_ref[...] = (plus_ref[...].astype(F32) + from_below_ref[...].astype(F32)).astype(BF16)
+
+    @pl.when(part == 1)
+    def _():
+        minus_out_ref[...] = (minus_ref[...].astype(F32) + from_above_ref[...].astype(F32)).astype(BF16)
+        plus_out_ref[...] = plus_ref[...]
 
 
 def rms(values, gain):
     return values * lax.rsqrt(jnp.mean(values * values, axis=-1, keepdims=True) + EPS) * gain
 
 
-def norms_kernel(tiles_ref, residual_ref, mix_ref, pre_ref, updated_ref, normed_ref):
-    projected = tiles_ref[0].astype(F32)
-    for k in range(1, tiles_ref.shape[0]):
-        projected = projected + tiles_ref[k].astype(F32)
+def norms_kernel(own_ref, below_ref, above_ref, residual_ref, mix_ref, pre_ref, updated_ref, normed_ref):
+    projected = own_ref[...].astype(F32) + below_ref[...].astype(F32) + above_ref[...].astype(F32)
     updated = (residual_ref[...].astype(F32) + rms(projected, mix_ref[...])).astype(BF16)
     updated_ref[...] = updated
-    normed = rms(updated.astype(F32), pre_ref[...]).astype(BF16)
-    for k in range(normed_ref.shape[0]):
-        normed_ref[k] = normed
-
-
-def mixer_kernel(x_ref, up_ref, down_ref, out_ref, hidden_ref, *, steps, block):
+    normed_ref[...] = rms(updated.astype(F32), pre_ref[...]).astype(BF16)
+
+
+def result_kernel(own_ref, below_ref, above_ref, updated_ref, gain_ref, out_ref):
+    lowered = own_ref[...].astype(F32) + below_ref[...].astype(F32) + above_ref[...].astype(F32)
+    out_ref[...] = (updated_ref[...].astype(F32) + rms(lowered.T, gain_ref[...])).astype(BF16)
+
+
+def far_mixer_kernel(
+    own_ref, far_low_ref, far_high_ref, below_ref, above_ref, up_ref, down_ref,
+    hidden_ref, out_ref, low_ref, high_ref, x_ref, now_ref, *, steps, block,
+):
     step = pl.program_id(0)
+    rows = own_ref.shape[0]
+    half = rows // 2
+
+    @pl.when(step == 0)
+    def _():
+        x_ref[0:rows] = own_ref[...]
+        x_ref[rows : rows + half] = far_low_ref[...]
+        x_ref[rows + half : 2 * rows] = far_high_ref[...]
+        x_ref[2 * rows : 3 * rows] = below_ref[...]
+        x_ref[3 * rows :] = above_ref[...]
 
     @pl.when(step < steps)
     def _():
-        weight = up_ref[...].reshape(x_ref.shape[1], block)
-        rectified = jnp.maximum(mm(x_ref[...], weight), 0.0)
-        at = pl.multiple_of(step * block, block)
-        hidden_ref[:, pl.ds(at, block)] = (rectified * rectified).astype(BF16)
+        rectified = jnp.maximum(mm(x_ref[...], up_ref[...].reshape(x_ref.shape[1], block)), 0.0)
+        hidden = (rectified * rectified).astype(BF16).T
+        hidden_ref[...] = hidden[:, 2 * rows :]
+        now_ref[pl.ds(pl.multiple_of(step * block, block), block), :] = hidden[:, : 2 * rows]
 
     @pl.when(step >= steps)
     def _():
-        weight = down_ref[...].reshape(block, hidden_ref.shape[1])
-        out_ref[...] = mm_nt(hidden_ref[...], weight).astype(BF16)
+        lowered = mm(down_ref[...].reshape(block, now_ref.shape[0]), now_ref[...]).astype(BF16)
+        out_ref[...] = lowered[:, :rows]
+
+        @pl.when(step < steps + steps // 2)
+        def _():
+            low_ref[...] = lowered[:, rows:]
+
+        @pl.when(step >= steps + steps // 2)
+        def _():
+            high_ref[...] = lowered[:, rows:]
+
+
+def near_mixer_kernel(hidden_ref, down_ref, minus_ref, plus_ref):
+    lowered = mm(down_ref[...].reshape(-1, hidden_ref.shape[0]), hidden_ref[...]).astype(BF16)
+    rows = minus_ref.shape[1]
+    minus_ref[...] = lowered[:, :rows]
+    plus_ref[...] = lowered[:, rows:]
+
+
+SMALL = pltpu.CompilerParams(vmem_limit_bytes=16 * 1024 * 1024)
+LARGE = pltpu.CompilerParams(vmem_limit_bytes=50 * 1024 * 1024)
+
+
+def shifted(array, axis, by):
+    size = lax.axis_size(axis)
+    return lax.ppermute(array, axis, [(k, (k + by) % size) for k in range(size)])
+
+
+def joined(minus, plus, from_below, from_above, picks=(None, None)):
+    half, width = from_below.shape
+    flat = pl.BlockSpec((half, width), lambda i: (i, 0))
+    kept = pl.BlockSpec((half, width), lambda i: (0, 0))
+    out = jax.ShapeDtypeStruct((2 * half, width), BF16)
+
+    def source(pick):
+        if pick is None:
+            return flat
+        return pl.BlockSpec((None, half, width), lambda i: (pick, i, 0))
+
+    return pl.pallas_call(
+        join_kernel,
+        out_shape=(out, out),
+        grid=(2,),
+        in_specs=[source(picks[0]), source(picks[1]), kept, kept],
+        out_specs=[flat, flat],
+        compiler_params=SMALL,
+        name="join",
+        cost_estimate=pl.CostEstimate(flops=1_000_000, bytes_accessed=3_500_000, transcendentals=0),
+    )(minus, plus, from_below, from_above)
 
 
 def local(
@@ -278,32 +355,42 @@
     ).reshape(devices, 2, share, units)
 
     inside, starts = (jnp.asarray(t) for t in position_tables(devices))
-    index = lax.axis_index(SP).astype(jnp.int32).reshape(1)
-    wide_block = pl.BlockSpec((SPAN, 384), lambda s, i: (s, 0))
-    narrow_block = pl.BlockSpec((SPAN, 128), lambda s, i: (s, 0))
-    decay_blocks = [
-        pl.BlockSpec((3, SPAN), lambda s, i: (0, s)),
-        pl.BlockSpec((2, SPAN), lambda s, i: (0, s)),
-    ]
+    turn = lax.axis_index("tp")
+    order = jnp.stack(
+        [lax.axis_index(SP), (turn + 2) % ranks, turn, (turn + ranks - 1) % ranks, (turn + 1) % ranks]
+    ).astype(jnp.int32)
     table_blocks = [
         pl.BlockSpec((4, SPAN, LANES), lambda s, i: (0, 0, 0)),
         pl.BlockSpec((1, 4 * SPANS, LANES), lambda s, i: (i[0], 0, 0)),
     ]
-    before_block = pl.BlockSpec((1, 512, LANES), lambda s, i: (s, 0, 0))
-    before, message = pl.pallas_call(
+
+    def span_blocks(at):
+        return (
+            pl.BlockSpec((SPAN, 384), lambda s, i: (at(s, i), 0)),
+            pl.BlockSpec((SPAN, 128), lambda s, i: (at(s, i), 0)),
+            [
+                pl.BlockSpec((3, SPAN), lambda s, i: (0, at(s, i))),
+                pl.BlockSpec((2, SPAN), lambda s, i: (0, at(s, i))),
+            ],
+            [
+                pl.BlockSpec((1, 512, LANES), lambda s, i: (at(s, i), 0, 0)),
+                pl.BlockSpec((1, 8, LANES), lambda s, i: (at(s, i), 0, 0)),
+            ],
+        )
+
+    wide_block, narrow_block, decay_blocks, state_blocks = span_blocks(lambda s, i: s)
+    before, earlier, message = pl.pallas_call(
         states_kernel,
         out_shape=(
             jax.ShapeDtypeStruct((SPANS, 512, LANES), F32),
+            jax.ShapeDtypeStruct((SPANS, 8, LANES), F32),
             jax.ShapeDtypeStruct((devices, 16, LANES), BF16),
         ),
         grid_spec=pltpu.PrefetchScalarGridSpec(
             num_scalar_prefetch=1,
             grid=(SPANS,),
             in_specs=[wide_block, wide_block, narrow_block, narrow_block, *decay_blocks, *table_blocks],
-            out_specs=[
-                before_block,
-                pl.BlockSpec((devices, 16, LANES), lambda s, i: (0, 0, 0)),
-            ],
+            out_specs=[*state_blocks, pl.BlockSpec((devices, 16, LANES), lambda s, i: (0, 0, 0))],
             scratch_shapes=[
                 pltpu.VMEM((8, LANES), F32),
                 pltpu.VMEM((512, LANES), F32),
@@ -312,82 +399,137 @@
         ),
         name="states",
         cost_estimate=pl.CostEstimate(flops=60_000_000, bytes_accessed=2_500_000, transcendentals=20_000),
-    )(index, wide_key, wide_value, narrow_key, narrow_value, wide_decay, narrow_decay, inside, starts)
+    )(order, wide_key, wide_value, narrow_key, narrow_value, wide_decay, narrow_decay, inside, starts)
 
     arrived = lax.all_to_all(message, SP, 0, 0, tiled=True)
     prefixes = pl.pallas_call(
         prefix_kernel,
         out_shape=jax.ShapeDtypeStruct((devices, 8, LANES), BF16),
+        compiler_params=SMALL,
         name="prefix",
         cost_estimate=pl.CostEstimate(flops=2_000_000, bytes_accessed=400_000, transcendentals=8_000),
     )(arrived)
     prefix = lax.all_to_all(prefixes, SP, 0, 0, tiled=True).reshape(512, LANES)
 
-    partial = pl.pallas_call(
-        finish_kernel,
-        out_shape=jax.ShapeDtypeStruct((SPANS, SPAN, width), BF16),
-        grid_spec=pltpu.PrefetchScalarGridSpec(
-            num_scalar_prefetch=1,
-            grid=(SPANS,),
-            in_specs=[
-                wide_block, wide_block, wide_block, wide_block,
-                narrow_block, narrow_block, narrow_block, narrow_block,
-                *decay_blocks, *table_blocks, before_block,
-                pl.BlockSpec((512, LANES), lambda s, i: (0, 0)),
-                pl.BlockSpec((384, width), lambda s, i: (0, 0)),
-                pl.BlockSpec((128, width), lambda s, i: (0, 0)),
-            ],
-            out_specs=pl.BlockSpec((1, SPAN, width), lambda s, i: (s, 0, 0)),
-            scratch_shapes=[
-                pltpu.VMEM((8, LANES), F32),
-                pltpu.VMEM((8, LANES), F32),
-                pltpu.VMEM((SPAN, 512), BF16),
-            ],
-        ),
-        name="finish",
-        cost_estimate=pl.CostEstimate(flops=1_400_000_000, bytes_accessed=9_000_000, transcendentals=600_000),
-    )(
-        index, wide_query, wide_key, wide_value, wide_gate,
-        narrow_query, narrow_key, narrow_value, narrow_gate,
-        wide_decay, narrow_decay, inside, starts, before, prefix, wide_out, narrow_out,
-    )
-
-    tiles = lax.all_to_all(partial.reshape(ranks, rows, width), "tp", 0, 0, tiled=True)
+    def finish(first, count, out_shape, out_specs):
+        wide, narrow, decays, states = span_blocks(lambda s, i: i[1 + first + s])
+        return pl.pallas_call(
+            functools.partial(finish_kernel, first=first),
+            out_shape=out_shape,
+            grid_spec=pltpu.PrefetchScalarGridSpec(
+                num_scalar_prefetch=1,
+                grid=(count,),
+                in_specs=[
+                    wide, wide, wide, wide, narrow, narrow, narrow, narrow,
+                    *decays, *table_blocks, *states,
+                    pl.BlockSpec((512, LANES), lambda s, i: (0, 0)),
+                    pl.BlockSpec((384, width), lambda s, i: (0, 0)),
+                    pl.BlockSpec((128, width), lambda s, i: (0, 0)),
+                ],
+                out_specs=out_specs,
+                scratch_shapes=[pltpu.VMEM((8, LANES), F32), pltpu.VMEM((SPAN, 512), BF16)],
+            ),
+            compiler_params=SMALL,
+            name="finish" if first else "finish_far",
+            cost_estimate=pl.CostEstimate(
+                flops=350_000_000 * count,
+                bytes_accessed=3_000_000 + 1_500_000 * count,
+                transcendentals=150_000 * count,
+            ),
+        )(
+            order, wide_query, wide_key, wide_value, wide_gate,
+            narrow_query, narrow_key, narrow_value, narrow_gate,
+            wide_decay, narrow_decay, inside, starts, before, earlier, prefix, wide_out, narrow_out,
+        )
+
+    half = rows // 2
+    half_out = jax.ShapeDtypeStruct((half, width), BF16)
+    near_out = jax.ShapeDtypeStruct((3, rows, width), BF16)
+    low, high = finish(
+        0, 1, (half_out, half_out), [pl.BlockSpec((half, width), lambda s, i: (0, 0))] * 2
+    )
+    low, high = shifted(low, "tp", 1), shifted(high, "tp", -1)
+    (near,) = finish(
+        1, 3, (near_out,), [pl.BlockSpec((1, rows, width), lambda s, i: (s, 0, 0))]
+    )
+    minus, plus = joined(near, near, low, high, (1, 2))
+    below, above = shifted(plus, "tp", 1), shifted(minus, "tp", -1)
+    lines = 32
+    flat = pl.BlockSpec((lines, width), lambda i: (i, 0))
+    gain = pl.BlockSpec((1, width), lambda i: (0, 0))
     updated, normed = pl.pallas_call(
         norms_kernel,
+        out_shape=[jax.ShapeDtypeStruct((rows, width), BF16)] * 2,
+        grid=(rows // lines,),
+        in_specs=[
+            pl.BlockSpec((None, lines, width), lambda i: (0, i, 0)), flat, flat, flat, gain, gain,
+        ],
+        out_specs=[flat, flat],
+        compiler_params=SMALL,
+        name="norms",
+        cost_estimate=pl.CostEstimate(flops=4_000_000, bytes_accessed=3_500_000, transcendentals=300),
+    )(near, below, above, residual, gain_mix.reshape(1, width), gain_pre.reshape(1, width))
+    below, above = shifted(normed, "tp", 1), shifted(normed, "tp", -1)
+    low, high = shifted(below[:half], "tp", 1), shifted(above[half:], "tp", -1)
+
+    block = min(1024, units // 2)
+    steps, halves = units // block, units // block // 2
+    resident = pl.BlockSpec((rows, width), lambda i: (0, 0))
+    resident_half = pl.BlockSpec((half, width), lambda i: (0, 0))
+    turned = jax.ShapeDtypeStruct((width, rows), BF16)
+    turned_half = jax.ShapeDtypeStruct((width // 2, rows), BF16)
+    hidden, own, low, high = pl.pallas_call(
+        functools.partial(far_mixer_kernel, steps=steps, block=block),
         out_shape=(
-            jax.ShapeDtypeStruct((rows, width), BF16),
-            jax.ShapeDtypeStruct((ranks, rows, width), BF16),
+            jax.ShapeDtypeStruct((units, 2 * rows), BF16), turned, turned_half, turned_half,
         ),
-        name="norms",
-        cost_estimate=pl.CostEstimate(flops=4_000_000, bytes_accessed=6_000_000, transcendentals=300),
-    )(tiles, residual, gain_mix.reshape(1, width), gain_pre.reshape(1, width))
-    block_rows = lax.all_to_all(normed, "tp", 0, 0, tiled=True).reshape(length, width)
-
-    block = 256
-    steps = units // block
-    lowered = pl.pallas_call(
-        functools.partial(mixer_kernel, steps=steps, block=block),
-        out_shape=jax.ShapeDtypeStruct((length, width), BF16),
         grid=(2 * steps,),
         in_specs=[
-            pl.BlockSpec((length, width), lambda i: (0, 0)),
+            resident, resident_half, resident_half, resident, resident,
             pl.BlockSpec((devices, 1, share, block), lambda i: (0, 0, 0, jnp.minimum(i, steps - 1))),
             pl.BlockSpec(
                 (block // share, 1, share, units), lambda i: (jnp.maximum(i - steps, 0), 1, 0, 0)
             ),
         ],
-        out_specs=pl.BlockSpec((length, block), lambda i: (0, jnp.maximum(i - steps, 0))),
-        scratch_shapes=[pltpu.VMEM((length, units), BF16)],
-        compiler_params=pltpu.CompilerParams(vmem_limit_bytes=32 * 1024 * 1024),
-        name="mixer",
+        out_specs=[
+            pl.BlockSpec((block, 2 * rows), lambda i: (jnp.minimum(i, steps - 1), 0)),
+            pl.BlockSpec((block, rows), lambda i: (jnp.maximum(i - steps, 0), 0)),
+            pl.BlockSpec((block, rows), lambda i: (jnp.clip(i - steps, 0, halves - 1), 0)),
+            pl.BlockSpec((block, rows), lambda i: (jnp.clip(i - steps - halves, 0, halves - 1), 0)),
+        ],
+        scratch_shapes=[pltpu.VMEM((4 * rows, width), BF16), pltpu.VMEM((units, 2 * rows), BF16)],
+        compiler_params=LARGE,
+        name="mixer_far",
         cost_estimate=pl.CostEstimate(
-            flops=4 * length * width * units, bytes_accessed=22_000_000, transcendentals=0
+            flops=12 * rows * width * units, bytes_accessed=20_000_000, transcendentals=0
         ),
-    )(block_rows, both, both)
-    lowered = lax.all_to_all(lowered.reshape(ranks, rows, width), "tp", 0, 0, tiled=True)
-    lowered = jnp.sum(lowered.astype(F32), axis=0)
-    return (updated.astype(F32) + rms(lowered, gain_mlp)).astype(BF16)
+    )(normed, low, high, below, above, both, both)
+    low, high = shifted(low, "tp", 1), shifted(high, "tp", -1)
+    lasts = pl.BlockSpec((block, rows), lambda i: (i, 0))
+    minus, plus = pl.pallas_call(
+        near_mixer_kernel,
+        out_shape=(turned, turned),
+        grid=(width // block,),
+        in_specs=[
+            pl.BlockSpec((units, 2 * rows), lambda i: (0, 0)),
+            pl.BlockSpec((block // share, 1, share, units), lambda i: (i, 1, 0, 0)),
+        ],
+        out_specs=[lasts, lasts],
+        compiler_params=LARGE,
+        name="mixer_near",
+        cost_estimate=pl.CostEstimate(
+            flops=4 * rows * width * units, bytes_accessed=12_000_000, transcendentals=0
+        ),
+    )(hidden, both)
+    minus, plus = joined(minus, plus, low, high)
+    below, above = shifted(plus, "tp", 1), shifted(minus, "tp", -1)
+    return pl.pallas_call(
+        result_kernel,
+        out_shape=jax.ShapeDtypeStruct((rows, width), BF16),
+        compiler_params=SMALL,
+        name="result",
+        cost_estimate=pl.CostEstimate(flops=4_000_000, bytes_accessed=3_500_000, transcendentals=300),
+    )(own, below, above, updated, gain_mlp.reshape(1, width))
 
 
 def solution(mesh):

time: 192 us -> 164 us (0.85)
  blocking collectives: 131 us -> 42.5 us
  waiting for transfers between devices: 0.02 us -> 36.1 us
  starting transfers between devices: 0.01 us -> 20.2 us
  local copies, waits for them, and re-layouts: 6.26 us -> 11.7 us
    all_to_all x3 -> x0, blocking collectives: 88.6 us -> none  [the longest x1 31.3 us: local(): lax.all_to_all(partial.reshape(ranks, rows, width), 'tp', 0, 0, tiled=True)]
    ppermute x0 -> x12, waiting for transfers between devices: none -> 36.1 us  [shifted(): lax.ppermute(array, axis, [(k, (k + by) % size) for k in range(size)])]
    ppermute x0 -> x12, starting transfers between devices: none -> 20.2 us  [shifted(): lax.ppermute(array, axis, [(k, (k + by) % size) for k in range(size)])]
    unnamed x6 -> x48, local copies, waits for them, and re-layouts: 6.26 us -> 11 us
    pallas_call x3 -> x8, Pallas kernels: 28.5 us -> 29 us  [the longest x1 12.8 us: local(): pl.pallas_call(functools.partial(far_mixer_kernel, steps=steps, block=blo...]
  transfers between devices with their start and end apart: 1 -> 13, of which waited for: 0 -> 7; matrix products, arithmetic and copies ran while one was open for 0% -> 0% of each run, Pallas kernels for 12% -> 13%
where the time goes in v2:
time: 164 us; the launch traced here: 162 us
  blocking collectives  42.5 us (26%)
  Pallas kernels  36.2 us (22%)
  waiting for transfers between devices  36.1 us (22%)
  starting transfers between devices  20.2 us (12%)
  between operations  13.6 us (8%)
  local copies, waits for them, and re-layouts  11.7 us (7%)
  other arithmetic  1.77 us (1%)
    ppermute x12, waiting for transfers between devices, shifted(): lax.ppermute(array, axis, [(k, (k + by) % size) for k in range(size)])  36.1 us
    all_to_all x1, blocking collectives, local(): arrived = lax.all_to_all(message, SP, 0, 0, tiled=True)  25.4 us
    ppermute x12, starting transfers between devices, shifted(): lax.ppermute(array, axis, [(k, (k + by) % size) for k in range(size)])  20.2 us
    all_to_all x1, blocking collectives, local(): prefix = lax.all_to_all(prefixes, SP, 0, 0, tiled=True).reshape(512, LANES)  17.1 us
    pallas_call x1, Pallas kernels, local(): pl.pallas_call(functools.partial(far_mixer_kernel, steps=steps, block=blo...  12.8 us
    unnamed x48, local copies, waits for them, and re-layouts  11 us
    pallas_call x2, Pallas kernels, finish(): pl.pallas_call(functools.partial(finish_kernel, first=first), out_shape=o...  8.47 us
    pallas_call x1, Pallas kernels, local(): pl.pallas_call(states_kernel, out_shape=(jax.ShapeDtypeStruct((SPANS, 512...  7.08 us
  transfers between devices with their start and end apart: 13, of which 7 were waited for; matrix products, arithmetic and copies ran while one was open for 0% of the time, Pallas kernels for 13%

profile of v2, /device:TPU:32, one launch (start us, length us, event | category | flops | bytes accessed | tf_op | source)
XLA Modules:
  0.0 162.2 jit_solution(8531013655139151848)
XLA Ops:
  6.5 1.8 %pad_maximum_fusion = bf16[64,2048]{1,0:T(8,128)(2,1)} fusion(bf16[32,2048]{1,0:T(8,128)(2,1)} %bitcast.19, bf16[32,2048]{1,0:T(8,128)(2,1)} %param.33), kind=kLoop, calls=%fused_computation | loop fusion | flops 524288 | bytes 524288 | tf_op jit(solution)/shard_map/concatenate | solution.py:354
  9.1 7.1 %states.1 = (f32[4,512,128]{2,1,0:T(8,128)}, f32[4,8,128]{2,1,0:T(8,128)}, bf16[64,16,128]{2,1,0:T(8,128)(2,1)}) custom-call(s32[5]{0:T(128)} %stack.23._.order_ref, bf16[512,384]{1,0:T(8,128)(2,1)} %wk_ref.5, bf16[512,384]{1,0:T(8,128)(2,1)} %wv_ref.5, bf16[512,128]{1,0:T(8,128)(2,1)} %nk_ref.5, bf16[512,128]{1,0:T(8,128)(2,1)} %nv_ref.5, f32[3,512]{1,0:T(4,128)} %wd_ref.5, ...), custom_call_target="tpu_custom_call" | custom-call | flops 60000000 | bytes 2500000 | tf_op jit(solution)/shard_map/states/pallas_call | solution.py:382
  16.2 25.4 %all_to_all.10.message_ref = bf16[64,16,128]{2,1,0:T(8,128)(2,1)S(1)} all-to-all(bf16[64,16,128]{2,1,0:T(8,128)(2,1)} %get-tuple-element.24), channel_id=1, replica_groups=mesh['sp_0'=8,'sp_1'=4,'sp_2'=2,'tp'=4] {'sp_0','sp_1','sp_2'}, dimensions={0} | all-to-all | bytes 524288 | tf_op jit(solution)/shard_map/all_to_all | solution.py:404
  41.7 17.1 %all_to_all.11 = bf16[64,8,128]{2,1,0:T(8,128)(2,1)S(1)} all-to-all(bf16[64,8,128]{2,1,0:T(8,128)(2,1)S(1)} %prefix.1), channel_id=1, replica_groups=mesh['sp_0'=8,'sp_1'=4,'sp_2'=2,'tp'=4] {'sp_0','sp_1','sp_2'}, dimensions={0} | all-to-all | bytes 262144 | tf_op jit(solution)/shard_map/all_to_all | solution.py:412
  68.6 2.4 %finish_far.1 = (bf16[64,2048]{1,0:T(8,128)(2,1)S(1)}, bf16[64,2048]{1,0:T(8,128)(2,1)S(1)}) custom-call(s32[5]{0:T(128)S(1)} %copy-done.23, bf16[512,384]{1,0:T(8,128)(2,1)S(1)} %copy-done.7, bf16[512,384]{1,0:T(8,128)(2,1)S(1)} %copy-done.3, bf16[512,384]{1,0:T(8,128)(2,1)S(1)} %copy-done.4, bf16[512,384]{1,0:T(8,128)(2,1)S(1)} %copy-done.8, ...), custom_call_target="tpu_custom_call" | custom-call | flops 350000000 | bytes 4500000 | tf_op jit(solution)/shard_map/finish_far/pallas_call | solution.py:416
  71.0 1.7 %collective-permute-start = (bf16[64,2048]{1,0:T(8,128)(2,1)S(1)}, bf16[64,2048]{1,0:T(8,128)(2,1)S(1)}, u32[]{:S(2)}, u32[]{:S(2)}) collective-permute-start(bf16[64,2048]{1,0:T(8,128)(2,1)S(1)} %get-tuple-element.25), channel_id=1, source_target_pairs={{0,1},{1,2},{2,3},{3,0},{4,5},{5,6},{6,7},{7,4},{8,9},{9,10},{10,1... | collective-permute-start | bytes 786440 | tf_op jit(solution)/shard_map/ppermute | solution.py:314
  72.6 1.7 %collective-permute-start.1 = (bf16[64,2048]{1,0:T(8,128)(2,1)S(1)}, bf16[64,2048]{1,0:T(8,128)(2,1)S(1)}, u32[]{:S(2)}, u32[]{:S(2)}) collective-permute-start(bf16[64,2048]{1,0:T(8,128)(2,1)S(1)} %get-tuple-element.26), channel_id=1, source_target_pairs={{0,3},{1,0},{2,1},{3,2},{4,7},{5,4},{6,5},{7,6},{8,11},{9,8},{10,9... | collective-permute-start | bytes 786440 | tf_op jit(solution)/shard_map/ppermute | solution.py:314
  74.3 6.1 %finish.1.minus_ref.plus_ref.own_ref = bf16[3,128,2048]{2,1,0:T(8,128)(2,1)S(1)} custom-call(s32[5]{0:T(128)S(1)} %copy-done.23, bf16[512,384]{1,0:T(8,128)(2,1)S(1)} %copy-done.7, bf16[512,384]{1,0:T(8,128)(2,1)S(1)} %copy-done.3, bf16[512,384]{1,0:T(8,128)(2,1)S(1)} %copy-done.4, bf16[512,384]{1,0:T(8,128)(2,1)S(1)} %copy-done.8, ...), custom_call_target="tpu_custom_call" | custom-call | flops 1050000000 | bytes 7500000 | tf_op jit(solution)/shard_map/finish/pallas_call | solution.py:416
  80.9 1.6 collective-permute-start.2
  82.5 1.7 %collective-permute-start.3 = (bf16[128,2048]{1,0:T(8,128)(2,1)S(1)}, bf16[128,2048]{1,0:T(8,128)(2,1)S(1)}, u32[]{:S(2)}, u32[]{:S(2)}) collective-permute-start(bf16[128,2048]{1,0:T(8,128)(2,1)S(1)} %get-tuple-element.28), channel_id=1, source_target_pairs={{0,3},{1,0},{2,1},{3,2},{4,7},{5,4},{6,5},{7,6},{8,11},{9,8},{10,9... | collective-permute-start | bytes 1572872 | tf_op jit(solution)/shard_map/ppermute | solution.py:314
  84.2 11.2 %collective-permute-done.2.below_ref = bf16[128,2048]{1,0:T(8,128)(2,1)S(1)} collective-permute-done((bf16[128,2048]{1,0:T(8,128)(2,1)S(1)}, bf16[128,2048]{1,0:T(8,128)(2,1)S(1)}, u32[]{:S(2)}, u32[]{:S(2)}) %collective-permute-start.2) | collective-permute-done | bytes 524320 | tf_op jit(solution)/shard_map/ppermute | solution.py:314
  95.4 1.2 norms.1
  96.6 3.0 %collective-permute-start.6 = (bf16[128,2048]{1,0:T(8,128)(2,1)S(1)}, bf16[128,2048]{1,0:T(8,128)(2,1)S(1)}, u32[]{:S(2)}, u32[]{:S(2)}) collective-permute-start(bf16[128,2048]{1,0:T(8,128)(2,1)S(1)} %get-tuple-element.29.own_ref), channel_id=1, source_target_pairs={{0,3},{1,0},{2,1},{3,2},{4,7},{5,4},{6,5},{7,6},{8,11},{9,8},{10,9... | collective-permute-start | bytes 1572872 | tf_op jit(solution)/shard_map/ppermute | solution.py:314
  99.7 9.7 %collective-permute-done.6.above_ref = bf16[128,2048]{1,0:T(8,128)(2,1)S(1)} collective-permute-done((bf16[128,2048]{1,0:T(8,128)(2,1)S(1)}, bf16[128,2048]{1,0:T(8,128)(2,1)S(1)}, u32[]{:S(2)}, u32[]{:S(2)}) %collective-permute-start.6) | collective-permute-done | bytes 524320 | tf_op jit(solution)/shard_map/ppermute | solution.py:314
  109.4 3.8 %collective-permute-start.7 = (bf16[64,2048]{1,0:T(8,128)(2,1)S(1)}, bf16[64,2048]{1,0:T(8,128)(2,1)S(1)}, u32[]{:S(2)}, u32[]{:S(2)}) collective-permute-start(bf16[64,2048]{1,0:T(8,128)(2,1)S(1)} %slice.9), channel_id=1, source_target_pairs={{0,3},{1,0},{2,1},{3,2},{4,7},{5,4},{6,5},{7,6},{8,11},{9,8},{10,9... | collective-permute-start | bytes 786440 | tf_op jit(solution)/shard_map/ppermute | solution.py:314
  113.5 3.6 %collective-permute-done.7.far_high_ref = bf16[64,2048]{1,0:T(8,128)(2,1)S(1)} collective-permute-done((bf16[64,2048]{1,0:T(8,128)(2,1)S(1)}, bf16[64,2048]{1,0:T(8,128)(2,1)S(1)}, u32[]{:S(2)}, u32[]{:S(2)}) %collective-permute-start.7) | collective-permute-done | bytes 262176 | tf_op jit(solution)/shard_map/ppermute | solution.py:314
  117.1 4.0 %collective-permute-done.5.far_low_ref = bf16[64,2048]{1,0:T(8,128)(2,1)S(1)} collective-permute-done((bf16[64,2048]{1,0:T(8,128)(2,1)S(1)}, bf16[64,2048]{1,0:T(8,128)(2,1)S(1)}, u32[]{:S(2)}, u32[]{:S(2)}) %collective-permute-start.5) | collective-permute-done | bytes 262176 | tf_op jit(solution)/shard_map/ppermute | solution.py:314
  121.0 12.8 %mixer_far.1 = (bf16[2048,256]{1,0:T(8,128)(2,1)}, bf16[2048,128]{1,0:T(8,128)(2,1)S(1)}, bf16[1024,128]{1,0:T(8,128)(2,1)S(1)}, bf16[1024,128]{1,0:T(8,128)(2,1)S(1)}) custom-call(bf16[128,2048]{1,0:T(8,128)(2,1)S(1)} %get-tuple-element.29.own_ref, bf16[64,2048]{1,0:T(8,128)(2,1)S(1)} %collective-permute-done.5.far_low_ref, ...), custom_call_target="tpu_custom_call" | custom-call | flops 6442450944 | bytes 20000000 | tf_op jit(solution)/shard_map/mixer_far/pallas_call | solution.py:481
  133.9 3.2 %collective-permute-start.9 = (bf16[1024,128]{1,0:T(8,128)(2,1)S(1)}, bf16[1024,128]{1,0:T(8,128)(2,1)S(1)}, u32[]{:S(2)}, u32[]{:S(2)}) collective-permute-start(bf16[1024,128]{1,0:T(8,128)(2,1)S(1)} %get-tuple-element.35), channel_id=1, source_target_pairs={{0,3},{1,0},{2,1},{3,2},{4,7},{5,4},{6,5},{7,6},{8,11},{9,8},{10,9... | collective-permute-start | bytes 786440 | tf_op jit(solution)/shard_map/ppermute | solution.py:314
  137.1 1.2 copy-done.11
  138.3 4.7 %mixer_near.1 = (bf16[2048,128]{1,0:T(8,128)(2,1)S(1)}, bf16[2048,128]{1,0:T(8,128)(2,1)S(1)}) custom-call(bf16[2048,256]{1,0:T(8,128)(2,1)S(1)} %copy-done.11, bf16[64,2,32,2048]{3,2,1,0:T(8,128)(2,1)} %bitcast.18), custom_call_target="tpu_custom_call" | custom-call | flops 2147483648 | bytes 12000000 | tf_op jit(solution)/shard_map/mixer_near/pallas_call | solution.py:509
  143.4 3.2 %collective-permute-start.11 = (bf16[2048,128]{1,0:T(8,128)(2,1)S(1)}, bf16[2048,128]{1,0:T(8,128)(2,1)S(1)}, u32[]{:S(2)}, u32[]{:S(2)}) collective-permute-start(bf16[2048,128]{1,0:T(8,128)(2,1)S(1)} %get-tuple-element.37), channel_id=1, source_target_pairs={{0,3},{1,0},{2,1},{3,2},{4,7},{5,4},{6,5},{7,6},{8,11},{9,8},{10,9... | collective-permute-start | bytes 1572872 | tf_op jit(solution)/shard_map/ppermute | solution.py:314
  146.6 7.3 %collective-permute-done.10.below_ref = bf16[2048,128]{1,0:T(8,128)(2,1)S(1)} collective-permute-done((bf16[2048,128]{1,0:T(8,128)(2,1)S(1)}, bf16[2048,128]{1,0:T(8,128)(2,1)S(1)}, u32[]{:S(2)}, u32[]{:S(2)}) %collective-permute-start.10) | collective-permute-done | bytes 524320 | tf_op jit(solution)/shard_map/ppermute | solution.py:314
  154.0 1.4 result.1
  (67 shorter events, 11.7 us)
Async XLA Ops:
  6.5 114.5 %all-gather.2.cloned.1.call-start = ((), (), s32[]{:S(2)}) async-start(), calls=%async_computation.2 | async-start | bytes 17039360 | tf_op jit(solution)/shard_map/all_gather | solution.py:353
  6.5 52.3 %copy-start.15 = (f32[3,512]{1,0:T(4,128)S(1)}, f32[3,512]{1,0:T(4,128)}, u32[]{:S(2)}) copy-start(f32[3,512]{1,0:T(4,128)} %wd_ref.5) | copy-start | bytes 18436
  6.5 52.3 %copy-start.3 = (bf16[512,384]{1,0:T(8,128)(2,1)S(1)}, bf16[512,384]{1,0:T(8,128)(2,1)}, u32[]{:S(2)}) copy-start(bf16[512,384]{1,0:T(8,128)(2,1)} %wk_ref.5) | copy-start | bytes 1179652
  6.5 52.3 %copy-start.4 = (bf16[512,384]{1,0:T(8,128)(2,1)S(1)}, bf16[512,384]{1,0:T(8,128)(2,1)}, u32[]{:S(2)}) copy-start(bf16[512,384]{1,0:T(8,128)(2,1)} %wv_ref.5) | copy-start | bytes 1179652
  8.3 50.5 %copy-start = (bf16[384,2048]{1,0:T(8,128)(2,1)S(1)}, bf16[384,2048]{1,0:T(8,128)(2,1)}, u32[]{:S(2)}) copy-start(bf16[384,2048]{1,0:T(8,128)(2,1)} %wide_out_ref.3) | copy-start | bytes 4718596
  8.4 50.5 %copy-start.1 = (f32[64,16,128]{2,1,0:T(8,128)S(1)}, f32[64,16,128]{2,1,0:T(8,128)}, u32[]{:S(2)}) copy-start(f32[64,16,128]{2,1,0:T(8,128)} %constant.51.clone.start_ref) | copy-start | bytes 1572868
  16.2 42.7 %copy-start.2 = (f32[4,512,128]{2,1,0:T(8,128)S(1)}, f32[4,512,128]{2,1,0:T(8,128)}, u32[]{:S(2)}) copy-start(f32[4,512,128]{2,1,0:T(8,128)} %get-tuple-element.22.before_ref) | copy-start | bytes 3145732
  68.6 5.7 %copy-start.19 = (f32[2,512]{1,0:T(2,128)S(1)}, f32[2,512]{1,0:T(2,128)}, u32[]{:S(2)}) copy-start(f32[2,512]{1,0:T(2,128)} %nd_ref.5) | copy-start | bytes 12292
  71.0 9.6 %collective-permute-start = (bf16[64,2048]{1,0:T(8,128)(2,1)S(1)}, bf16[64,2048]{1,0:T(8,128)(2,1)S(1)}, u32[]{:S(2)}, u32[]{:S(2)}) collective-permute-start(bf16[64,2048]{1,0:T(8,128)(2,1)S(1)} %get-tuple-element.25), channel_id=1, source_target_pairs={{0,1},{1,2},{2,3},{3,0},{4,5},{5,6},{6,7},{7,4},{8,9},{9,10},{10,1... | collective-permute-start | bytes 786440 | tf_op jit(solution)/shard_map/ppermute | solution.py:314
  72.6 8.0 %collective-permute-start.1 = (bf16[64,2048]{1,0:T(8,128)(2,1)S(1)}, bf16[64,2048]{1,0:T(8,128)(2,1)S(1)}, u32[]{:S(2)}, u32[]{:S(2)}) collective-permute-start(bf16[64,2048]{1,0:T(8,128)(2,1)S(1)} %get-tuple-element.26), channel_id=1, source_target_pairs={{0,3},{1,0},{2,1},{3,2},{4,7},{5,4},{6,5},{7,6},{8,11},{9,8},{10,9... | collective-permute-start | bytes 786440 | tf_op jit(solution)/shard_map/ppermute | solution.py:314
  80.4 15.0 %copy-start.14 = (bf16[128,2048]{1,0:T(8,128)(2,1)S(1)}, bf16[128,2048]{1,0:T(8,128)(2,1)}, u32[]{:S(2)}) copy-start(bf16[128,2048]{1,0:T(8,128)(2,1)} %residual_ref.1) | copy-start | bytes 1572868
  80.4 15.0 %copy-start.20 = (f32[2048]{0:T(1024)S(1)}, f32[2048]{0:T(1024)}, u32[]{:S(2)}) copy-start(f32[2048]{0:T(1024)} %param.35) | copy-start | bytes 24580
  80.4 15.0 %copy-start.21 = (f32[2048]{0:T(1024)S(1)}, f32[2048]{0:T(1024)}, u32[]{:S(2)}) copy-start(f32[2048]{0:T(1024)} %param.36) | copy-start | bytes 24580
  80.9 14.5 %collective-permute-start.2 = (bf16[128,2048]{1,0:T(8,128)(2,1)S(1)}, bf16[128,2048]{1,0:T(8,128)(2,1)S(1)}, u32[]{:S(2)}, u32[]{:S(2)}) collective-permute-start(bf16[128,2048]{1,0:T(8,128)(2,1)S(1)} %get-tuple-element.27), channel_id=1, source_target_pairs={{0,1},{1,2},{2,3},{3,0},{4,5},{5,6},{6,7},{7,4},{8,9},{9,10},{10,1... | collective-permute-start | bytes 1572872 | tf_op jit(solution)/shard_map/ppermute | solution.py:314
  82.5 12.9 %collective-permute-start.3 = (bf16[128,2048]{1,0:T(8,128)(2,1)S(1)}, bf16[128,2048]{1,0:T(8,128)(2,1)S(1)}, u32[]{:S(2)}, u32[]{:S(2)}) collective-permute-start(bf16[128,2048]{1,0:T(8,128)(2,1)S(1)} %get-tuple-element.28), channel_id=1, source_target_pairs={{0,3},{1,0},{2,1},{3,2},{4,7},{5,4},{6,5},{7,6},{8,11},{9,8},{10,9... | collective-permute-start | bytes 1572872 | tf_op jit(solution)/shard_map/ppermute | solution.py:314
  96.6 12.7 %collective-permute-start.6 = (bf16[128,2048]{1,0:T(8,128)(2,1)S(1)}, bf16[128,2048]{1,0:T(8,128)(2,1)S(1)}, u32[]{:S(2)}, u32[]{:S(2)}) collective-permute-start(bf16[128,2048]{1,0:T(8,128)(2,1)S(1)} %get-tuple-element.29.own_ref), channel_id=1, source_target_pairs={{0,3},{1,0},{2,1},{3,2},{4,7},{5,4},{6,5},{7,6},{8,11},{9,8},{10,9... | collective-permute-start | bytes 1572872 | tf_op jit(solution)/shard_map/ppermute | solution.py:314
  99.7 13.5 %collective-permute-start.4 = (bf16[128,2048]{1,0:T(8,128)(2,1)S(1)}, bf16[128,2048]{1,0:T(8,128)(2,1)S(1)}, u32[]{:S(2)}, u32[]{:S(2)}) collective-permute-start(bf16[128,2048]{1,0:T(8,128)(2,1)S(1)} %get-tuple-element.29.own_ref), channel_id=1, source_target_pairs={{0,1},{1,2},{2,3},{3,0},{4,5},{5,6},{6,7},{7,4},{8,9},{9,10},{10,1... | collective-permute-start | bytes 1572872 | tf_op jit(solution)/shard_map/ppermute | solution.py:314
  109.4 7.7 %collective-permute-start.7 = (bf16[64,2048]{1,0:T(8,128)(2,1)S(1)}, bf16[64,2048]{1,0:T(8,128)(2,1)S(1)}, u32[]{:S(2)}, u32[]{:S(2)}) collective-permute-start(bf16[64,2048]{1,0:T(8,128)(2,1)S(1)} %slice.9), channel_id=1, source_target_pairs={{0,3},{1,0},{2,1},{3,2},{4,7},{5,4},{6,5},{7,6},{8,11},{9,8},{10,9... | collective-permute-start | bytes 786440 | tf_op jit(solution)/shard_map/ppermute | solution.py:314
  113.2 7.8 %collective-permute-start.5 = (bf16[64,2048]{1,0:T(8,128)(2,1)S(1)}, bf16[64,2048]{1,0:T(8,128)(2,1)S(1)}, u32[]{:S(2)}, u32[]{:S(2)}) collective-permute-start(bf16[64,2048]{1,0:T(8,128)(2,1)S(1)} %slice.8), channel_id=1, source_target_pairs={{0,1},{1,2},{2,3},{3,0},{4,5},{5,6},{6,7},{7,4},{8,9},{9,10},{10,1... | collective-permute-start | bytes 786440 | tf_op jit(solution)/shard_map/ppermute | solution.py:314
  133.9 9.2 %collective-permute-start.8 = (bf16[1024,128]{1,0:T(8,128)(2,1)S(1)}, bf16[1024,128]{1,0:T(8,128)(2,1)S(1)}, u32[]{:S(2)}, u32[]{:S(2)}) collective-permute-start(bf16[1024,128]{1,0:T(8,128)(2,1)S(1)} %get-tuple-element.34), channel_id=1, source_target_pairs={{0,1},{1,2},{2,3},{3,0},{4,5},{5,6},{6,7},{7,4},{8,9},{9,10},{10,1... | collective-permute-start | bytes 786440 | tf_op jit(solution)/shard_map/ppermute | solution.py:314
  133.9 9.2 %collective-permute-start.9 = (bf16[1024,128]{1,0:T(8,128)(2,1)S(1)}, bf16[1024,128]{1,0:T(8,128)(2,1)S(1)}, u32[]{:S(2)}, u32[]{:S(2)}) collective-permute-start(bf16[1024,128]{1,0:T(8,128)(2,1)S(1)} %get-tuple-element.35), channel_id=1, source_target_pairs={{0,3},{1,0},{2,1},{3,2},{4,7},{5,4},{6,5},{7,6},{8,11},{9,8},{10,9... | collective-permute-start | bytes 786440 | tf_op jit(solution)/shard_map/ppermute | solution.py:314
  143.1 10.9 %copy-start.22 = (f32[2048]{0:T(1024)S(1)}, f32[2048]{0:T(1024)}, u32[]{:S(2)}) copy-start(f32[2048]{0:T(1024)} %param.37) | copy-start | bytes 24580
  143.3 10.6 %collective-permute-start.10 = (bf16[2048,128]{1,0:T(8,128)(2,1)S(1)}, bf16[2048,128]{1,0:T(8,128)(2,1)S(1)}, u32[]{:S(2)}, u32[]{:S(2)}) collective-permute-start(bf16[2048,128]{1,0:T(8,128)(2,1)S(1)} %get-tuple-element.36), channel_id=1, source_target_pairs={{0,1},{1,2},{2,3},{3,0},{4,5},{5,6},{6,7},{7,4},{8,9},{9,10},{10,1... | collective-permute-start | bytes 1572872 | tf_op jit(solution)/shard_map/ppermute | solution.py:314
  143.4 10.6 %collective-permute-start.11 = (bf16[2048,128]{1,0:T(8,128)(2,1)S(1)}, bf16[2048,128]{1,0:T(8,128)(2,1)S(1)}, u32[]{:S(2)}, u32[]{:S(2)}) collective-permute-start(bf16[2048,128]{1,0:T(8,128)(2,1)S(1)} %get-tuple-element.37), channel_id=1, source_target_pairs={{0,3},{1,0},{2,1},{3,2},{4,7},{5,4},{6,5},{7,6},{8,11},{9,8},{10,9... | collective-permute-start | bytes 1572872 | tf_op jit(solution)/shard_map/ppermute | solution.py:314
  (13 other events, 16.7 us)
Sparse Core Ops, SparseCore 0:
  10.1 102.5 all-gather.1

commit v3 on v2

--- a/solution.py
+++ b/solution.py
@@ -101,14 +101,24 @@
     return lax.dot_general(a, b, (((0,), (0,)), ((), ())), preferred_element_type=F32)
 
 
+def turned_span(place, turn):
+    return (turn + jnp.where(place == 0, 2, jnp.where(place == 3, 1, jnp.where(place == 2, 3, 0)))) & 3
+
+
 def states_kernel(
-    _, wk_ref, wv_ref, nk_ref, nv_ref, wd_ref, nd_ref, inside_ref, start_ref,
-    before_ref, earlier_ref, message_ref, rows_ref, state_ref, decay_ref,
+    _, __, wk_ref, wv_ref, nk_ref, nv_ref, wd_ref, nd_ref, inside_ref, start_ref, *refs, staged,
 ):
+    sources, refs = refs[:staged], refs[staged:]
+    before_ref, earlier_ref, message_ref = refs[:3]
+    targets, refs = refs[3 : 3 + staged], refs[3 + staged :]
+    rows_ref, state_ref, decay_ref, sems = refs
     span = pl.program_id(0)
+    copies = [pltpu.make_async_copy(a, b, sems.at[k]) for k, (a, b) in enumerate(zip(sources, targets))]
 
     @pl.when(span == 0)
     def _():
+        for copy in copies:
+            copy.start()
         state_ref[...] = jnp.zeros_like(state_ref)
         decay_ref[...] = jnp.zeros_like(decay_ref)
 
@@ -151,6 +161,8 @@
             ends = jnp.broadcast_to(pair[None], (count, 8, LANES))
             message_ref[at : at + count] = jnp.concatenate([body, ends], axis=1).astype(BF16)
             at += count
+        for copy in copies:
+            copy.wait()
 
 
 def prefix_kernel(message_ref, out_ref):
@@ -170,12 +182,12 @@
 
 
 def finish_kernel(
-    order_ref, wq_ref, wk_ref, wv_ref, wg_ref, nq_ref, nk_ref, nv_ref, ng_ref, wd_ref, nd_ref,
+    index_ref, turn_ref, wq_ref, wk_ref, wv_ref, wg_ref, nq_ref, nk_ref, nv_ref, ng_ref, wd_ref, nd_ref,
     inside_ref, start_ref, before_ref, earlier_ref, prefix_ref, wide_out_ref, narrow_out_ref,
     *out_refs, first,
 ):
     *out_refs, rows_ref, mixed_ref = out_refs
-    span = order_ref[1 + first + pl.program_id(0)]
+    span = turned_span(first + pl.program_id(0), turn_ref[0])
     total = running_decay(wd_ref, nd_ref, rows_ref)
     columns = total.T
     grown = jnp.exp(columns)
@@ -249,11 +261,21 @@
     return values * lax.rsqrt(jnp.mean(values * values, axis=-1, keepdims=True) + EPS) * gain
 
 
-def norms_kernel(own_ref, below_ref, above_ref, residual_ref, mix_ref, pre_ref, updated_ref, normed_ref):
+def norms_kernel(
+    own_ref, below_ref, above_ref, residual_ref, mix_ref, pre_ref, updated_ref, low_ref, high_ref
+):
     projected = own_ref[...].astype(F32) + below_ref[...].astype(F32) + above_ref[...].astype(F32)
     updated = (residual_ref[...].astype(F32) + rms(projected, mix_ref[...])).astype(BF16)
     updated_ref[...] = updated
-    normed_ref[...] = rms(updated.astype(F32), pre_ref[...]).astype(BF16)
+    normed = rms(updated.astype(F32), pre_ref[...]).astype(BF16)
+
+    @pl.when(pl.program_id(0) == 0)
+    def _():
+        low_ref[...] = normed
+
+    @pl.when(pl.program_id(0) == 1)
+    def _():
+        high_ref[...] = normed
 
 
 def result_kernel(own_ref, below_ref, above_ref, updated_ref, gain_ref, out_ref):
@@ -261,52 +283,78 @@
     out_ref[...] = (updated_ref[...].astype(F32) + rms(lowered.T, gain_ref[...])).astype(BF16)
 
 
-def far_mixer_kernel(
-    own_ref, far_low_ref, far_high_ref, below_ref, above_ref, up_ref, down_ref,
-    hidden_ref, out_ref, low_ref, high_ref, x_ref, now_ref, *, steps, block,
-):
-    step = pl.program_id(0)
-    rows = own_ref.shape[0]
-    half = rows // 2
-
-    @pl.when(step == 0)
-    def _():
-        x_ref[0:rows] = own_ref[...]
-        x_ref[rows : rows + half] = far_low_ref[...]
-        x_ref[rows + half : 2 * rows] = far_high_ref[...]
-        x_ref[2 * rows : 3 * rows] = below_ref[...]
-        x_ref[3 * rows :] = above_ref[...]
-
-    @pl.when(step < steps)
-    def _():
-        rectified = jnp.maximum(mm(x_ref[...], up_ref[...].reshape(x_ref.shape[1], block)), 0.0)
+def far_mixer_kernel(*refs, ups, downs):
+    halves, refs = refs[:8], refs[8:]
+    both_ref, hidden_ref, out_ref, low_ref, high_ref, down_ref, up_ref, x_ref, now_ref, sems = refs
+    devices, share, units = up_ref.shape
+    half = halves[0].shape[0]
+    rows = 2 * half
+    block = units // ups
+    group = devices // downs
+    lines = group * share
+
+    def up_copy(k):
+        at = pl.multiple_of(k * block, block)
+        return pltpu.make_async_copy(
+            both_ref.at[:, 0, :, pl.ds(at, block)], up_ref.at[:, :, pl.ds(at, block)], sems.at[k]
+        )
+
+    def down_copy(k):
+        at = k * group
+        return pltpu.make_async_copy(
+            both_ref.at[pl.ds(at, group), 1], down_ref.at[pl.ds(at, group)], sems.at[ups + k]
+        )
+
+    for k in range(ups):
+        up_copy(k).start()
+    for k in range(downs):
+        down_copy(k).start()
+    for k, ref in enumerate(halves):
+        x_ref[k * half : (k + 1) * half] = ref[...]
+
+    @pl.loop(0, ups)
+    def _(k):
+        up_copy(k).wait()
+        at = pl.multiple_of(k * block, block)
+        weight = up_ref[:, :, pl.ds(at, block)].reshape(devices * share, block)
+        rectified = jnp.maximum(mm(x_ref[...], weight), 0.0)
         hidden = (rectified * rectified).astype(BF16).T
-        hidden_ref[...] = hidden[:, 2 * rows :]
-        now_ref[pl.ds(pl.multiple_of(step * block, block), block), :] = hidden[:, : 2 * rows]
-
-    @pl.when(step >= steps)
-    def _():
-        lowered = mm(down_ref[...].reshape(block, now_ref.shape[0]), now_ref[...]).astype(BF16)
-        out_ref[...] = lowered[:, :rows]
-
-        @pl.when(step < steps + steps // 2)
-        def _():
-            low_ref[...] = lowered[:, rows:]
-
-        @pl.when(step >= steps + steps // 2)
-        def _():
-            high_ref[...] = lowered[:, rows:]
-
-
-def near_mixer_kernel(hidden_ref, down_ref, minus_ref, plus_ref):
-    lowered = mm(down_ref[...].reshape(-1, hidden_ref.shape[0]), hidden_ref[...]).astype(BF16)
+        hidden_ref[pl.ds(at, block), :] = hidden[:, 2 * rows :]
+        now_ref[pl.ds(at, block), :] = hidden[:, : 2 * rows]
+
+    def lower(k, far_ref, base):
+        down_copy(k).wait()
+        weight = down_ref[pl.ds(k * group, group)].reshape(lines, units)
+        lowered = mm(weight, now_ref[...]).astype(BF16)
+        out_ref[pl.ds(pl.multiple_of(k * lines, lines), lines), :] = lowered[:, :rows]
+        far_ref[pl.ds(pl.multiple_of((k - base) * lines, lines), lines), :] = lowered[:, rows:]
+
+    @pl.loop(0, downs // 2)
+    def _(k):
+        lower(k, low_ref, 0)
+
+    @pl.loop(downs // 2, downs)
+    def _(k):
+        lower(k, high_ref, downs // 2)
+
+
+def near_mixer_kernel(hidden_ref, down_ref, minus_ref, plus_ref, *, parts):
+    devices, share, units = down_ref.shape
+    group = devices // parts
+    lines = group * share
     rows = minus_ref.shape[1]
-    minus_ref[...] = lowered[:, :rows]
-    plus_ref[...] = lowered[:, rows:]
+
+    @pl.loop(0, parts)
+    def _(k):
+        weight = down_ref[pl.ds(k * group, group)].reshape(lines, units)
+        lowered = mm(weight, hidden_ref[...]).astype(BF16)
+        at = pl.multiple_of(k * lines, lines)
+        minus_ref[pl.ds(at, lines), :] = lowered[:, :rows]
+        plus_ref[pl.ds(at, lines), :] = lowered[:, rows:]
 
 
 SMALL = pltpu.CompilerParams(vmem_limit_bytes=16 * 1024 * 1024)
-LARGE = pltpu.CompilerParams(vmem_limit_bytes=50 * 1024 * 1024)
+LARGE = pltpu.CompilerParams(vmem_limit_bytes=32 * 1024 * 1024)
 
 
 def shifted(array, axis, by):
@@ -355,51 +403,72 @@
     ).reshape(devices, 2, share, units)
 
     inside, starts = (jnp.asarray(t) for t in position_tables(devices))
-    turn = lax.axis_index("tp")
-    order = jnp.stack(
-        [lax.axis_index(SP), (turn + 2) % ranks, turn, (turn + ranks - 1) % ranks, (turn + 1) % ranks]
-    ).astype(jnp.int32)
+    scalars = [
+        lax.axis_index(SP).astype(jnp.int32).reshape(1),
+        lax.axis_index("tp").astype(jnp.int32).reshape(1),
+    ]
     table_blocks = [
-        pl.BlockSpec((4, SPAN, LANES), lambda s, i: (0, 0, 0)),
-        pl.BlockSpec((1, 4 * SPANS, LANES), lambda s, i: (i[0], 0, 0)),
+        pl.BlockSpec((4, SPAN, LANES), lambda s, i, t: (0, 0, 0)),
+        pl.BlockSpec((1, 4 * SPANS, LANES), lambda s, i, t: (i[0], 0, 0)),
     ]
 
     def span_blocks(at):
         return (
-            pl.BlockSpec((SPAN, 384), lambda s, i: (at(s, i), 0)),
-            pl.BlockSpec((SPAN, 128), lambda s, i: (at(s, i), 0)),
+            pl.BlockSpec((SPAN, 384), lambda s, i, t: (at(s, i, t), 0)),
+            pl.BlockSpec((SPAN, 128), lambda s, i, t: (at(s, i, t), 0)),
             [
-                pl.BlockSpec((3, SPAN), lambda s, i: (0, at(s, i))),
-                pl.BlockSpec((2, SPAN), lambda s, i: (0, at(s, i))),
+                pl.BlockSpec((3, SPAN), lambda s, i, t: (0, at(s, i, t))),
+                pl.BlockSpec((2, SPAN), lambda s, i, t: (0, at(s, i, t))),
             ],
             [
-                pl.BlockSpec((1, 512, LANES), lambda s, i: (at(s, i), 0, 0)),
-                pl.BlockSpec((1, 8, LANES), lambda s, i: (at(s, i), 0, 0)),
+                pl.BlockSpec((1, 512, LANES), lambda s, i, t: (at(s, i, t), 0, 0)),
+                pl.BlockSpec((1, 8, LANES), lambda s, i, t: (at(s, i, t), 0, 0)),
             ],
         )
 
-    wide_block, narrow_block, decay_blocks, state_blocks = span_blocks(lambda s, i: s)
-    before, earlier, message = pl.pallas_call(
-        states_kernel,
+    wide_block, narrow_block, decay_blocks, state_blocks = span_blocks(lambda s, i, t: s)
+    staged = (wide_gate, narrow_query, narrow_value, narrow_gate, narrow_out)
+    before, earlier, message, *held = pl.pallas_call(
+        functools.partial(states_kernel, staged=len(staged)),
         out_shape=(
             jax.ShapeDtypeStruct((SPANS, 512, LANES), F32),
             jax.ShapeDtypeStruct((SPANS, 8, LANES), F32),
             jax.ShapeDtypeStruct((devices, 16, LANES), BF16),
+            *(pltpu.VMEM(x.shape, x.dtype) for x in staged),
         ),
         grid_spec=pltpu.PrefetchScalarGridSpec(
-            num_scalar_prefetch=1,
+            num_scalar_prefetch=2,
             grid=(SPANS,),
-            in_specs=[wide_block, wide_block, narrow_block, narrow_block, *decay_blocks, *table_blocks],
-            out_specs=[*state_blocks, pl.BlockSpec((devices, 16, LANES), lambda s, i: (0, 0, 0))],
+            in_specs=[
+                wide_block, wide_block, narrow_block, narrow_block, *decay_blocks, *table_blocks,
+                *([pl.BlockSpec(memory_space=pltpu.HBM)] * len(staged)),
+            ],
+            out_specs=[
+                *state_blocks,
+                pl.BlockSpec((devices, 16, LANES), lambda s, i, t: (0, 0, 0)),
+                *([pl.BlockSpec(memory_space=pltpu.VMEM)] * len(staged)),
+            ],
             scratch_shapes=[
                 pltpu.VMEM((8, LANES), F32),
                 pltpu.VMEM((512, LANES), F32),
                 pltpu.VMEM((8, LANES), F32),
+                pltpu.SemaphoreType.DMA((len(staged),)),
             ],
         ),
+        compiler_params=SMALL,
         name="states",
         cost_estimate=pl.CostEstimate(flops=60_000_000, bytes_accessed=2_500_000, transcendentals=20_000),
-    )(order, wide_key, wide_value, narrow_key, narrow_value, wide_decay, narrow_decay, inside, starts)
+    )(
+        *scalars,
+        *(
+            pltpu.with_memory_space_constraint(x, pltpu.HBM)
+            for x in (
+                wide_key, wide_value, narrow_key, narrow_value,
+                wide_decay, narrow_decay, inside, starts, *staged,
+            )
+        ),
+    )
+    gate_held, query_held, value_held, narrow_gate_held, out_held = held
 
     arrived = lax.all_to_all(message, SP, 0, 0, tiled=True)
     prefixes = pl.pallas_call(
@@ -412,19 +481,19 @@
     prefix = lax.all_to_all(prefixes, SP, 0, 0, tiled=True).reshape(512, LANES)
 
     def finish(first, count, out_shape, out_specs):
-        wide, narrow, decays, states = span_blocks(lambda s, i: i[1 + first + s])
+        wide, narrow, decays, states = span_blocks(lambda s, i, t: turned_span(first + s, t[0]))
         return pl.pallas_call(
             functools.partial(finish_kernel, first=first),
             out_shape=out_shape,
             grid_spec=pltpu.PrefetchScalarGridSpec(
-                num_scalar_prefetch=1,
+                num_scalar_prefetch=2,
                 grid=(count,),
                 in_specs=[
                     wide, wide, wide, wide, narrow, narrow, narrow, narrow,
                     *decays, *table_blocks, *states,
-                    pl.BlockSpec((512, LANES), lambda s, i: (0, 0)),
-                    pl.BlockSpec((384, width), lambda s, i: (0, 0)),
-                    pl.BlockSpec((128, width), lambda s, i: (0, 0)),
+                    pl.BlockSpec((512, LANES), lambda s, i, t: (0, 0)),
+                    pl.BlockSpec((384, width), lambda s, i, t: (0, 0)),
+                    pl.BlockSpec((128, width), lambda s, i, t: (0, 0)),
                 ],
                 out_specs=out_specs,
                 scratch_shapes=[pltpu.VMEM((8, LANES), F32), pltpu.VMEM((SPAN, 512), BF16)],
@@ -437,90 +506,80 @@
                 transcendentals=150_000 * count,
             ),
         )(
-            order, wide_query, wide_key, wide_value, wide_gate,
-            narrow_query, narrow_key, narrow_value, narrow_gate,
-            wide_decay, narrow_decay, inside, starts, before, earlier, prefix, wide_out, narrow_out,
+            *scalars, wide_query, wide_key, wide_value, gate_held,
+            query_held, narrow_key, value_held, narrow_gate_held,
+            wide_decay, narrow_decay, inside, starts, before, earlier, prefix, wide_out, out_held,
         )
 
     half = rows // 2
     half_out = jax.ShapeDtypeStruct((half, width), BF16)
     near_out = jax.ShapeDtypeStruct((3, rows, width), BF16)
     low, high = finish(
-        0, 1, (half_out, half_out), [pl.BlockSpec((half, width), lambda s, i: (0, 0))] * 2
+        0, 1, (half_out, half_out), [pl.BlockSpec((half, width), lambda s, i, t: (0, 0))] * 2
     )
     low, high = shifted(low, "tp", 1), shifted(high, "tp", -1)
     (near,) = finish(
-        1, 3, (near_out,), [pl.BlockSpec((1, rows, width), lambda s, i: (s, 0, 0))]
+        1, 3, (near_out,), [pl.BlockSpec((1, rows, width), lambda s, i, t: (s, 0, 0))]
     )
     minus, plus = joined(near, near, low, high, (1, 2))
     below, above = shifted(plus, "tp", 1), shifted(minus, "tp", -1)
-    lines = 32
-    flat = pl.BlockSpec((lines, width), lambda i: (i, 0))
+    flat = pl.BlockSpec((half, width), lambda i: (i, 0))
+    kept = pl.BlockSpec((half, width), lambda i: (0, 0))
     gain = pl.BlockSpec((1, width), lambda i: (0, 0))
-    updated, normed = pl.pallas_call(
+    updated, low, high = pl.pallas_call(
         norms_kernel,
-        out_shape=[jax.ShapeDtypeStruct((rows, width), BF16)] * 2,
-        grid=(rows // lines,),
+        out_shape=[jax.ShapeDtypeStruct((rows, width), BF16), half_out, half_out],
+        grid=(2,),
         in_specs=[
-            pl.BlockSpec((None, lines, width), lambda i: (0, i, 0)), flat, flat, flat, gain, gain,
+            pl.BlockSpec((None, half, width), lambda i: (0, i, 0)), flat, flat, flat, gain, gain,
         ],
-        out_specs=[flat, flat],
+        out_specs=[flat, kept, kept],
         compiler_params=SMALL,
         name="norms",
         cost_estimate=pl.CostEstimate(flops=4_000_000, bytes_accessed=3_500_000, transcendentals=300),
     )(near, below, above, residual, gain_mix.reshape(1, width), gain_pre.reshape(1, width))
-    below, above = shifted(normed, "tp", 1), shifted(normed, "tp", -1)
-    low, high = shifted(below[:half], "tp", 1), shifted(above[half:], "tp", -1)
-
-    block = min(1024, units // 2)
-    steps, halves = units // block, units // block // 2
-    resident = pl.BlockSpec((rows, width), lambda i: (0, 0))
-    resident_half = pl.BlockSpec((half, width), lambda i: (0, 0))
-    turned = jax.ShapeDtypeStruct((width, rows), BF16)
-    turned_half = jax.ShapeDtypeStruct((width // 2, rows), BF16)
-    hidden, own, low, high = pl.pallas_call(
-        functools.partial(far_mixer_kernel, steps=steps, block=block),
+    below_low, above_high = shifted(low, "tp", 1), shifted(high, "tp", -1)
+    below_high, above_low = shifted(high, "tp", 1), shifted(low, "tp", -1)
+    far_low, far_high = shifted(below_low, "tp", 1), shifted(above_high, "tp", -1)
+
+    ups, downs = 4, 4
+    whole = pl.BlockSpec(memory_space=pltpu.VMEM)
+    turned_half = pltpu.VMEM((width // 2, rows), BF16)
+    hidden, own, low, high, down = pl.pallas_call(
+        functools.partial(far_mixer_kernel, ups=ups, downs=downs),
         out_shape=(
-            jax.ShapeDtypeStruct((units, 2 * rows), BF16), turned, turned_half, turned_half,
+            pltpu.VMEM((units, 2 * rows), BF16),
+            pltpu.VMEM((width, rows), BF16),
+            turned_half,
+            turned_half,
+            pltpu.VMEM((devices, share, units), BF16),
         ),
-        grid=(2 * steps,),
-        in_specs=[
-            resident, resident_half, resident_half, resident, resident,
-            pl.BlockSpec((devices, 1, share, block), lambda i: (0, 0, 0, jnp.minimum(i, steps - 1))),
-            pl.BlockSpec(
-                (block // share, 1, share, units), lambda i: (jnp.maximum(i - steps, 0), 1, 0, 0)
-            ),
+        in_specs=[*([whole] * 8), pl.BlockSpec(memory_space=pltpu.HBM)],
+        out_specs=[whole] * 5,
+        scratch_shapes=[
+            pltpu.VMEM((devices, share, units), BF16),
+            pltpu.VMEM((4 * rows, width), BF16),
+            pltpu.VMEM((units, 2 * rows), BF16),
+            pltpu.SemaphoreType.DMA((ups + downs,)),
         ],
-        out_specs=[
-            pl.BlockSpec((block, 2 * rows), lambda i: (jnp.minimum(i, steps - 1), 0)),
-            pl.BlockSpec((block, rows), lambda i: (jnp.maximum(i - steps, 0), 0)),
-            pl.BlockSpec((block, rows), lambda i: (jnp.clip(i - steps, 0, halves - 1), 0)),
-            pl.BlockSpec((block, rows), lambda i: (jnp.clip(i - steps - halves, 0, halves - 1), 0)),
-        ],
-        scratch_shapes=[pltpu.VMEM((4 * rows, width), BF16), pltpu.VMEM((units, 2 * rows), BF16)],
         compiler_params=LARGE,
         name="mixer_far",
         cost_estimate=pl.CostEstimate(
             flops=12 * rows * width * units, bytes_accessed=20_000_000, transcendentals=0
         ),
-    )(normed, low, high, below, above, both, both)
+    )(low, high, far_low, far_high, below_low, below_high, above_low, above_high, both)
     low, high = shifted(low, "tp", 1), shifted(high, "tp", -1)
-    lasts = pl.BlockSpec((block, rows), lambda i: (i, 0))
     minus, plus = pl.pallas_call(
-        near_mixer_kernel,
-        out_shape=(turned, turned),
-        grid=(width // block,),
-        in_specs=[
-            pl.BlockSpec((units, 2 * rows), lambda i: (0, 0)),
-            pl.BlockSpec((block // share, 1, share, units), lambda i: (i, 1, 0, 0)),
-        ],
-        out_specs=[lasts, lasts],
-        compiler_params=LARGE,
+        functools.partial(near_mixer_kernel, parts=2),
+        out_shape=(jax.ShapeDtypeStruct((width, rows), BF16),) * 2,
+        in_specs=[whole] * 2,
+        out_specs=[whole] * 2,
+        compiler_params=SMALL,
         name="mixer_near",
         cost_estimate=pl.CostEstimate(
-            flops=4 * rows * width * units, bytes_accessed=12_000_000, transcendentals=0
+            flops=4 * rows * width * units, bytes_accessed=2_000_000, transcendentals=0
         ),
-    )(hidden, both)
+    )(hidden, down)
     minus, plus = joined(minus, plus, low, high)
     below, above = shifted(plus, "tp", 1), shifted(minus, "tp", -1)
     return pl.pallas_call(

time: 164 us -> 158 us (0.963)
  Pallas kernels: 36.2 us -> 28.3 us
  local copies, waits for them, and re-layouts: 11.7 us -> 8.69 us
  waiting for transfers between devices: 36.1 us -> 39 us
  starting transfers between devices: 20.2 us -> 21.9 us
    pallas_call x3, Pallas kernels: 24.6 us -> 18 us  [the longest x1 9.89 us: local(): pl.pallas_call(functools.partial(far_mixer_kernel, ups=ups, downs=downs),...]
    unnamed x48 -> x26, local copies, waits for them, and re-layouts: 11 us -> 8.69 us
    ppermute x12 -> x14, starting transfers between devices: 20.2 us -> 21.9 us  [shifted(): lax.ppermute(array, axis, [(k, (k + by) % size) for k in range(size)])]
    ppermute x12 -> x14, waiting for transfers between devices: 36.1 us -> 37.6 us  [shifted(): lax.ppermute(array, axis, [(k, (k + by) % size) for k in range(size)])]
  transfers between devices with their start and end apart: 13 -> 15, of which waited for: 7 -> 9; matrix products, arithmetic and copies ran while one was open for 0% -> 0% of each run, Pallas kernels for 13% -> 11%
where the time goes in v3:
time: 158 us; the launch traced here: 156 us
  blocking collectives  42.8 us (27%)
  waiting for transfers between devices  39 us (25%)
  Pallas kernels  28.3 us (18%)
  starting transfers between devices  21.9 us (14%)
  between operations  13.5 us (9%)
  local copies, waits for them, and re-layouts  8.69 us (6%)
  other arithmetic  1.69 us (1%)
    ppermute x14, waiting for transfers between devices, shifted(): lax.ppermute(array, axis, [(k, (k + by) % size) for k in range(size)])  37.6 us
    all_to_all x1, blocking collectives, local(): arrived = lax.all_to_all(message, SP, 0, 0, tiled=True)  25.3 us
    ppermute x14, starting transfers between devices, shifted(): lax.ppermute(array, axis, [(k, (k + by) % size) for k in range(size)])  21.9 us
    all_to_all x1, blocking collectives, local(): prefix = lax.all_to_all(prefixes, SP, 0, 0, tiled=True).reshape(512, LANES)  17.5 us
    pallas_call x1, Pallas kernels, local(): pl.pallas_call(functools.partial(far_mixer_kernel, ups=ups, downs=downs),...  9.89 us
    unnamed x26, local copies, waits for them, and re-layouts  8.69 us
    pallas_call x2, Pallas kernels, finish(): pl.pallas_call(functools.partial(finish_kernel, first=first), out_shape=o...  7.48 us
    pallas_call x1, Pallas kernels, local(): pl.pallas_call(functools.partial(states_kernel, staged=len(staged)), out_...  5.66 us
  transfers between devices with their start and end apart: 15, of which 9 were waited for; matrix products, arithmetic and copies ran while one was open for 0% of the time, Pallas kernels for 11%

profile of v3, /device:TPU:32, one launch (start us, length us, event | category | flops | bytes accessed | tf_op | source)
XLA Modules:
  0.0 155.9 jit_solution(10360466241893661689)
XLA Ops:
  6.5 1.7 %pad_maximum_fusion = bf16[64,2048]{1,0:T(8,128)(2,1)} fusion(bf16[32,2048]{1,0:T(8,128)(2,1)} %bitcast.13, bf16[32,2048]{1,0:T(8,128)(2,1)} %param.33), kind=kLoop, calls=%fused_computation | loop fusion | flops 524288 | bytes 524288 | tf_op jit(solution)/shard_map/concatenate | solution.py:402
  8.3 5.7 %states.1 = (f32[4,512,128]{2,1,0:T(8,128)S(1)}, f32[4,8,128]{2,1,0:T(8,128)S(1)}, bf16[64,16,128]{2,1,0:T(8,128)(2,1)S(1)}, bf16[512,384]{1,0:T(8,128)(2,1)S(1)...) custom-call(s32[1]{0:T(128)} %bitcast._.index_ref, ...), custom_call_target="tpu_custom_call" | custom-call | flops 60000000 | bytes 2500000 | tf_op jit(solution)/shard_map/states/pallas_call | solution.py:431
  13.9 25.3 %all_to_all.10.message_ref = bf16[64,16,128]{2,1,0:T(8,128)(2,1)S(1)} all-to-all(bf16[64,16,128]{2,1,0:T(8,128)(2,1)S(1)} %get-tuple-element.35), channel_id=1, replica_groups=mesh['sp_0'=8,'sp_1'=4,'sp_2'=2,'tp'=4] {'sp_0','sp_1','sp_2'}, dimensions={0} | all-to-all | bytes 524288 | tf_op jit(solution)/shard_map/all_to_all | solution.py:473
  39.4 17.5 %all_to_all.11 = bf16[64,8,128]{2,1,0:T(8,128)(2,1)S(1)} all-to-all(bf16[64,8,128]{2,1,0:T(8,128)(2,1)S(1)} %prefix.1), channel_id=1, replica_groups=mesh['sp_0'=8,'sp_1'=4,'sp_2'=2,'tp'=4] {'sp_0','sp_1','sp_2'}, dimensions={0} | all-to-all | bytes 262144 | tf_op jit(solution)/shard_map/all_to_all | solution.py:481
  65.6 1.9 %finish_far.1 = (bf16[64,2048]{1,0:T(8,128)(2,1)S(1)}, bf16[64,2048]{1,0:T(8,128)(2,1)S(1)}) custom-call(s32[1]{0:T(128)} %bitcast._.index_ref, s32[1]{0:T(128)} %bitcast.1.__.turn_ref, bf16[512,384]{1,0:T(8,128)(2,1)S(1)} %copy-done.5, bf16[512,384]{1,0:T(8,128)(2,1)S(1)} %copy-done.2, bf16[512,384]{1,0:T(8,128)(2,1)S(1)} %copy-done.3, ...), custom_call_target="tpu_custom_call" | custom-call | flops 350000000 | bytes 4500000 | tf_op jit(solution)/shard_map/finish_far/pallas_call | solution.py:485
  67.5 1.5 collective-permute-start
  69.0 1.8 %collective-permute-start.1 = (bf16[64,2048]{1,0:T(8,128)(2,1)S(1)}, bf16[64,2048]{1,0:T(8,128)(2,1)S(1)}, u32[]{:S(2)}, u32[]{:S(2)}) collective-permute-start(bf16[64,2048]{1,0:T(8,128)(2,1)S(1)} %get-tuple-element.38), channel_id=1, source_target_pairs={{0,3},{1,0},{2,1},{3,2},{4,7},{5,4},{6,5},{7,6},{8,11},{9,8},{10,9... | collective-permute-start | bytes 786440 | tf_op jit(solution)/shard_map/ppermute | solution.py:362
  70.8 5.6 %finish.1.minus_ref.plus_ref.own_ref = bf16[3,128,2048]{2,1,0:T(8,128)(2,1)S(1)} custom-call(s32[1]{0:T(128)} %bitcast._.index_ref, s32[1]{0:T(128)} %bitcast.1.__.turn_ref, bf16[512,384]{1,0:T(8,128)(2,1)S(1)} %copy-done.5, bf16[512,384]{1,0:T(8,128)(2,1)S(1)} %copy-done.2, bf16[512,384]{1,0:T(8,128)(2,1)S(1)} %copy-done.3, ...), custom_call_target="tpu_custom_call" | custom-call | flops 1050000000 | bytes 7500000 | tf_op jit(solution)/shard_map/finish/pallas_call | solution.py:485
  77.3 1.7 %collective-permute-start.2 = (bf16[128,2048]{1,0:T(8,128)(2,1)S(1)}, bf16[128,2048]{1,0:T(8,128)(2,1)S(1)}, u32[]{:S(2)}, u32[]{:S(2)}) collective-permute-start(bf16[128,2048]{1,0:T(8,128)(2,1)S(1)} %get-tuple-element.39), channel_id=1, source_target_pairs={{0,1},{1,2},{2,3},{3,0},{4,5},{5,6},{6,7},{7,4},{8,9},{9,10},{10,1... | collective-permute-start | bytes 1572872 | tf_op jit(solution)/shard_map/ppermute | solution.py:362
  78.9 1.6 %collective-permute-start.3 = (bf16[128,2048]{1,0:T(8,128)(2,1)S(1)}, bf16[128,2048]{1,0:T(8,128)(2,1)S(1)}, u32[]{:S(2)}, u32[]{:S(2)}) collective-permute-start(bf16[128,2048]{1,0:T(8,128)(2,1)S(1)} %get-tuple-element.40), channel_id=1, source_target_pairs={{0,3},{1,0},{2,1},{3,2},{4,7},{5,4},{6,5},{7,6},{8,11},{9,8},{10,9... | collective-permute-start | bytes 1572872 | tf_op jit(solution)/shard_map/ppermute | solution.py:362
  80.6 11.2 %collective-permute-done.2.below_ref = bf16[128,2048]{1,0:T(8,128)(2,1)S(1)} collective-permute-done((bf16[128,2048]{1,0:T(8,128)(2,1)S(1)}, bf16[128,2048]{1,0:T(8,128)(2,1)S(1)}, u32[]{:S(2)}, u32[]{:S(2)}) %collective-permute-start.2) | collective-permute-done | bytes 524320 | tf_op jit(solution)/shard_map/ppermute | solution.py:362
  93.8 2.1 %collective-permute-start.6 = (bf16[64,2048]{1,0:T(8,128)(2,1)S(1)}, bf16[64,2048]{1,0:T(8,128)(2,1)S(1)}, u32[]{:S(2)}, u32[]{:S(2)}) collective-permute-start(bf16[64,2048]{1,0:T(8,128)(2,1)S(1)} %get-tuple-element.42.refs_1_), channel_id=1, source_target_pairs={{0,3},{1,0},{2,1},{3,2},{4,7},{5,4},{6,5},{7,6},{8,11},{9,8},{10,9... | collective-permute-start | bytes 786440 | tf_op jit(solution)/shard_map/ppermute | solution.py:362
  95.9 1.7 %collective-permute-start.9 = (bf16[64,2048]{1,0:T(8,128)(2,1)S(1)}, bf16[64,2048]{1,0:T(8,128)(2,1)S(1)}, u32[]{:S(2)}, u32[]{:S(2)}) collective-permute-start(bf16[64,2048]{1,0:T(8,128)(2,1)S(1)} %get-tuple-element.41.refs_0_), channel_id=1, source_target_pairs={{0,3},{1,0},{2,1},{3,2},{4,7},{5,4},{6,5},{7,6},{8,11},{9,8},{10,9... | collective-permute-start | bytes 786440 | tf_op jit(solution)/shard_map/ppermute | solution.py:362
  98.0 4.5 %collective-permute-done.4.refs_4_ = bf16[64,2048]{1,0:T(8,128)(2,1)S(1)} collective-permute-done((bf16[64,2048]{1,0:T(8,128)(2,1)S(1)}, bf16[64,2048]{1,0:T(8,128)(2,1)S(1)}, u32[]{:S(2)}, u32[]{:S(2)}) %collective-permute-start.4) | collective-permute-done | bytes 262176 | tf_op jit(solution)/shard_map/ppermute | solution.py:362
  103.0 3.3 %collective-permute-start.7 = (bf16[64,2048]{1,0:T(8,128)(2,1)S(1)}, bf16[64,2048]{1,0:T(8,128)(2,1)S(1)}, u32[]{:S(2)}, u32[]{:S(2)}) collective-permute-start(bf16[64,2048]{1,0:T(8,128)(2,1)S(1)} %collective-permute-done.6.refs_7_), channel_id=1, source_target_pairs={{0,3},{1,0},{2,1},{3,2},{4,7},{5,4},{6,5},{7,6},{8,11},{9,8},{10,9... | collective-permute-start | bytes 786440 | tf_op jit(solution)/shard_map/ppermute | solution.py:362
  106.3 1.9 %collective-permute-done.9.refs_6_ = bf16[64,2048]{1,0:T(8,128)(2,1)S(1)} collective-permute-done((bf16[64,2048]{1,0:T(8,128)(2,1)S(1)}, bf16[64,2048]{1,0:T(8,128)(2,1)S(1)}, u32[]{:S(2)}, u32[]{:S(2)}) %collective-permute-start.9) | collective-permute-done | bytes 262176 | tf_op jit(solution)/shard_map/ppermute | solution.py:362
  108.3 3.7 %collective-permute-done.5.refs_2_ = bf16[64,2048]{1,0:T(8,128)(2,1)S(1)} collective-permute-done((bf16[64,2048]{1,0:T(8,128)(2,1)S(1)}, bf16[64,2048]{1,0:T(8,128)(2,1)S(1)}, u32[]{:S(2)}, u32[]{:S(2)}) %collective-permute-start.5) | collective-permute-done | bytes 262176 | tf_op jit(solution)/shard_map/ppermute | solution.py:362
  113.3 9.9 %mixer_far.1 = (bf16[2048,256]{1,0:T(8,128)(2,1)S(1)}, bf16[2048,128]{1,0:T(8,128)(2,1)S(1)}, bf16[1024,128]{1,0:T(8,128)(2,1)S(1)}, bf16[1024,128]{1,0:T(8,128)(2,1)S(1)}, bf16[64,32,2048]{2,1,0:T(8,128)(2,1)S(1)}) custom-call(bf16[64,2048]{1,0:T(8,128)(2,1)S(1)} %get-tuple-element.41.refs_0_, bf16[64,2048]{1,0:T(8,128)(2,1)S(1)} %get-tuple-element.42.refs_1_, ...), custom_call_target="tpu_custom_call" | custom-call | flops 6442450944 | bytes 20000000 | tf_op jit(solution)/shard_map/mixer_far/pallas_call | solution.py:548
  123.2 1.5 collective-permute-start.10
  124.7 1.8 %collective-permute-start.11 = (bf16[1024,128]{1,0:T(8,128)(2,1)S(1)}, bf16[1024,128]{1,0:T(8,128)(2,1)S(1)}, u32[]{:S(2)}, u32[]{:S(2)}) collective-permute-start(bf16[1024,128]{1,0:T(8,128)(2,1)S(1)} %get-tuple-element.49), channel_id=1, source_target_pairs={{0,3},{1,0},{2,1},{3,2},{4,7},{5,4},{6,5},{7,6},{8,11},{9,8},{10,9... | collective-permute-start | bytes 786440 | tf_op jit(solution)/shard_map/ppermute | solution.py:362
  126.6 2.5 %mixer_near.1 = (bf16[2048,128]{1,0:T(8,128)(2,1)S(1)}, bf16[2048,128]{1,0:T(8,128)(2,1)S(1)}) custom-call(bf16[2048,256]{1,0:T(8,128)(2,1)S(1)} %get-tuple-element.44.hidden_ref, bf16[64,32,2048]{2,1,0:T(8,128)(2,1)S(1)} %get-tuple-element.45.down_ref), custom_call_target="tpu_custom_call" | custom-call | flops 2147483648 | bytes 2000000 | tf_op jit(solution)/shard_map/mixer_near/pallas_call | solution.py:572
  129.1 3.9 %collective-permute-done.10.from_below_ref = bf16[1024,128]{1,0:T(8,128)(2,1)S(1)} collective-permute-done((bf16[1024,128]{1,0:T(8,128)(2,1)S(1)}, bf16[1024,128]{1,0:T(8,128)(2,1)S(1)}, u32[]{:S(2)}, u32[]{:S(2)}) %collective-permute-start.10) | collective-permute-done | bytes 262176 | tf_op jit(solution)/shard_map/ppermute | solution.py:362
  134.7 1.8 %collective-permute-start.13 = (bf16[2048,128]{1,0:T(8,128)(2,1)S(1)}, bf16[2048,128]{1,0:T(8,128)(2,1)S(1)}, u32[]{:S(2)}, u32[]{:S(2)}) collective-permute-start(bf16[2048,128]{1,0:T(8,128)(2,1)S(1)} %get-tuple-element.51), channel_id=1, source_target_pairs={{0,3},{1,0},{2,1},{3,2},{4,7},{5,4},{6,5},{7,6},{8,11},{9,8},{10,9... | collective-permute-start | bytes 1572872 | tf_op jit(solution)/shard_map/ppermute | solution.py:362
  136.5 11.2 %collective-permute-done.12.below_ref = bf16[2048,128]{1,0:T(8,128)(2,1)S(1)} collective-permute-done((bf16[2048,128]{1,0:T(8,128)(2,1)S(1)}, bf16[2048,128]{1,0:T(8,128)(2,1)S(1)}, u32[]{:S(2)}, u32[]{:S(2)}) %collective-permute-start.12) | collective-permute-done | bytes 524320 | tf_op jit(solution)/shard_map/ppermute | solution.py:362
  (46 shorter events, 16.9 us)
Async XLA Ops:
  6.5 106.8 %all-gather.2.cloned.1.call-start = ((), (), s32[]{:S(2)}) async-start(), calls=%async_computation.2 | async-start | bytes 17039360 | tf_op jit(solution)/shard_map/all_gather | solution.py:401
  56.9 1.4 copy-start
  58.3 1.0 copy-start.1
  59.4 1.0 copy-start.2
  60.4 1.0 copy-start.3
  62.3 1.0 copy-start.5
  65.6 26.2 %copy-start.7 = (bf16[128,2048]{1,0:T(8,128)(2,1)S(1)}, bf16[128,2048]{1,0:T(8,128)(2,1)}, u32[]{:S(2)}) copy-start(bf16[128,2048]{1,0:T(8,128)(2,1)} %residual_ref.1) | copy-start | bytes 1572868
  65.6 26.2 %copy-start.10 = (f32[2048]{0:T(1024)S(1)}, f32[2048]{0:T(1024)}, u32[]{:S(2)}) copy-start(f32[2048]{0:T(1024)} %param.35) | copy-start | bytes 24580
  65.6 26.2 %copy-start.11 = (f32[2048]{0:T(1024)S(1)}, f32[2048]{0:T(1024)}, u32[]{:S(2)}) copy-start(f32[2048]{0:T(1024)} %param.36) | copy-start | bytes 24580
  67.5 9.6 %collective-permute-start = (bf16[64,2048]{1,0:T(8,128)(2,1)S(1)}, bf16[64,2048]{1,0:T(8,128)(2,1)S(1)}, u32[]{:S(2)}, u32[]{:S(2)}) collective-permute-start(bf16[64,2048]{1,0:T(8,128)(2,1)S(1)} %get-tuple-element.37), channel_id=1, source_target_pairs={{0,1},{1,2},{2,3},{3,0},{4,5},{5,6},{6,7},{7,4},{8,9},{9,10},{10,1... | collective-permute-start | bytes 786440 | tf_op jit(solution)/shard_map/ppermute | solution.py:362
  69.0 8.1 %collective-permute-start.1 = (bf16[64,2048]{1,0:T(8,128)(2,1)S(1)}, bf16[64,2048]{1,0:T(8,128)(2,1)S(1)}, u32[]{:S(2)}, u32[]{:S(2)}) collective-permute-start(bf16[64,2048]{1,0:T(8,128)(2,1)S(1)} %get-tuple-element.38), channel_id=1, source_target_pairs={{0,3},{1,0},{2,1},{3,2},{4,7},{5,4},{6,5},{7,6},{8,11},{9,8},{10,9... | collective-permute-start | bytes 786440 | tf_op jit(solution)/shard_map/ppermute | solution.py:362
  77.3 14.5 %collective-permute-start.2 = (bf16[128,2048]{1,0:T(8,128)(2,1)S(1)}, bf16[128,2048]{1,0:T(8,128)(2,1)S(1)}, u32[]{:S(2)}, u32[]{:S(2)}) collective-permute-start(bf16[128,2048]{1,0:T(8,128)(2,1)S(1)} %get-tuple-element.39), channel_id=1, source_target_pairs={{0,1},{1,2},{2,3},{3,0},{4,5},{5,6},{6,7},{7,4},{8,9},{9,10},{10,1... | collective-permute-start | bytes 1572872 | tf_op jit(solution)/shard_map/ppermute | solution.py:362
  78.9 12.8 %collective-permute-start.3 = (bf16[128,2048]{1,0:T(8,128)(2,1)S(1)}, bf16[128,2048]{1,0:T(8,128)(2,1)S(1)}, u32[]{:S(2)}, u32[]{:S(2)}) collective-permute-start(bf16[128,2048]{1,0:T(8,128)(2,1)S(1)} %get-tuple-element.40), channel_id=1, source_target_pairs={{0,3},{1,0},{2,1},{3,2},{4,7},{5,4},{6,5},{7,6},{8,11},{9,8},{10,9... | collective-permute-start | bytes 1572872 | tf_op jit(solution)/shard_map/ppermute | solution.py:362
  92.6 9.9 %collective-permute-start.4 = (bf16[64,2048]{1,0:T(8,128)(2,1)S(1)}, bf16[64,2048]{1,0:T(8,128)(2,1)S(1)}, u32[]{:S(2)}, u32[]{:S(2)}) collective-permute-start(bf16[64,2048]{1,0:T(8,128)(2,1)S(1)} %get-tuple-element.41.refs_0_), channel_id=1, source_target_pairs={{0,1},{1,2},{2,3},{3,0},{4,5},{5,6},{6,7},{7,4},{8,9},{9,10},{10,1... | collective-permute-start | bytes 786440 | tf_op jit(solution)/shard_map/ppermute | solution.py:362
  93.8 9.2 %collective-permute-start.6 = (bf16[64,2048]{1,0:T(8,128)(2,1)S(1)}, bf16[64,2048]{1,0:T(8,128)(2,1)S(1)}, u32[]{:S(2)}, u32[]{:S(2)}) collective-permute-start(bf16[64,2048]{1,0:T(8,128)(2,1)S(1)} %get-tuple-element.42.refs_1_), channel_id=1, source_target_pairs={{0,3},{1,0},{2,1},{3,2},{4,7},{5,4},{6,5},{7,6},{8,11},{9,8},{10,9... | collective-permute-start | bytes 786440 | tf_op jit(solution)/shard_map/ppermute | solution.py:362
  95.9 12.3 %collective-permute-start.9 = (bf16[64,2048]{1,0:T(8,128)(2,1)S(1)}, bf16[64,2048]{1,0:T(8,128)(2,1)S(1)}, u32[]{:S(2)}, u32[]{:S(2)}) collective-permute-start(bf16[64,2048]{1,0:T(8,128)(2,1)S(1)} %get-tuple-element.41.refs_0_), channel_id=1, source_target_pairs={{0,3},{1,0},{2,1},{3,2},{4,7},{5,4},{6,5},{7,6},{8,11},{9,8},{10,9... | collective-permute-start | bytes 786440 | tf_op jit(solution)/shard_map/ppermute | solution.py:362
  97.7 10.6 %collective-permute-start.8 = (bf16[64,2048]{1,0:T(8,128)(2,1)S(1)}, bf16[64,2048]{1,0:T(8,128)(2,1)S(1)}, u32[]{:S(2)}, u32[]{:S(2)}) collective-permute-start(bf16[64,2048]{1,0:T(8,128)(2,1)S(1)} %get-tuple-element.42.refs_1_), channel_id=1, source_target_pairs={{0,1},{1,2},{2,3},{3,0},{4,5},{5,6},{6,7},{7,4},{8,9},{9,10},{10,1... | collective-permute-start | bytes 786440 | tf_op jit(solution)/shard_map/ppermute | solution.py:362
  102.5 9.5 %collective-permute-start.5 = (bf16[64,2048]{1,0:T(8,128)(2,1)S(1)}, bf16[64,2048]{1,0:T(8,128)(2,1)S(1)}, u32[]{:S(2)}, u32[]{:S(2)}) collective-permute-start(bf16[64,2048]{1,0:T(8,128)(2,1)S(1)} %collective-permute-done.4.refs_4_), channel_id=1, source_target_pairs={{0,1},{1,2},{2,3},{3,0},{4,5},{5,6},{6,7},{7,4},{8,9},{9,10},{10,1... | collective-permute-start | bytes 786440 | tf_op jit(solution)/shard_map/ppermute | solution.py:362
  103.0 9.0 %collective-permute-start.7 = (bf16[64,2048]{1,0:T(8,128)(2,1)S(1)}, bf16[64,2048]{1,0:T(8,128)(2,1)S(1)}, u32[]{:S(2)}, u32[]{:S(2)}) collective-permute-start(bf16[64,2048]{1,0:T(8,128)(2,1)S(1)} %collective-permute-done.6.refs_7_), channel_id=1, source_target_pairs={{0,3},{1,0},{2,1},{3,2},{4,7},{5,4},{6,5},{7,6},{8,11},{9,8},{10,9... | collective-permute-start | bytes 786440 | tf_op jit(solution)/shard_map/ppermute | solution.py:362
  123.2 24.5 %copy-start.12 = (f32[2048]{0:T(1024)S(1)}, f32[2048]{0:T(1024)}, u32[]{:S(2)}) copy-start(f32[2048]{0:T(1024)} %param.37) | copy-start | bytes 24580
  123.2 9.7 %collective-permute-start.10 = (bf16[1024,128]{1,0:T(8,128)(2,1)S(1)}, bf16[1024,128]{1,0:T(8,128)(2,1)S(1)}, u32[]{:S(2)}, u32[]{:S(2)}) collective-permute-start(bf16[1024,128]{1,0:T(8,128)(2,1)S(1)} %get-tuple-element.48), channel_id=1, source_target_pairs={{0,1},{1,2},{2,3},{3,0},{4,5},{5,6},{6,7},{7,4},{8,9},{9,10},{10,1... | collective-permute-start | bytes 786440 | tf_op jit(solution)/shard_map/ppermute | solution.py:362
  124.7 8.3 %collective-permute-start.11 = (bf16[1024,128]{1,0:T(8,128)(2,1)S(1)}, bf16[1024,128]{1,0:T(8,128)(2,1)S(1)}, u32[]{:S(2)}, u32[]{:S(2)}) collective-permute-start(bf16[1024,128]{1,0:T(8,128)(2,1)S(1)} %get-tuple-element.49), channel_id=1, source_target_pairs={{0,3},{1,0},{2,1},{3,2},{4,7},{5,4},{6,5},{7,6},{8,11},{9,8},{10,9... | collective-permute-start | bytes 786440 | tf_op jit(solution)/shard_map/ppermute | solution.py:362
  133.2 14.5 %collective-permute-start.12 = (bf16[2048,128]{1,0:T(8,128)(2,1)S(1)}, bf16[2048,128]{1,0:T(8,128)(2,1)S(1)}, u32[]{:S(2)}, u32[]{:S(2)}) collective-permute-start(bf16[2048,128]{1,0:T(8,128)(2,1)S(1)} %get-tuple-element.50), channel_id=1, source_target_pairs={{0,1},{1,2},{2,3},{3,0},{4,5},{5,6},{6,7},{7,4},{8,9},{9,10},{10,1... | collective-permute-start | bytes 1572872 | tf_op jit(solution)/shard_map/ppermute | solution.py:362
  134.7 13.0 %collective-permute-start.13 = (bf16[2048,128]{1,0:T(8,128)(2,1)S(1)}, bf16[2048,128]{1,0:T(8,128)(2,1)S(1)}, u32[]{:S(2)}, u32[]{:S(2)}) collective-permute-start(bf16[2048,128]{1,0:T(8,128)(2,1)S(1)} %get-tuple-element.51), channel_id=1, source_target_pairs={{0,3},{1,0},{2,1},{3,2},{4,7},{5,4},{6,5},{7,6},{8,11},{9,8},{10,9... | collective-permute-start | bytes 1572872 | tf_op jit(solution)/shard_map/ppermute | solution.py:362
  (4 other events, 3.2 us)
Sparse Core Ops, SparseCore 0:
  10.1 103.1 all-gather.1

commit v4 on v3

--- a/solution.py
+++ b/solution.py
@@ -106,14 +106,17 @@
 
 
 def states_kernel(
-    _, __, wk_ref, wv_ref, nk_ref, nv_ref, wd_ref, nd_ref, inside_ref, start_ref, *refs, staged,
+    index_ref, _, wk_ref, wv_ref, nk_ref, nv_ref, wd_ref, nd_ref, inside_ref, start_ref, *refs, staged,
 ):
     sources, refs = refs[:staged], refs[staged:]
     before_ref, earlier_ref, message_ref = refs[:3]
     targets, refs = refs[3 : 3 + staged], refs[3 + staged :]
     rows_ref, state_ref, decay_ref, sems = refs
     span = pl.program_id(0)
-    copies = [pltpu.make_async_copy(a, b, sems.at[k]) for k, (a, b) in enumerate(zip(sources, targets))]
+    copies = [
+        pltpu.make_async_copy(a.at[pl.ds(index_ref[0], 1)] if k == 0 else a, b, sems.at[k])
+        for k, (a, b) in enumerate(zip(sources, targets))
+    ]
 
     @pl.when(span == 0)
     def _():
@@ -278,14 +281,41 @@
         high_ref[...] = normed
 
 
-def result_kernel(own_ref, below_ref, above_ref, updated_ref, gain_ref, out_ref):
-    lowered = own_ref[...].astype(F32) + below_ref[...].astype(F32) + above_ref[...].astype(F32)
-    out_ref[...] = (updated_ref[...].astype(F32) + rms(lowered.T, gain_ref[...])).astype(BF16)
+def tail_join_kernel(plus_ref, minus_ref, from_below_ref, from_above_ref, plus_out_ref, minus_out_ref):
+    plus_out_ref[...] = (plus_ref[...].astype(F32) + from_below_ref[...].astype(F32)).astype(BF16)
+    minus_out_ref[...] = (minus_ref[...].astype(F32) + from_above_ref[...].astype(F32)).astype(BF16)
+
+
+def result_kernel(
+    own_ref, below_low_ref, below_high_ref, above_low_ref, above_high_ref,
+    updated_ref, gain_ref, out_ref,
+):
+    half = below_low_ref.shape[0]
+    lowered = [
+        own_ref[part].astype(F32) + below[...].astype(F32) + above[...].astype(F32)
+        for part, below, above in (
+            (slice(0, half), below_low_ref, above_low_ref),
+            (slice(half, 2 * half), below_high_ref, above_high_ref),
+        )
+    ]
+    lowered = jnp.concatenate(lowered, axis=0).T
+    out_ref[...] = (updated_ref[...].astype(F32) + rms(lowered, gain_ref[...])).astype(BF16)
+
+
+def up_block(x_ref, up_ref, at, block):
+    weight = up_ref[:, :, pl.ds(at, block)].reshape(-1, block)
+    rectified = jnp.maximum(mm(x_ref[...], weight), 0.0)
+    return (rectified * rectified).astype(BF16).T
+
+
+def down_block(down_ref, hidden_ref, k, group):
+    weight = down_ref[pl.ds(k * group, group)].reshape(-1, hidden_ref.shape[0])
+    return mm(weight, hidden_ref[...]).astype(BF16)
 
 
 def far_mixer_kernel(*refs, ups, downs):
-    halves, refs = refs[:8], refs[8:]
-    both_ref, hidden_ref, out_ref, low_ref, high_ref, down_ref, up_ref, x_ref, now_ref, sems = refs
+    halves, refs = refs[:4], refs[4:]
+    both_ref, up_ref, down_ref, out_ref, low_ref, high_ref, x_ref, hidden_ref, sems = refs
     devices, share, units = up_ref.shape
     half = halves[0].shape[0]
     rows = 2 * half
@@ -316,16 +346,11 @@
     def _(k):
         up_copy(k).wait()
         at = pl.multiple_of(k * block, block)
-        weight = up_ref[:, :, pl.ds(at, block)].reshape(devices * share, block)
-        rectified = jnp.maximum(mm(x_ref[...], weight), 0.0)
-        hidden = (rectified * rectified).astype(BF16).T
-        hidden_ref[pl.ds(at, block), :] = hidden[:, 2 * rows :]
-        now_ref[pl.ds(at, block), :] = hidden[:, : 2 * rows]
+        hidden_ref[pl.ds(at, block), :] = up_block(x_ref, up_ref, at, block)
 
     def lower(k, far_ref, base):
         down_copy(k).wait()
-        weight = down_ref[pl.ds(k * group, group)].reshape(lines, units)
-        lowered = mm(weight, now_ref[...]).astype(BF16)
+        lowered = down_block(down_ref, hidden_ref, k, group)
         out_ref[pl.ds(pl.multiple_of(k * lines, lines), lines), :] = lowered[:, :rows]
         far_ref[pl.ds(pl.multiple_of((k - base) * lines, lines), lines), :] = lowered[:, rows:]
 
@@ -338,23 +363,34 @@
         lower(k, high_ref, downs // 2)
 
 
-def near_mixer_kernel(hidden_ref, down_ref, minus_ref, plus_ref, *, parts):
-    devices, share, units = down_ref.shape
-    group = devices // parts
+def near_mixer_kernel(*refs, ups, downs):
+    halves, refs = refs[:4], refs[4:]
+    up_ref, down_ref, minus_low_ref, minus_high_ref, plus_low_ref, plus_high_ref, x_ref, hidden_ref = refs
+    devices, share, units = up_ref.shape
+    half = halves[0].shape[0]
+    rows = 2 * half
+    block = units // ups
+    group = devices // downs
     lines = group * share
-    rows = minus_ref.shape[1]
-
-    @pl.loop(0, parts)
+    for k, ref in enumerate(halves):
+        x_ref[k * half : (k + 1) * half] = ref[...]
+
+    @pl.loop(0, ups)
     def _(k):
-        weight = down_ref[pl.ds(k * group, group)].reshape(lines, units)
-        lowered = mm(weight, hidden_ref[...]).astype(BF16)
-        at = pl.multiple_of(k * lines, lines)
-        minus_ref[pl.ds(at, lines), :] = lowered[:, :rows]
-        plus_ref[pl.ds(at, lines), :] = lowered[:, rows:]
+        at = pl.multiple_of(k * block, block)
+        hidden_ref[pl.ds(at, block), :] = up_block(x_ref, up_ref, at, block)
+
+    for first, minus_ref, plus_ref in (
+        (0, minus_low_ref, plus_low_ref), (downs // 2, minus_high_ref, plus_high_ref)
+    ):
+        for k in range(downs // 2):
+            lowered = down_block(down_ref, hidden_ref, first + k, group)
+            at = slice(k * lines, (k + 1) * lines)
+            minus_ref[at, :] = lowered[:, :rows]
+            plus_ref[at, :] = lowered[:, rows:]
 
 
 SMALL = pltpu.CompilerParams(vmem_limit_bytes=16 * 1024 * 1024)
-LARGE = pltpu.CompilerParams(vmem_limit_bytes=32 * 1024 * 1024)
 
 
 def shifted(array, axis, by):
@@ -427,14 +463,18 @@
         )
 
     wide_block, narrow_block, decay_blocks, state_blocks = span_blocks(lambda s, i, t: s)
-    staged = (wide_gate, narrow_query, narrow_value, narrow_gate, narrow_out)
+    staged = (
+        starts, inside, wide_decay, narrow_decay, wide_query, wide_key, wide_value, wide_gate,
+        narrow_query, narrow_key, narrow_value, narrow_gate, wide_out, narrow_out,
+    )
     before, earlier, message, *held = pl.pallas_call(
         functools.partial(states_kernel, staged=len(staged)),
         out_shape=(
             jax.ShapeDtypeStruct((SPANS, 512, LANES), F32),
             jax.ShapeDtypeStruct((SPANS, 8, LANES), F32),
             jax.ShapeDtypeStruct((devices, 16, LANES), BF16),
-            *(pltpu.VMEM(x.shape, x.dtype) for x in staged),
+            pltpu.VMEM((1, *starts.shape[1:]), F32),
+            *(pltpu.VMEM(x.shape, x.dtype) for x in staged[1:]),
         ),
         grid_spec=pltpu.PrefetchScalarGridSpec(
             num_scalar_prefetch=2,
@@ -468,7 +508,6 @@
             )
         ),
     )
-    gate_held, query_held, value_held, narrow_gate_held, out_held = held
 
     arrived = lax.all_to_all(message, SP, 0, 0, tiled=True)
     prefixes = pl.pallas_call(
@@ -490,7 +529,8 @@
                 grid=(count,),
                 in_specs=[
                     wide, wide, wide, wide, narrow, narrow, narrow, narrow,
-                    *decays, *table_blocks, *states,
+                    *decays, table_blocks[0],
+                    pl.BlockSpec((1, 4 * SPANS, LANES), lambda s, i, t: (0, 0, 0)), *states,
                     pl.BlockSpec((512, LANES), lambda s, i, t: (0, 0)),
                     pl.BlockSpec((384, width), lambda s, i, t: (0, 0)),
                     pl.BlockSpec((128, width), lambda s, i, t: (0, 0)),
@@ -506,9 +546,7 @@
                 transcendentals=150_000 * count,
             ),
         )(
-            *scalars, wide_query, wide_key, wide_value, gate_held,
-            query_held, narrow_key, value_held, narrow_gate_held,
-            wide_decay, narrow_decay, inside, starts, before, earlier, prefix, wide_out, out_held,
+            *scalars, *held[4:12], held[2], held[3], held[1], held[0], before, earlier, prefix, *held[12:],
         )
 
     half = rows // 2
@@ -544,51 +582,55 @@
 
     ups, downs = 4, 4
     whole = pl.BlockSpec(memory_space=pltpu.VMEM)
+    turned = pltpu.VMEM((width, rows), BF16)
     turned_half = pltpu.VMEM((width // 2, rows), BF16)
-    hidden, own, low, high, down = pl.pallas_call(
+    weights = pltpu.VMEM((devices, share, units), BF16)
+    scratch = [pltpu.VMEM((2 * rows, width), BF16), pltpu.VMEM((units, 2 * rows), BF16)]
+    up, down, own, low, high = pl.pallas_call(
         functools.partial(far_mixer_kernel, ups=ups, downs=downs),
-        out_shape=(
-            pltpu.VMEM((units, 2 * rows), BF16),
-            pltpu.VMEM((width, rows), BF16),
-            turned_half,
-            turned_half,
-            pltpu.VMEM((devices, share, units), BF16),
-        ),
-        in_specs=[*([whole] * 8), pl.BlockSpec(memory_space=pltpu.HBM)],
+        out_shape=(weights, weights, turned, turned_half, turned_half),
+        in_specs=[*([whole] * 4), pl.BlockSpec(memory_space=pltpu.HBM)],
         out_specs=[whole] * 5,
-        scratch_shapes=[
-            pltpu.VMEM((devices, share, units), BF16),
-            pltpu.VMEM((4 * rows, width), BF16),
-            pltpu.VMEM((units, 2 * rows), BF16),
-            pltpu.SemaphoreType.DMA((ups + downs,)),
-        ],
-        compiler_params=LARGE,
+        scratch_shapes=[*scratch, pltpu.SemaphoreType.DMA((ups + downs,))],
+        compiler_params=SMALL,
         name="mixer_far",
         cost_estimate=pl.CostEstimate(
-            flops=12 * rows * width * units, bytes_accessed=20_000_000, transcendentals=0
+            flops=8 * rows * width * units, bytes_accessed=20_000_000, transcendentals=0
         ),
-    )(low, high, far_low, far_high, below_low, below_high, above_low, above_high, both)
+    )(low, high, far_low, far_high, pltpu.with_memory_space_constraint(both, pltpu.HBM))
     low, high = shifted(low, "tp", 1), shifted(high, "tp", -1)
-    minus, plus = pl.pallas_call(
-        functools.partial(near_mixer_kernel, parts=2),
-        out_shape=(jax.ShapeDtypeStruct((width, rows), BF16),) * 2,
-        in_specs=[whole] * 2,
-        out_specs=[whole] * 2,
+    minus_low, minus_high, plus_low, plus_high = pl.pallas_call(
+        functools.partial(near_mixer_kernel, ups=2, downs=2),
+        out_shape=(turned_half,) * 4,
+        in_specs=[whole] * 6,
+        out_specs=[whole] * 4,
+        scratch_shapes=scratch,
         compiler_params=SMALL,
         name="mixer_near",
         cost_estimate=pl.CostEstimate(
-            flops=4 * rows * width * units, bytes_accessed=2_000_000, transcendentals=0
+            flops=8 * rows * width * units, bytes_accessed=2_000_000, transcendentals=0
         ),
-    )(hidden, down)
-    minus, plus = joined(minus, plus, low, high)
-    below, above = shifted(plus, "tp", 1), shifted(minus, "tp", -1)
+    )(below_low, below_high, above_low, above_high, up, down)
+    below_high, above_low = shifted(plus_high, "tp", 1), shifted(minus_low, "tp", -1)
+    plus_low, minus_high = pl.pallas_call(
+        tail_join_kernel,
+        out_shape=(turned_half,) * 2,
+        in_specs=[whole] * 4,
+        out_specs=[whole] * 2,
+        compiler_params=SMALL,
+        name="tail_join",
+        cost_estimate=pl.CostEstimate(flops=500_000, bytes_accessed=1_500_000, transcendentals=0),
+    )(plus_low, minus_high, low, high)
+    below_low, above_high = shifted(plus_low, "tp", 1), shifted(minus_high, "tp", -1)
     return pl.pallas_call(
         result_kernel,
         out_shape=jax.ShapeDtypeStruct((rows, width), BF16),
         compiler_params=SMALL,
         name="result",
         cost_estimate=pl.CostEstimate(flops=4_000_000, bytes_accessed=3_500_000, transcendentals=300),
-    )(own, below, above, updated, gain_mlp.reshape(1, width))
+    )(
+        own, below_low, below_high, above_low, above_high, updated, gain_mlp.reshape(1, width)
+    )
 
 
 def solution(mesh):

time: 158 us -> 155 us (0.981)
  local copies, waits for them, and re-layouts: 8.69 us -> 0.02 us
  starting transfers between devices: 21.9 us -> 26.3 us
    all_gather x1, waiting for transfers between devices: 1.37 us -> 11.5 us  [local(): lax.all_gather(jnp.concatenate([up_weight, down_weight.T], axis=0), SP, a...]
    ppermute x14 -> x16, waiting for transfers between devices: 37.6 us -> 28 us  [shifted(): lax.ppermute(array, axis, [(k, (k + by) % size) for k in range(size)])]
    unnamed x26 -> x8, local copies, waits for them, and re-layouts: 8.69 us -> 0.02 us
    ppermute x14 -> x16, starting transfers between devices: 21.9 us -> 26.3 us  [shifted(): lax.ppermute(array, axis, [(k, (k + by) % size) for k in range(size)])]
    pallas_call x1 -> x2, Pallas kernels: 2.49 us -> 5.17 us  [the longest x1 5.05 us: local(): pl.pallas_call(functools.partial(near_mixer_kernel, ups=2, downs=2), out_...]
    pallas_call x1, Pallas kernels: 9.89 us -> 7.73 us  [local(): pl.pallas_call(functools.partial(far_mixer_kernel, ups=ups, downs=downs),...]
  transfers between devices with their start and end apart: 15 -> 17, of which waited for: 9 -> 8; matrix products, arithmetic and copies ran while one was open for 0% -> 0% of each run, Pallas kernels for 11% -> 18%
where the time goes in v4:
time: 155 us; the launch traced here: 153 us
  blocking collectives  42.6 us (27%)
  waiting for transfers between devices  39.5 us (25%)
  Pallas kernels  29.1 us (19%)
  starting transfers between devices  26.3 us (17%)
  between operations  13.5 us (9%)
  other arithmetic  1.69 us (1%)
    ppermute x16, waiting for transfers between devices, shifted(): lax.ppermute(array, axis, [(k, (k + by) % size) for k in range(size)])  28 us
    ppermute x16, starting transfers between devices, shifted(): lax.ppermute(array, axis, [(k, (k + by) % size) for k in range(size)])  26.3 us
    all_to_all x1, blocking collectives, local(): arrived = lax.all_to_all(message, SP, 0, 0, tiled=True)  25.6 us
    all_to_all x1, blocking collectives, local(): prefix = lax.all_to_all(prefixes, SP, 0, 0, tiled=True).reshape(512, LANES)  16.9 us
    all_gather x1, waiting for transfers between devices, local(): lax.all_gather(jnp.concatenate([up_weight, down_weight.T], axis=0), SP, a...  11.5 us
    pallas_call x1, Pallas kernels, local(): pl.pallas_call(functools.partial(far_mixer_kernel, ups=ups, downs=downs),...  7.73 us
    pallas_call x2, Pallas kernels, finish(): pl.pallas_call(functools.partial(finish_kernel, first=first), out_shape=o...  7.43 us
    pallas_call x1, Pallas kernels, local(): pl.pallas_call(functools.partial(states_kernel, staged=len(staged)), out_...  6.18 us
  transfers between devices with their start and end apart: 17, of which 8 were waited for; matrix products, arithmetic and copies ran while one was open for 0% of the time, Pallas kernels for 18%

profile of v4, /device:TPU:32, one launch (start us, length us, event | category | flops | bytes accessed | tf_op | source)
XLA Modules:
  0.0 152.8 jit_solution(3960897548799182347)
XLA Ops:
  6.5 1.7 %pad_maximum_fusion = bf16[64,2048]{1,0:T(8,128)(2,1)} fusion(bf16[32,2048]{1,0:T(8,128)(2,1)} %bitcast.14, bf16[32,2048]{1,0:T(8,128)(2,1)} %param.33), kind=kLoop, calls=%fused_computation | loop fusion | flops 524288 | bytes 524288 | tf_op jit(solution)/shard_map/concatenate | solution.py:438
  8.3 6.2 %states.1 = (f32[4,512,128]{2,1,0:T(8,128)S(1)}, f32[4,8,128]{2,1,0:T(8,128)S(1)}, bf16[64,16,128]{2,1,0:T(8,128)(2,1)S(1)}, f32[1,16,128]{2,1,0:T(8,128)S(1)}, ...) custom-call(s32[1]{0:T(128)} %bitcast.index_ref, ...), custom_call_target="tpu_custom_call" | custom-call | flops 60000000 | bytes 2500000 | tf_op jit(solution)/shard_map/states/pallas_call | solution.py:470
  14.4 25.6 %all_to_all.10.message_ref = bf16[64,16,128]{2,1,0:T(8,128)(2,1)S(1)} all-to-all(bf16[64,16,128]{2,1,0:T(8,128)(2,1)S(1)} %get-tuple-element.54), channel_id=1, replica_groups=mesh['sp_0'=8,'sp_1'=4,'sp_2'=2,'tp'=4] {'sp_0','sp_1','sp_2'}, dimensions={0} | all-to-all | bytes 524288 | tf_op jit(solution)/shard_map/all_to_all | solution.py:512
  40.2 16.9 %all_to_all.11 = bf16[64,8,128]{2,1,0:T(8,128)(2,1)S(1)} all-to-all(bf16[64,8,128]{2,1,0:T(8,128)(2,1)S(1)} %prefix.1), channel_id=1, replica_groups=mesh['sp_0'=8,'sp_1'=4,'sp_2'=2,'tp'=4] {'sp_0','sp_1','sp_2'}, dimensions={0} | all-to-all | bytes 262144 | tf_op jit(solution)/shard_map/all_to_all | solution.py:520
  57.2 1.9 %finish_far.1 = (bf16[64,2048]{1,0:T(8,128)(2,1)S(1)}, bf16[64,2048]{1,0:T(8,128)(2,1)S(1)}) custom-call(s32[1]{0:T(128)} %bitcast.index_ref, s32[1]{0:T(128)} %bitcast.1._.turn_ref, bf16[512,384]{1,0:T(8,128)(2,1)S(1)} %get-tuple-element.40.wq_ref, bf16[512,384]{1,0:T(8,128)(2,1)S(1)} %get-tuple-element.41.wk_ref, ...), custom_call_target="tpu_custom_call" | custom-call | flops 350000000 | bytes 4500000 | tf_op jit(solution)/shard_map/finish_far/pallas_call | solution.py:524
  59.0 1.6 %collective-permute-start = (bf16[64,2048]{1,0:T(8,128)(2,1)S(1)}, bf16[64,2048]{1,0:T(8,128)(2,1)S(1)}, u32[]{:S(2)}, u32[]{:S(2)}) collective-permute-start(bf16[64,2048]{1,0:T(8,128)(2,1)S(1)} %get-tuple-element.57), channel_id=1, source_target_pairs={{0,1},{1,2},{2,3},{3,0},{4,5},{5,6},{6,7},{7,4},{8,9},{9,10},{10,1... | collective-permute-start | bytes 786440 | tf_op jit(solution)/shard_map/ppermute | solution.py:398
  60.6 1.7 %collective-permute-start.1 = (bf16[64,2048]{1,0:T(8,128)(2,1)S(1)}, bf16[64,2048]{1,0:T(8,128)(2,1)S(1)}, u32[]{:S(2)}, u32[]{:S(2)}) collective-permute-start(bf16[64,2048]{1,0:T(8,128)(2,1)S(1)} %get-tuple-element.58), channel_id=1, source_target_pairs={{0,3},{1,0},{2,1},{3,2},{4,7},{5,4},{6,5},{7,6},{8,11},{9,8},{10,9... | collective-permute-start | bytes 786440 | tf_op jit(solution)/shard_map/ppermute | solution.py:398
  62.4 5.6 %finish.1.minus_ref.plus_ref.own_ref = bf16[3,128,2048]{2,1,0:T(8,128)(2,1)S(1)} custom-call(s32[1]{0:T(128)} %bitcast.index_ref, s32[1]{0:T(128)} %bitcast.1._.turn_ref, bf16[512,384]{1,0:T(8,128)(2,1)S(1)} %get-tuple-element.40.wq_ref, bf16[512,384]{1,0:T(8,128)(2,1)S(1)} %get-tuple-element.41.wk_ref, bf16[512,384]{1,0:T(8,128)(2,1)S(1)} %get-tuple-element.42.wv_ref, ...), custom_call_target="tpu_custom_call" | custom-call | flops 1050000000 | bytes 7500000 | tf_op jit(solution)/shard_map/finish/pallas_call | solution.py:524
  70.4 1.9 %collective-permute-start.3 = (bf16[128,2048]{1,0:T(8,128)(2,1)S(1)}, bf16[128,2048]{1,0:T(8,128)(2,1)S(1)}, u32[]{:S(2)}, u32[]{:S(2)}) collective-permute-start(bf16[128,2048]{1,0:T(8,128)(2,1)S(1)} %get-tuple-element.60), channel_id=1, source_target_pairs={{0,3},{1,0},{2,1},{3,2},{4,7},{5,4},{6,5},{7,6},{8,11},{9,8},{10,9... | collective-permute-start | bytes 1572872 | tf_op jit(solution)/shard_map/ppermute | solution.py:398
  72.3 11.0 %collective-permute-done.2.below_ref = bf16[128,2048]{1,0:T(8,128)(2,1)S(1)} collective-permute-done((bf16[128,2048]{1,0:T(8,128)(2,1)S(1)}, bf16[128,2048]{1,0:T(8,128)(2,1)S(1)}, u32[]{:S(2)}, u32[]{:S(2)}) %collective-permute-start.2) | collective-permute-done | bytes 524320 | tf_op jit(solution)/shard_map/ppermute | solution.py:398
  85.2 2.4 %collective-permute-start.6 = (bf16[64,2048]{1,0:T(8,128)(2,1)S(1)}, bf16[64,2048]{1,0:T(8,128)(2,1)S(1)}, u32[]{:S(2)}, u32[]{:S(2)}) collective-permute-start(bf16[64,2048]{1,0:T(8,128)(2,1)S(1)} %get-tuple-element.62.refs_1_), channel_id=1, source_target_pairs={{0,3},{1,0},{2,1},{3,2},{4,7},{5,4},{6,5},{7,6},{8,11},{9,8},{10,9... | collective-permute-start | bytes 786440 | tf_op jit(solution)/shard_map/ppermute | solution.py:398
  87.5 4.6 %collective-permute-done.4.refs_0_ = bf16[64,2048]{1,0:T(8,128)(2,1)S(1)} collective-permute-done((bf16[64,2048]{1,0:T(8,128)(2,1)S(1)}, bf16[64,2048]{1,0:T(8,128)(2,1)S(1)}, u32[]{:S(2)}, u32[]{:S(2)}) %collective-permute-start.4) | collective-permute-done | bytes 262176 | tf_op jit(solution)/shard_map/ppermute | solution.py:398
  92.2 3.2 %collective-permute-start.7 = (bf16[64,2048]{1,0:T(8,128)(2,1)S(1)}, bf16[64,2048]{1,0:T(8,128)(2,1)S(1)}, u32[]{:S(2)}, u32[]{:S(2)}) collective-permute-start(bf16[64,2048]{1,0:T(8,128)(2,1)S(1)} %collective-permute-done.6.refs_3_), channel_id=1, source_target_pairs={{0,3},{1,0},{2,1},{3,2},{4,7},{5,4},{6,5},{7,6},{8,11},{9,8},{10,9... | collective-permute-start | bytes 786440 | tf_op jit(solution)/shard_map/ppermute | solution.py:398
  95.4 3.2 %collective-permute-start.9 = (bf16[64,2048]{1,0:T(8,128)(2,1)S(1)}, bf16[64,2048]{1,0:T(8,128)(2,1)S(1)}, u32[]{:S(2)}, u32[]{:S(2)}) collective-permute-start(bf16[64,2048]{1,0:T(8,128)(2,1)S(1)} %get-tuple-element.61.refs_0_), channel_id=1, source_target_pairs={{0,3},{1,0},{2,1},{3,2},{4,7},{5,4},{6,5},{7,6},{8,11},{9,8},{10,9... | collective-permute-start | bytes 786440 | tf_op jit(solution)/shard_map/ppermute | solution.py:398
  98.6 3.5 %collective-permute-done.5.refs_2_ = bf16[64,2048]{1,0:T(8,128)(2,1)S(1)} collective-permute-done((bf16[64,2048]{1,0:T(8,128)(2,1)S(1)}, bf16[64,2048]{1,0:T(8,128)(2,1)S(1)}, u32[]{:S(2)}, u32[]{:S(2)}) %collective-permute-start.5) | collective-permute-done | bytes 262176 | tf_op jit(solution)/shard_map/ppermute | solution.py:398
  102.1 11.5 %all-gather.2.cloned.1.call-done = bf16[4096,2048]{1,0:T(8,128)(2,1)} async-done(((bf16[64,2048]{1,0:T(8,128)(2,1)}), bf16[4096,2048]{1,0:T(8,128)(2,1)}) %all-gather.2.cloned.1.call-update) | async-done | bytes 16777232 | tf_op jit(solution)/shard_map/all_gather | solution.py:437
  113.6 7.7 %mixer_far.1 = (bf16[64,32,2048]{2,1,0:T(8,128)(2,1)S(1)}, bf16[64,32,2048]{2,1,0:T(8,128)(2,1)S(1)}, bf16[2048,128]{1,0:T(8,128)(2,1)S(1)}, bf16[1024,128]{1,0:T(8,128)(2,1)S(1)}, bf16[1024,128]{1,0:T(8,128)(2,1)S(1)}) custom-call(bf16[64,2048]{1,0:T(8,128)(2,1)S(1)} %get-tuple-element.61.refs_0_, bf16[64,2048]{1,0:T(8,128)(2,1)S(1)} %get-tuple-element.62.refs_1_, ...), custom_call_target="tpu_custom_call" | custom-call | flops 4294967296 | bytes 20000000 | tf_op jit(solution)/shard_map/mixer_far/pallas_call | solution.py:589
  121.3 1.6 %collective-permute-start.10 = (bf16[1024,128]{1,0:T(8,128)(2,1)S(1)}, bf16[1024,128]{1,0:T(8,128)(2,1)S(1)}, u32[]{:S(2)}, u32[]{:S(2)}) collective-permute-start(bf16[1024,128]{1,0:T(8,128)(2,1)S(1)} %get-tuple-element.68), channel_id=1, source_target_pairs={{0,1},{1,2},{2,3},{3,0},{4,5},{5,6},{6,7},{7,4},{8,9},{9,10},{10,1... | collective-permute-start | bytes 786440 | tf_op jit(solution)/shard_map/ppermute | solution.py:398
  122.9 1.8 %collective-permute-start.11 = (bf16[1024,128]{1,0:T(8,128)(2,1)S(1)}, bf16[1024,128]{1,0:T(8,128)(2,1)S(1)}, u32[]{:S(2)}, u32[]{:S(2)}) collective-permute-start(bf16[1024,128]{1,0:T(8,128)(2,1)S(1)} %get-tuple-element.69), channel_id=1, source_target_pairs={{0,3},{1,0},{2,1},{3,2},{4,7},{5,4},{6,5},{7,6},{8,11},{9,8},{10,9... | collective-permute-start | bytes 786440 | tf_op jit(solution)/shard_map/ppermute | solution.py:398
  124.7 5.0 %mixer_near.1 = (bf16[1024,128]{1,0:T(8,128)(2,1)S(1)}, bf16[1024,128]{1,0:T(8,128)(2,1)S(1)}, bf16[1024,128]{1,0:T(8,128)(2,1)S(1)}, bf16[1024,128]{1,0:T(8,128)(2,1)S(1)}) custom-call(bf16[64,2048]{1,0:T(8,128)(2,1)S(1)} %collective-permute-done.4.refs_0_, bf16[64,2048]{1,0:T(8,128)(2,1)S(1)} %collective-permute-done.8.refs_1_, ...), custom_call_target="tpu_custom_call" | custom-call | flops 4294967296 | bytes 2000000 | tf_op jit(solution)/shard_map/mixer_near/pallas_call | solution.py:602
  130.1 3.0 %collective-permute-start.14 = (bf16[1024,128]{1,0:T(8,128)(2,1)S(1)}, bf16[1024,128]{1,0:T(8,128)(2,1)S(1)}, u32[]{:S(2)}, u32[]{:S(2)}) collective-permute-start(bf16[1024,128]{1,0:T(8,128)(2,1)S(1)} %get-tuple-element.72), channel_id=1, source_target_pairs={{0,3},{1,0},{2,1},{3,2},{4,7},{5,4},{6,5},{7,6},{8,11},{9,8},{10,9... | collective-permute-start | bytes 786440 | tf_op jit(solution)/shard_map/ppermute | solution.py:398
  133.3 3.2 %collective-permute-start.15 = (bf16[1024,128]{1,0:T(8,128)(2,1)S(1)}, bf16[1024,128]{1,0:T(8,128)(2,1)S(1)}, u32[]{:S(2)}, u32[]{:S(2)}) collective-permute-start(bf16[1024,128]{1,0:T(8,128)(2,1)S(1)} %get-tuple-element.73), channel_id=1, source_target_pairs={{0,3},{1,0},{2,1},{3,2},{4,7},{5,4},{6,5},{7,6},{8,11},{9,8},{10,9... | collective-permute-start | bytes 786440 | tf_op jit(solution)/shard_map/ppermute | solution.py:398
  136.5 3.7 %collective-permute-done.13.below_high_ref = bf16[1024,128]{1,0:T(8,128)(2,1)S(1)} collective-permute-done((bf16[1024,128]{1,0:T(8,128)(2,1)S(1)}, bf16[1024,128]{1,0:T(8,128)(2,1)S(1)}, u32[]{:S(2)}, u32[]{:S(2)}) %collective-permute-start.13) | collective-permute-done | bytes 262176 | tf_op jit(solution)/shard_map/ppermute | solution.py:398
  140.2 4.3 %collective-permute-done.12.below_low_ref = bf16[1024,128]{1,0:T(8,128)(2,1)S(1)} collective-permute-done((bf16[1024,128]{1,0:T(8,128)(2,1)S(1)}, bf16[1024,128]{1,0:T(8,128)(2,1)S(1)}, u32[]{:S(2)}, u32[]{:S(2)}) %collective-permute-start.12) | collective-permute-done | bytes 262176 | tf_op jit(solution)/shard_map/ppermute | solution.py:398
  (32 shorter events, 6.4 us)
Async XLA Ops:
  6.5 107.1 %all-gather.2.cloned.1.call-start = ((), (), s32[]{:S(2)}) async-start(), calls=%async_computation.2 | async-start | bytes 17039360 | tf_op jit(solution)/shard_map/all_gather | solution.py:437
  40.2 43.1 %copy-start = (bf16[128,2048]{1,0:T(8,128)(2,1)S(1)}, bf16[128,2048]{1,0:T(8,128)(2,1)}, u32[]{:S(2)}) copy-start(bf16[128,2048]{1,0:T(8,128)(2,1)} %residual_ref.1) | copy-start | bytes 1572868
  40.2 43.1 %copy-start.1 = (f32[2048]{0:T(1024)S(1)}, f32[2048]{0:T(1024)}, u32[]{:S(2)}) copy-start(f32[2048]{0:T(1024)} %param.35) | copy-start | bytes 24580
  40.2 43.1 %copy-start.2 = (f32[2048]{0:T(1024)S(1)}, f32[2048]{0:T(1024)}, u32[]{:S(2)}) copy-start(f32[2048]{0:T(1024)} %param.36) | copy-start | bytes 24580
  59.0 9.7 %collective-permute-start = (bf16[64,2048]{1,0:T(8,128)(2,1)S(1)}, bf16[64,2048]{1,0:T(8,128)(2,1)S(1)}, u32[]{:S(2)}, u32[]{:S(2)}) collective-permute-start(bf16[64,2048]{1,0:T(8,128)(2,1)S(1)} %get-tuple-element.57), channel_id=1, source_target_pairs={{0,1},{1,2},{2,3},{3,0},{4,5},{5,6},{6,7},{7,4},{8,9},{9,10},{10,1... | collective-permute-start | bytes 786440 | tf_op jit(solution)/shard_map/ppermute | solution.py:398
  60.6 8.1 %collective-permute-start.1 = (bf16[64,2048]{1,0:T(8,128)(2,1)S(1)}, bf16[64,2048]{1,0:T(8,128)(2,1)S(1)}, u32[]{:S(2)}, u32[]{:S(2)}) collective-permute-start(bf16[64,2048]{1,0:T(8,128)(2,1)S(1)} %get-tuple-element.58), channel_id=1, source_target_pairs={{0,3},{1,0},{2,1},{3,2},{4,7},{5,4},{6,5},{7,6},{8,11},{9,8},{10,9... | collective-permute-start | bytes 786440 | tf_op jit(solution)/shard_map/ppermute | solution.py:398
  69.0 14.3 %collective-permute-start.2 = (bf16[128,2048]{1,0:T(8,128)(2,1)S(1)}, bf16[128,2048]{1,0:T(8,128)(2,1)S(1)}, u32[]{:S(2)}, u32[]{:S(2)}) collective-permute-start(bf16[128,2048]{1,0:T(8,128)(2,1)S(1)} %get-tuple-element.59), channel_id=1, source_target_pairs={{0,1},{1,2},{2,3},{3,0},{4,5},{5,6},{6,7},{7,4},{8,9},{9,10},{10,1... | collective-permute-start | bytes 1572872 | tf_op jit(solution)/shard_map/ppermute | solution.py:398
  70.4 12.9 %collective-permute-start.3 = (bf16[128,2048]{1,0:T(8,128)(2,1)S(1)}, bf16[128,2048]{1,0:T(8,128)(2,1)S(1)}, u32[]{:S(2)}, u32[]{:S(2)}) collective-permute-start(bf16[128,2048]{1,0:T(8,128)(2,1)S(1)} %get-tuple-element.60), channel_id=1, source_target_pairs={{0,3},{1,0},{2,1},{3,2},{4,7},{5,4},{6,5},{7,6},{8,11},{9,8},{10,9... | collective-permute-start | bytes 1572872 | tf_op jit(solution)/shard_map/ppermute | solution.py:398
  84.2 8.0 %collective-permute-start.4 = (bf16[64,2048]{1,0:T(8,128)(2,1)S(1)}, bf16[64,2048]{1,0:T(8,128)(2,1)S(1)}, u32[]{:S(2)}, u32[]{:S(2)}) collective-permute-start(bf16[64,2048]{1,0:T(8,128)(2,1)S(1)} %get-tuple-element.61.refs_0_), channel_id=1, source_target_pairs={{0,1},{1,2},{2,3},{3,0},{4,5},{5,6},{6,7},{7,4},{8,9},{9,10},{10,1... | collective-permute-start | bytes 786440 | tf_op jit(solution)/shard_map/ppermute | solution.py:398
  85.2 7.0 %collective-permute-start.6 = (bf16[64,2048]{1,0:T(8,128)(2,1)S(1)}, bf16[64,2048]{1,0:T(8,128)(2,1)S(1)}, u32[]{:S(2)}, u32[]{:S(2)}) collective-permute-start(bf16[64,2048]{1,0:T(8,128)(2,1)S(1)} %get-tuple-element.62.refs_1_), channel_id=1, source_target_pairs={{0,3},{1,0},{2,1},{3,2},{4,7},{5,4},{6,5},{7,6},{8,11},{9,8},{10,9... | collective-permute-start | bytes 786440 | tf_op jit(solution)/shard_map/ppermute | solution.py:398
  92.2 9.9 %collective-permute-start.5 = (bf16[64,2048]{1,0:T(8,128)(2,1)S(1)}, bf16[64,2048]{1,0:T(8,128)(2,1)S(1)}, u32[]{:S(2)}, u32[]{:S(2)}) collective-permute-start(bf16[64,2048]{1,0:T(8,128)(2,1)S(1)} %collective-permute-done.4.refs_0_), channel_id=1, source_target_pairs={{0,1},{1,2},{2,3},{3,0},{4,5},{5,6},{6,7},{7,4},{8,9},{9,10},{10,1... | collective-permute-start | bytes 786440 | tf_op jit(solution)/shard_map/ppermute | solution.py:398
  92.2 9.9 %collective-permute-start.7 = (bf16[64,2048]{1,0:T(8,128)(2,1)S(1)}, bf16[64,2048]{1,0:T(8,128)(2,1)S(1)}, u32[]{:S(2)}, u32[]{:S(2)}) collective-permute-start(bf16[64,2048]{1,0:T(8,128)(2,1)S(1)} %collective-permute-done.6.refs_3_), channel_id=1, source_target_pairs={{0,3},{1,0},{2,1},{3,2},{4,7},{5,4},{6,5},{7,6},{8,11},{9,8},{10,9... | collective-permute-start | bytes 786440 | tf_op jit(solution)/shard_map/ppermute | solution.py:398
  95.4 29.3 %collective-permute-start.8 = (bf16[64,2048]{1,0:T(8,128)(2,1)S(1)}, bf16[64,2048]{1,0:T(8,128)(2,1)S(1)}, u32[]{:S(2)}, u32[]{:S(2)}) collective-permute-start(bf16[64,2048]{1,0:T(8,128)(2,1)S(1)} %get-tuple-element.62.refs_1_), channel_id=1, source_target_pairs={{0,1},{1,2},{2,3},{3,0},{4,5},{5,6},{6,7},{7,4},{8,9},{9,10},{10,1... | collective-permute-start | bytes 786440 | tf_op jit(solution)/shard_map/ppermute | solution.py:398
  95.4 29.3 %collective-permute-start.9 = (bf16[64,2048]{1,0:T(8,128)(2,1)S(1)}, bf16[64,2048]{1,0:T(8,128)(2,1)S(1)}, u32[]{:S(2)}, u32[]{:S(2)}) collective-permute-start(bf16[64,2048]{1,0:T(8,128)(2,1)S(1)} %get-tuple-element.61.refs_0_), channel_id=1, source_target_pairs={{0,3},{1,0},{2,1},{3,2},{4,7},{5,4},{6,5},{7,6},{8,11},{9,8},{10,9... | collective-permute-start | bytes 786440 | tf_op jit(solution)/shard_map/ppermute | solution.py:398
  121.3 11.7 %collective-permute-start.10 = (bf16[1024,128]{1,0:T(8,128)(2,1)S(1)}, bf16[1024,128]{1,0:T(8,128)(2,1)S(1)}, u32[]{:S(2)}, u32[]{:S(2)}) collective-permute-start(bf16[1024,128]{1,0:T(8,128)(2,1)S(1)} %get-tuple-element.68), channel_id=1, source_target_pairs={{0,1},{1,2},{2,3},{3,0},{4,5},{5,6},{6,7},{7,4},{8,9},{9,10},{10,1... | collective-permute-start | bytes 786440 | tf_op jit(solution)/shard_map/ppermute | solution.py:398
  122.9 10.1 %collective-permute-start.11 = (bf16[1024,128]{1,0:T(8,128)(2,1)S(1)}, bf16[1024,128]{1,0:T(8,128)(2,1)S(1)}, u32[]{:S(2)}, u32[]{:S(2)}) collective-permute-start(bf16[1024,128]{1,0:T(8,128)(2,1)S(1)} %get-tuple-element.69), channel_id=1, source_target_pairs={{0,3},{1,0},{2,1},{3,2},{4,7},{5,4},{6,5},{7,6},{8,11},{9,8},{10,9... | collective-permute-start | bytes 786440 | tf_op jit(solution)/shard_map/ppermute | solution.py:398
  124.7 19.9 %copy-start.3 = (f32[2048]{0:T(1024)S(1)}, f32[2048]{0:T(1024)}, u32[]{:S(2)}) copy-start(f32[2048]{0:T(1024)} %param.37) | copy-start | bytes 24580
  129.7 10.5 %collective-permute-start.13 = (bf16[1024,128]{1,0:T(8,128)(2,1)S(1)}, bf16[1024,128]{1,0:T(8,128)(2,1)S(1)}, u32[]{:S(2)}, u32[]{:S(2)}) collective-permute-start(bf16[1024,128]{1,0:T(8,128)(2,1)S(1)} %get-tuple-element.71), channel_id=1, source_target_pairs={{0,1},{1,2},{2,3},{3,0},{4,5},{5,6},{6,7},{7,4},{8,9},{9,10},{10,1... | collective-permute-start | bytes 786440 | tf_op jit(solution)/shard_map/ppermute | solution.py:398
  130.1 10.1 %collective-permute-start.14 = (bf16[1024,128]{1,0:T(8,128)(2,1)S(1)}, bf16[1024,128]{1,0:T(8,128)(2,1)S(1)}, u32[]{:S(2)}, u32[]{:S(2)}) collective-permute-start(bf16[1024,128]{1,0:T(8,128)(2,1)S(1)} %get-tuple-element.72), channel_id=1, source_target_pairs={{0,3},{1,0},{2,1},{3,2},{4,7},{5,4},{6,5},{7,6},{8,11},{9,8},{10,9... | collective-permute-start | bytes 786440 | tf_op jit(solution)/shard_map/ppermute | solution.py:398
  133.2 11.4 %collective-permute-start.12 = (bf16[1024,128]{1,0:T(8,128)(2,1)S(1)}, bf16[1024,128]{1,0:T(8,128)(2,1)S(1)}, u32[]{:S(2)}, u32[]{:S(2)}) collective-permute-start(bf16[1024,128]{1,0:T(8,128)(2,1)S(1)} %get-tuple-element.70), channel_id=1, source_target_pairs={{0,1},{1,2},{2,3},{3,0},{4,5},{5,6},{6,7},{7,4},{8,9},{9,10},{10,1... | collective-permute-start | bytes 786440 | tf_op jit(solution)/shard_map/ppermute | solution.py:398
  133.3 11.3 %collective-permute-start.15 = (bf16[1024,128]{1,0:T(8,128)(2,1)S(1)}, bf16[1024,128]{1,0:T(8,128)(2,1)S(1)}, u32[]{:S(2)}, u32[]{:S(2)}) collective-permute-start(bf16[1024,128]{1,0:T(8,128)(2,1)S(1)} %get-tuple-element.73), channel_id=1, source_target_pairs={{0,3},{1,0},{2,1},{3,2},{4,7},{5,4},{6,5},{7,6},{8,11},{9,8},{10,9... | collective-permute-start | bytes 786440 | tf_op jit(solution)/shard_map/ppermute | solution.py:398
Sparse Core Ops, SparseCore 0:
  10.1 103.4 all-gather.1

commit v5 on v4

--- a/solution.py
+++ b/solution.py
@@ -12,6 +12,7 @@
 SPAN = 128
 LANES = 128
 SPANS = 4
+SPAN_PART = 16
 SP = ("sp_0", "sp_1", "sp_2")
 SP_TP = ("sp_0", "sp_1", "sp_2", "tp")
 EPS = 1e-06
@@ -23,37 +24,37 @@
 
 def position_tables(devices):
     lane = np.arange(LANES)
-
-    def inverse(head_dim):
+    inside, upper, lower = [], [], []
+    for head_dim in (128, 64):
         half = head_dim // 2
-        return 10000.0 ** (-2.0 * (lane % half) / head_dim), np.where(
-            lane % head_dim < half, -1.0, 1.0
+        rate = 10000.0 ** (-2.0 * (lane % half) / head_dim)
+        sign = np.where(lane % head_dim < half, -1.0, 1.0)
+        for table, positions in (
+            (inside, np.arange(SPAN)),
+            (upper, np.arange(devices * SPANS // SPAN_PART) * SPAN_PART * SPAN),
+            (lower, np.arange(SPAN_PART) * SPAN),
+        ):
+            angles = positions[:, None] * rate
+            table += [np.cos(angles), np.sin(angles) * sign]
+    return [np.stack(t).astype(np.float32) for t in (inside, upper, lower)]
+
+
+def turned_by(first, second):
+    return (
+        first[0] * second[0] - first[1] * second[1],
+        first[1] * second[0] + first[0] * second[1],
+    )
+
+
+def span_tables(table_refs, block, group):
+    inside_ref, upper_ref, lower_ref = table_refs
+    start = turned_by(
+        *(
+            [ref[2 * group + k, pl.ds(at, 1), :] for k in range(2)]
+            for ref, at in ((upper_ref, block // SPAN_PART), (lower_ref, block % SPAN_PART))
         )
-
-    row = np.arange(SPAN)[:, None]
-    first = (np.arange(devices * SPANS) * SPAN)[:, None]
-    inside, starts = [], []
-    for head_dim in (128, 64):
-        rate, sign = inverse(head_dim)
-        inside += [np.cos(row * rate), np.sin(row * rate) * sign]
-        starts += [
-            np.cos(first * rate).reshape(devices, SPANS, LANES),
-            (np.sin(first * rate) * sign).reshape(devices, SPANS, LANES),
-        ]
-    return (
-        np.stack(inside).astype(np.float32),
-        np.concatenate(starts, axis=1).astype(np.float32),
-    )
-
-
-def span_tables(inside_ref, start_ref, span, group):
-    cos_row, sin_row = inside_ref[2 * group], inside_ref[2 * group + 1]
-    cos_start = start_ref[0, pl.ds(2 * group * SPANS + span, 1), :]
-    sin_start = start_ref[0, pl.ds((2 * group + 1) * SPANS + span, 1), :]
-    return (
-        cos_row * cos_start - sin_row * sin_start,
-        sin_row * cos_start + cos_row * sin_start,
-    )
+    )
+    return turned_by((inside_ref[2 * group], inside_ref[2 * group + 1]), start)
 
 
 def rotated_wide(x, tables):
@@ -106,17 +107,16 @@
 
 
 def states_kernel(
-    index_ref, _, wk_ref, wv_ref, nk_ref, nv_ref, wd_ref, nd_ref, inside_ref, start_ref, *refs, staged,
+    index_ref, _, wk_ref, wv_ref, nk_ref, nv_ref, wd_ref, nd_ref, *refs, staged,
 ):
+    table_refs, refs = refs[:3], refs[3:]
     sources, refs = refs[:staged], refs[staged:]
     before_ref, earlier_ref, message_ref = refs[:3]
     targets, refs = refs[3 : 3 + staged], refs[3 + staged :]
     rows_ref, state_ref, decay_ref, sems = refs
     span = pl.program_id(0)
-    copies = [
-        pltpu.make_async_copy(a.at[pl.ds(index_ref[0], 1)] if k == 0 else a, b, sems.at[k])
-        for k, (a, b) in enumerate(zip(sources, targets))
-    ]
+    place = index_ref[0] * SPANS + span
+    copies = [pltpu.make_async_copy(a, b, sems.at[k]) for k, (a, b) in enumerate(zip(sources, targets))]
 
     @pl.when(span == 0)
     def _():
@@ -131,13 +131,13 @@
     kept = jnp.exp(last)
     before_ref[0] = state_ref[...]
     earlier_ref[0] = decay_ref[...]
-    tables = span_tables(inside_ref, start_ref, span, 0)
+    tables = span_tables(table_refs, place, 0)
     for head in range(3):
         cut = slice(head * 128, head * 128 + 128)
         keys = rotated_wide(wk_ref[:, cut], tables) * WIDE_SCALE
         scaled = (keys * tail[:, head : head + 1]).astype(BF16)
         state_ref[cut, :] = state_ref[cut, :] * kept[head : head + 1, :] + mm_tn(scaled, wv_ref[:, cut])
-    tables = span_tables(inside_ref, start_ref, span, 1)
+    tables = span_tables(table_refs, place, 1)
     keys = rotated_narrow(nk_ref[...], tables) * NARROW_SCALE
     tails = jnp.where(low_lanes((SPAN, LANES)), tail[:, 3:4], tail[:, 4:5])
     own = mm_tn((keys * tails).astype(BF16), nv_ref[...])
@@ -186,11 +186,13 @@
 
 def finish_kernel(
     index_ref, turn_ref, wq_ref, wk_ref, wv_ref, wg_ref, nq_ref, nk_ref, nv_ref, ng_ref, wd_ref, nd_ref,
-    inside_ref, start_ref, before_ref, earlier_ref, prefix_ref, wide_out_ref, narrow_out_ref,
+    inside_ref, upper_ref, lower_ref, before_ref, earlier_ref, prefix_ref, wide_out_ref, narrow_out_ref,
     *out_refs, first,
 ):
     *out_refs, rows_ref, mixed_ref = out_refs
     span = turned_span(first + pl.program_id(0), turn_ref[0])
+    place = index_ref[0] * SPANS + span
+    table_refs = (inside_ref, upper_ref, lower_ref)
     total = running_decay(wd_ref, nd_ref, rows_ref)
     columns = total.T
     grown = jnp.exp(columns)
@@ -202,7 +204,7 @@
         gaps = columns[:, head : head + 1] - total[head : head + 1, :]
         return (scores * jnp.exp(jnp.where(causal, gaps, -jnp.inf))).astype(BF16)
 
-    tables = span_tables(inside_ref, start_ref, span, 0)
+    tables = span_tables(table_refs, place, 0)
     for head in range(3):
         cut = slice(head * 128, head * 128 + 128)
         queries = rotated_wide(wq_ref[:, cut], tables).astype(BF16)
@@ -215,7 +217,7 @@
         scale = lax.rsqrt(jnp.mean(output * output, axis=-1, keepdims=True) + EPS)
         mixed_ref[:, cut] = gated(output, wg_ref[:, cut], scale)
 
-    tables = span_tables(inside_ref, start_ref, span, 1)
+    tables = span_tables(table_refs, place, 1)
     queries = rotated_narrow(nq_ref[...], tables).astype(BF16)
     keys = (rotated_narrow(nk_ref[...], tables) * NARROW_SCALE).astype(BF16)
     values = nv_ref[...]
@@ -314,11 +316,10 @@
 
 
 def far_mixer_kernel(*refs, ups, downs):
-    halves, refs = refs[:4], refs[4:]
-    both_ref, up_ref, down_ref, out_ref, low_ref, high_ref, x_ref, hidden_ref, sems = refs
+    halves, refs = refs[:2], refs[2:]
+    both_ref, up_ref, down_ref, low_ref, high_ref, x_ref, hidden_ref, sems = refs
     devices, share, units = up_ref.shape
     half = halves[0].shape[0]
-    rows = 2 * half
     block = units // ups
     group = devices // downs
     lines = group * share
@@ -351,8 +352,7 @@
     def lower(k, far_ref, base):
         down_copy(k).wait()
         lowered = down_block(down_ref, hidden_ref, k, group)
-        out_ref[pl.ds(pl.multiple_of(k * lines, lines), lines), :] = lowered[:, :rows]
-        far_ref[pl.ds(pl.multiple_of((k - base) * lines, lines), lines), :] = lowered[:, rows:]
+        far_ref[pl.ds(pl.multiple_of((k - base) * lines, lines), lines), :] = lowered
 
     @pl.loop(0, downs // 2)
     def _(k):
@@ -388,6 +388,18 @@
             at = slice(k * lines, (k + 1) * lines)
             minus_ref[at, :] = lowered[:, :rows]
             plus_ref[at, :] = lowered[:, rows:]
+
+
+def own_mixer_kernel(first_ref, second_ref, up_ref, down_ref, out_ref, x_ref, hidden_ref, *, parts):
+    devices, share, units = up_ref.shape
+    half = first_ref.shape[0]
+    x_ref[:half] = first_ref[...]
+    x_ref[half:] = second_ref[...]
+    hidden_ref[...] = up_block(x_ref, up_ref, 0, units)
+    group = devices // parts
+    lines = group * share
+    for k in range(parts):
+        out_ref[k * lines : (k + 1) * lines, :] = down_block(down_ref, hidden_ref, k, group)
 
 
 SMALL = pltpu.CompilerParams(vmem_limit_bytes=16 * 1024 * 1024)
@@ -438,15 +450,12 @@
         jnp.concatenate([up_weight, down_weight.T], axis=0), SP, axis=0, tiled=True
     ).reshape(devices, 2, share, units)
 
-    inside, starts = (jnp.asarray(t) for t in position_tables(devices))
+    tables = [jnp.asarray(t) for t in position_tables(devices)]
     scalars = [
         lax.axis_index(SP).astype(jnp.int32).reshape(1),
         lax.axis_index("tp").astype(jnp.int32).reshape(1),
     ]
-    table_blocks = [
-        pl.BlockSpec((4, SPAN, LANES), lambda s, i, t: (0, 0, 0)),
-        pl.BlockSpec((1, 4 * SPANS, LANES), lambda s, i, t: (i[0], 0, 0)),
-    ]
+    table_blocks = [pl.BlockSpec(t.shape, lambda s, i, t: (0, 0, 0)) for t in tables]
 
     def span_blocks(at):
         return (
@@ -464,7 +473,7 @@
 
     wide_block, narrow_block, decay_blocks, state_blocks = span_blocks(lambda s, i, t: s)
     staged = (
-        starts, inside, wide_decay, narrow_decay, wide_query, wide_key, wide_value, wide_gate,
+        *tables, wide_decay, narrow_decay, wide_query, wide_key, wide_value, wide_gate,
         narrow_query, narrow_key, narrow_value, narrow_gate, wide_out, narrow_out,
     )
     before, earlier, message, *held = pl.pallas_call(
@@ -473,8 +482,7 @@
             jax.ShapeDtypeStruct((SPANS, 512, LANES), F32),
             jax.ShapeDtypeStruct((SPANS, 8, LANES), F32),
             jax.ShapeDtypeStruct((devices, 16, LANES), BF16),
-            pltpu.VMEM((1, *starts.shape[1:]), F32),
-            *(pltpu.VMEM(x.shape, x.dtype) for x in staged[1:]),
+            *(pltpu.VMEM(x.shape, x.dtype) for x in staged),
         ),
         grid_spec=pltpu.PrefetchScalarGridSpec(
             num_scalar_prefetch=2,
@@ -504,7 +512,7 @@
             pltpu.with_memory_space_constraint(x, pltpu.HBM)
             for x in (
                 wide_key, wide_value, narrow_key, narrow_value,
-                wide_decay, narrow_decay, inside, starts, *staged,
+                wide_decay, narrow_decay, *tables, *staged,
             )
         ),
     )
@@ -529,8 +537,7 @@
                 grid=(count,),
                 in_specs=[
                     wide, wide, wide, wide, narrow, narrow, narrow, narrow,
-                    *decays, table_blocks[0],
-                    pl.BlockSpec((1, 4 * SPANS, LANES), lambda s, i, t: (0, 0, 0)), *states,
+                    *decays, *table_blocks, *states,
                     pl.BlockSpec((512, LANES), lambda s, i, t: (0, 0)),
                     pl.BlockSpec((384, width), lambda s, i, t: (0, 0)),
                     pl.BlockSpec((128, width), lambda s, i, t: (0, 0)),
@@ -546,7 +553,7 @@
                 transcendentals=150_000 * count,
             ),
         )(
-            *scalars, *held[4:12], held[2], held[3], held[1], held[0], before, earlier, prefix, *held[12:],
+            *scalars, *held[5:13], *held[3:5], *held[:3], before, earlier, prefix, *held[13:],
         )
 
     half = rows // 2
@@ -586,21 +593,23 @@
     turned_half = pltpu.VMEM((width // 2, rows), BF16)
     weights = pltpu.VMEM((devices, share, units), BF16)
     scratch = [pltpu.VMEM((2 * rows, width), BF16), pltpu.VMEM((units, 2 * rows), BF16)]
-    up, down, own, low, high = pl.pallas_call(
+    scratch_half = [pltpu.VMEM((rows, width), BF16), pltpu.VMEM((units, rows), BF16)]
+    own_low, own_high = low, high
+    up, down, low, high = pl.pallas_call(
         functools.partial(far_mixer_kernel, ups=ups, downs=downs),
-        out_shape=(weights, weights, turned, turned_half, turned_half),
-        in_specs=[*([whole] * 4), pl.BlockSpec(memory_space=pltpu.HBM)],
-        out_specs=[whole] * 5,
-        scratch_shapes=[*scratch, pltpu.SemaphoreType.DMA((ups + downs,))],
+        out_shape=(weights, weights, turned_half, turned_half),
+        in_specs=[*([whole] * 2), pl.BlockSpec(memory_space=pltpu.HBM)],
+        out_specs=[whole] * 4,
+        scratch_shapes=[*scratch_half, pltpu.SemaphoreType.DMA((ups + downs,))],
         compiler_params=SMALL,
         name="mixer_far",
         cost_estimate=pl.CostEstimate(
-            flops=8 * rows * width * units, bytes_accessed=20_000_000, transcendentals=0
+            flops=4 * rows * width * units, bytes_accessed=20_000_000, transcendentals=0
         ),
-    )(low, high, far_low, far_high, pltpu.with_memory_space_constraint(both, pltpu.HBM))
+    )(far_low, far_high, pltpu.with_memory_space_constraint(both, pltpu.HBM))
     low, high = shifted(low, "tp", 1), shifted(high, "tp", -1)
     minus_low, minus_high, plus_low, plus_high = pl.pallas_call(
-        functools.partial(near_mixer_kernel, ups=2, downs=2),
+        functools.partial(near_mixer_kernel, ups=1, downs=2),
         out_shape=(turned_half,) * 4,
         in_specs=[whole] * 6,
         out_specs=[whole] * 4,
@@ -622,6 +631,19 @@
         cost_estimate=pl.CostEstimate(flops=500_000, bytes_accessed=1_500_000, transcendentals=0),
     )(plus_low, minus_high, low, high)
     below_low, above_high = shifted(plus_low, "tp", 1), shifted(minus_high, "tp", -1)
+    own_low, _ = lax.optimization_barrier((own_low, plus_low))
+    own = pl.pallas_call(
+        functools.partial(own_mixer_kernel, parts=2),
+        out_shape=turned,
+        in_specs=[whole] * 4,
+        out_specs=whole,
+        scratch_shapes=scratch_half,
+        compiler_params=SMALL,
+        name="mixer_own",
+        cost_estimate=pl.CostEstimate(
+            flops=4 * rows * width * units, bytes_accessed=2_000_000, transcendentals=0
+        ),
+    )(own_low, own_high, up, down)
     return pl.pallas_call(
         result_kernel,
         out_shape=jax.ShapeDtypeStruct((rows, width), BF16),

time: 155 us -> 154 us (level)
  waiting for transfers between devices: 39.5 us -> 35.9 us
  Pallas kernels: 29.1 us -> 31.4 us
    ppermute x16, waiting for transfers between devices: 28 us -> 24.5 us  [shifted(): lax.ppermute(array, axis, [(k, (k + by) % size) for k in range(size)])]
    pallas_call x1 -> x2, Pallas kernels: 5.05 us -> 7.95 us  [the longest x1 4.49 us: local(): pl.pallas_call(functools.partial(near_mixer_kernel, ups=1, downs=2), out_...]
  transfers between devices with their start and end apart: 17 -> 17, of which waited for: 8 -> 7; matrix products, arithmetic and copies ran while one was open for 0% -> 0% of each run, Pallas kernels for 18% -> 20%
where the time goes in v5:
time: 154 us; the launch traced here: 152 us
  blocking collectives  42.7 us (28%)
  waiting for transfers between devices  35.9 us (23%)
  Pallas kernels  31.4 us (20%)
  starting transfers between devices  26.4 us (17%)
  between operations  13.5 us (9%)
  other arithmetic  1.69 us (1%)
    ppermute x16, starting transfers between devices, shifted(): lax.ppermute(array, axis, [(k, (k + by) % size) for k in range(size)])  26.4 us
    all_to_all x1, blocking collectives, local(): arrived = lax.all_to_all(message, SP, 0, 0, tiled=True)  25.7 us
    ppermute x16, waiting for transfers between devices, shifted(): lax.ppermute(array, axis, [(k, (k + by) % size) for k in range(size)])  24.5 us
    all_to_all x1, blocking collectives, local(): prefix = lax.all_to_all(prefixes, SP, 0, 0, tiled=True).reshape(512, LANES)  17 us
    all_gather x1, waiting for transfers between devices, local(): lax.all_gather(jnp.concatenate([up_weight, down_weight.T], axis=0), SP, a...  11.3 us
    pallas_call x2, Pallas kernels, finish(): pl.pallas_call(functools.partial(finish_kernel, first=first), out_shape=o...  7.47 us
    pallas_call x1, Pallas kernels, local(): pl.pallas_call(functools.partial(far_mixer_kernel, ups=ups, downs=downs),...  7.04 us
    pallas_call x1, Pallas kernels, local(): pl.pallas_call(functools.partial(states_kernel, staged=len(staged)), out_...  6.23 us
  transfers between devices with their start and end apart: 17, of which 7 were waited for; matrix products, arithmetic and copies ran while one was open for 0% of the time, Pallas kernels for 20%

profile of v5, /device:TPU:32, one launch (start us, length us, event | category | flops | bytes accessed | tf_op | source)
XLA Modules:
  0.0 151.5 jit_solution(1254135459799332258)
XLA Ops:
  6.5 1.7 %pad_maximum_fusion = bf16[64,2048]{1,0:T(8,128)(2,1)} fusion(bf16[32,2048]{1,0:T(8,128)(2,1)} %bitcast.14, bf16[32,2048]{1,0:T(8,128)(2,1)} %param.34), kind=kLoop, calls=%fused_computation | loop fusion | flops 524288 | bytes 524288 | tf_op jit(solution)/shard_map/concatenate | solution.py:450
  8.3 6.2 %states.1 = (f32[4,512,128]{2,1,0:T(8,128)S(1)}, f32[4,8,128]{2,1,0:T(8,128)S(1)}, bf16[64,16,128]{2,1,0:T(8,128)(2,1)S(1)}, f32[4,128,128]{2,1,0:T(8,128)S(1)},...) custom-call(s32[1]{0:T(128)} %bitcast.index_ref, ...), custom_call_target="tpu_custom_call" | custom-call | flops 60000000 | bytes 2500000 | tf_op jit(solution)/shard_map/states/pallas_call | solution.py:479
  14.5 25.7 %all_to_all.10.message_ref = bf16[64,16,128]{2,1,0:T(8,128)(2,1)S(1)} all-to-all(bf16[64,16,128]{2,1,0:T(8,128)(2,1)S(1)} %get-tuple-element.56), channel_id=1, replica_groups=mesh['sp_0'=8,'sp_1'=4,'sp_2'=2,'tp'=4] {'sp_0','sp_1','sp_2'}, dimensions={0} | all-to-all | bytes 524288 | tf_op jit(solution)/shard_map/all_to_all | solution.py:520
  40.3 17.0 %all_to_all.11 = bf16[64,8,128]{2,1,0:T(8,128)(2,1)S(1)} all-to-all(bf16[64,8,128]{2,1,0:T(8,128)(2,1)S(1)} %prefix.1), channel_id=1, replica_groups=mesh['sp_0'=8,'sp_1'=4,'sp_2'=2,'tp'=4] {'sp_0','sp_1','sp_2'}, dimensions={0} | all-to-all | bytes 262144 | tf_op jit(solution)/shard_map/all_to_all | solution.py:528
  57.4 1.9 %finish_far.1 = (bf16[64,2048]{1,0:T(8,128)(2,1)S(1)}, bf16[64,2048]{1,0:T(8,128)(2,1)S(1)}) custom-call(s32[1]{0:T(128)} %bitcast.index_ref, s32[1]{0:T(128)} %bitcast.1._.turn_ref, bf16[512,384]{1,0:T(8,128)(2,1)S(1)} %get-tuple-element.41.wq_ref, bf16[512,384]{1,0:T(8,128)(2,1)S(1)} %get-tuple-element.42.wk_ref, ...), custom_call_target="tpu_custom_call" | custom-call | flops 350000000 | bytes 4500000 | tf_op jit(solution)/shard_map/finish_far/pallas_call | solution.py:532
  60.5 2.0 %collective-permute-start.1 = (bf16[64,2048]{1,0:T(8,128)(2,1)S(1)}, bf16[64,2048]{1,0:T(8,128)(2,1)S(1)}, u32[]{:S(2)}, u32[]{:S(2)}) collective-permute-start(bf16[64,2048]{1,0:T(8,128)(2,1)S(1)} %get-tuple-element.60), channel_id=1, source_target_pairs={{0,3},{1,0},{2,1},{3,2},{4,7},{5,4},{6,5},{7,6},{8,11},{9,8},{10,9... | collective-permute-start | bytes 786440 | tf_op jit(solution)/shard_map/ppermute | solution.py:410
  62.5 5.6 %finish.1.minus_ref.plus_ref.own_ref = bf16[3,128,2048]{2,1,0:T(8,128)(2,1)S(1)} custom-call(s32[1]{0:T(128)} %bitcast.index_ref, s32[1]{0:T(128)} %bitcast.1._.turn_ref, bf16[512,384]{1,0:T(8,128)(2,1)S(1)} %get-tuple-element.41.wq_ref, bf16[512,384]{1,0:T(8,128)(2,1)S(1)} %get-tuple-element.42.wk_ref, bf16[512,384]{1,0:T(8,128)(2,1)S(1)} %get-tuple-element.43.wv_ref, ...), custom_call_target="tpu_custom_call" | custom-call | flops 1050000000 | bytes 7500000 | tf_op jit(solution)/shard_map/finish/pallas_call | solution.py:532
  70.4 2.0 %collective-permute-start.3 = (bf16[128,2048]{1,0:T(8,128)(2,1)S(1)}, bf16[128,2048]{1,0:T(8,128)(2,1)S(1)}, u32[]{:S(2)}, u32[]{:S(2)}) collective-permute-start(bf16[128,2048]{1,0:T(8,128)(2,1)S(1)} %get-tuple-element.62), channel_id=1, source_target_pairs={{0,3},{1,0},{2,1},{3,2},{4,7},{5,4},{6,5},{7,6},{8,11},{9,8},{10,9... | collective-permute-start | bytes 1572872 | tf_op jit(solution)/shard_map/ppermute | solution.py:410
  72.3 11.1 %collective-permute-done.2.below_ref = bf16[128,2048]{1,0:T(8,128)(2,1)S(1)} collective-permute-done((bf16[128,2048]{1,0:T(8,128)(2,1)S(1)}, bf16[128,2048]{1,0:T(8,128)(2,1)S(1)}, u32[]{:S(2)}, u32[]{:S(2)}) %collective-permute-start.2) | collective-permute-done | bytes 524320 | tf_op jit(solution)/shard_map/ppermute | solution.py:410
  85.2 2.4 %collective-permute-start.7 = (bf16[64,2048]{1,0:T(8,128)(2,1)S(1)}, bf16[64,2048]{1,0:T(8,128)(2,1)S(1)}, u32[]{:S(2)}, u32[]{:S(2)}) collective-permute-start(bf16[64,2048]{1,0:T(8,128)(2,1)S(1)} %get-tuple-element.64.second_ref), channel_id=1, source_target_pairs={{0,3},{1,0},{2,1},{3,2},{4,7},{5,4},{6,5},{7,6},{8,11},{9,8},{10,9... | collective-permute-start | bytes 786440 | tf_op jit(solution)/shard_map/ppermute | solution.py:410
  87.6 4.7 %collective-permute-done.4.refs_0_ = bf16[64,2048]{1,0:T(8,128)(2,1)S(1)} collective-permute-done((bf16[64,2048]{1,0:T(8,128)(2,1)S(1)}, bf16[64,2048]{1,0:T(8,128)(2,1)S(1)}, u32[]{:S(2)}, u32[]{:S(2)}) %collective-permute-start.4) | collective-permute-done | bytes 262176 | tf_op jit(solution)/shard_map/ppermute | solution.py:410
  92.3 3.2 %collective-permute-start.9 = (bf16[64,2048]{1,0:T(8,128)(2,1)S(1)}, bf16[64,2048]{1,0:T(8,128)(2,1)S(1)}, u32[]{:S(2)}, u32[]{:S(2)}) collective-permute-start(bf16[64,2048]{1,0:T(8,128)(2,1)S(1)} %collective-permute-done.7.refs_3_), channel_id=1, source_target_pairs={{0,3},{1,0},{2,1},{3,2},{4,7},{5,4},{6,5},{7,6},{8,11},{9,8},{10,9... | collective-permute-start | bytes 786440 | tf_op jit(solution)/shard_map/ppermute | solution.py:410
  95.5 3.2 %collective-permute-start.6 = (bf16[64,2048]{1,0:T(8,128)(2,1)S(1)}, bf16[64,2048]{1,0:T(8,128)(2,1)S(1)}, u32[]{:S(2)}, u32[]{:S(2)}) collective-permute-start(bf16[64,2048]{1,0:T(8,128)(2,1)S(1)} %get-tuple-element.72.first_ref), channel_id=1, source_target_pairs={{0,3},{1,0},{2,1},{3,2},{4,7},{5,4},{6,5},{7,6},{8,11},{9,8},{10,9... | collective-permute-start | bytes 786440 | tf_op jit(solution)/shard_map/ppermute | solution.py:410
  98.8 3.5 %collective-permute-done.8.refs_0_ = bf16[64,2048]{1,0:T(8,128)(2,1)S(1)} collective-permute-done((bf16[64,2048]{1,0:T(8,128)(2,1)S(1)}, bf16[64,2048]{1,0:T(8,128)(2,1)S(1)}, u32[]{:S(2)}, u32[]{:S(2)}) %collective-permute-start.8) | collective-permute-done | bytes 262176 | tf_op jit(solution)/shard_map/ppermute | solution.py:410
  102.3 11.3 %all-gather.2.cloned.1.call-done = bf16[4096,2048]{1,0:T(8,128)(2,1)} async-done(((bf16[64,2048]{1,0:T(8,128)(2,1)}), bf16[4096,2048]{1,0:T(8,128)(2,1)}) %all-gather.2.cloned.1.call-update) | async-done | bytes 16777232 | tf_op jit(solution)/shard_map/all_gather | solution.py:449
  113.6 7.0 %mixer_far.1 = (bf16[64,32,2048]{2,1,0:T(8,128)(2,1)S(1)}, bf16[64,32,2048]{2,1,0:T(8,128)(2,1)S(1)}, bf16[1024,128]{1,0:T(8,128)(2,1)S(1)}, bf16[1024,128]{1,0:T(8,128)(2,1)S(1)}) custom-call(bf16[64,2048]{1,0:T(8,128)(2,1)S(1)} %collective-permute-done.8.refs_0_, bf16[64,2048]{1,0:T(8,128)(2,1)S(1)} %collective-permute-done.9.refs_1_, ...), custom_call_target="tpu_custom_call" | custom-call | flops 2147483648 | bytes 20000000 | tf_op jit(solution)/shard_map/mixer_far/pallas_call | solution.py:598
  120.6 1.6 %collective-permute-start.10 = (bf16[1024,128]{1,0:T(8,128)(2,1)S(1)}, bf16[1024,128]{1,0:T(8,128)(2,1)S(1)}, u32[]{:S(2)}, u32[]{:S(2)}) collective-permute-start(bf16[1024,128]{1,0:T(8,128)(2,1)S(1)} %get-tuple-element.69), channel_id=1, source_target_pairs={{0,1},{1,2},{2,3},{3,0},{4,5},{5,6},{6,7},{7,4},{8,9},{9,10},{10,1... | collective-permute-start | bytes 786440 | tf_op jit(solution)/shard_map/ppermute | solution.py:410
  122.2 1.8 %collective-permute-start.11 = (bf16[1024,128]{1,0:T(8,128)(2,1)S(1)}, bf16[1024,128]{1,0:T(8,128)(2,1)S(1)}, u32[]{:S(2)}, u32[]{:S(2)}) collective-permute-start(bf16[1024,128]{1,0:T(8,128)(2,1)S(1)} %get-tuple-element.70), channel_id=1, source_target_pairs={{0,3},{1,0},{2,1},{3,2},{4,7},{5,4},{6,5},{7,6},{8,11},{9,8},{10,9... | collective-permute-start | bytes 786440 | tf_op jit(solution)/shard_map/ppermute | solution.py:410
  124.0 4.5 %mixer_near.1 = (bf16[1024,128]{1,0:T(8,128)(2,1)S(1)}, bf16[1024,128]{1,0:T(8,128)(2,1)S(1)}, bf16[1024,128]{1,0:T(8,128)(2,1)S(1)}, bf16[1024,128]{1,0:T(8,128)(2,1)S(1)}) custom-call(bf16[64,2048]{1,0:T(8,128)(2,1)S(1)} %collective-permute-done.4.refs_0_, bf16[64,2048]{1,0:T(8,128)(2,1)S(1)} %collective-permute-done.5.refs_1_, ...), custom_call_target="tpu_custom_call" | custom-call | flops 4294967296 | bytes 2000000 | tf_op jit(solution)/shard_map/mixer_near/pallas_call | solution.py:611
  128.8 3.0 %collective-permute-start.14 = (bf16[1024,128]{1,0:T(8,128)(2,1)S(1)}, bf16[1024,128]{1,0:T(8,128)(2,1)S(1)}, u32[]{:S(2)}, u32[]{:S(2)}) collective-permute-start(bf16[1024,128]{1,0:T(8,128)(2,1)S(1)} %get-tuple-element.74), channel_id=1, source_target_pairs={{0,3},{1,0},{2,1},{3,2},{4,7},{5,4},{6,5},{7,6},{8,11},{9,8},{10,9... | collective-permute-start | bytes 786440 | tf_op jit(solution)/shard_map/ppermute | solution.py:410
  132.1 3.1 %collective-permute-start.15 = (bf16[1024,128]{1,0:T(8,128)(2,1)S(1)}, bf16[1024,128]{1,0:T(8,128)(2,1)S(1)}, u32[]{:S(2)}, u32[]{:S(2)}) collective-permute-start(bf16[1024,128]{1,0:T(8,128)(2,1)S(1)} %get-tuple-element.75), channel_id=1, source_target_pairs={{0,3},{1,0},{2,1},{3,2},{4,7},{5,4},{6,5},{7,6},{8,11},{9,8},{10,9... | collective-permute-start | bytes 786440 | tf_op jit(solution)/shard_map/ppermute | solution.py:410
  135.2 3.5 %mixer_own.1.own_ref = bf16[2048,128]{1,0:T(8,128)(2,1)S(1)} custom-call(bf16[64,2048]{1,0:T(8,128)(2,1)S(1)} %get-tuple-element.72.first_ref, bf16[64,2048]{1,0:T(8,128)(2,1)S(1)} %get-tuple-element.64.second_ref, bf16[64,32,2048]{2,1,0:T(8,128)(2,1)S(1)} %get-tuple-element.65.refs_4_.up_ref, bf16[64,32,2048]{2,1,0:T(8,128)(2,1)S(1)} %get-tuple-element.66.refs_5_.down_ref), custom_call_target="tpu_custom_call" | custom-call | flops 2147483648 | bytes 2000000 | tf_op jit(solution)/shard_map/mixer_own/pallas_call | solution.py:635
  138.9 4.3 %collective-permute-done.12.below_low_ref = bf16[1024,128]{1,0:T(8,128)(2,1)S(1)} collective-permute-done((bf16[1024,128]{1,0:T(8,128)(2,1)S(1)}, bf16[1024,128]{1,0:T(8,128)(2,1)S(1)}, u32[]{:S(2)}, u32[]{:S(2)}) %collective-permute-start.12) | collective-permute-done | bytes 262176 | tf_op jit(solution)/shard_map/ppermute | solution.py:410
  143.3 1.4 result.1
  (33 shorter events, 6.4 us)
Async XLA Ops:
  6.5 107.1 %all-gather.2.cloned.1.call-start = ((), (), s32[]{:S(2)}) async-start(), calls=%async_computation.2 | async-start | bytes 17039360 | tf_op jit(solution)/shard_map/all_gather | solution.py:449
  57.3 26.1 %copy-start = (bf16[128,2048]{1,0:T(8,128)(2,1)S(1)}, bf16[128,2048]{1,0:T(8,128)(2,1)}, u32[]{:S(2)}) copy-start(bf16[128,2048]{1,0:T(8,128)(2,1)} %residual_ref.1) | copy-start | bytes 1572868
  57.3 26.1 %copy-start.1 = (f32[2048]{0:T(1024)S(1)}, f32[2048]{0:T(1024)}, u32[]{:S(2)}) copy-start(f32[2048]{0:T(1024)} %param.36) | copy-start | bytes 24580
  57.3 26.1 %copy-start.2 = (f32[2048]{0:T(1024)S(1)}, f32[2048]{0:T(1024)}, u32[]{:S(2)}) copy-start(f32[2048]{0:T(1024)} %param.37) | copy-start | bytes 24580
  59.2 9.6 %collective-permute-start = (bf16[64,2048]{1,0:T(8,128)(2,1)S(1)}, bf16[64,2048]{1,0:T(8,128)(2,1)S(1)}, u32[]{:S(2)}, u32[]{:S(2)}) collective-permute-start(bf16[64,2048]{1,0:T(8,128)(2,1)S(1)} %get-tuple-element.59), channel_id=1, source_target_pairs={{0,1},{1,2},{2,3},{3,0},{4,5},{5,6},{6,7},{7,4},{8,9},{9,10},{10,1... | collective-permute-start | bytes 786440 | tf_op jit(solution)/shard_map/ppermute | solution.py:410
  60.5 8.3 %collective-permute-start.1 = (bf16[64,2048]{1,0:T(8,128)(2,1)S(1)}, bf16[64,2048]{1,0:T(8,128)(2,1)S(1)}, u32[]{:S(2)}, u32[]{:S(2)}) collective-permute-start(bf16[64,2048]{1,0:T(8,128)(2,1)S(1)} %get-tuple-element.60), channel_id=1, source_target_pairs={{0,3},{1,0},{2,1},{3,2},{4,7},{5,4},{6,5},{7,6},{8,11},{9,8},{10,9... | collective-permute-start | bytes 786440 | tf_op jit(solution)/shard_map/ppermute | solution.py:410
  69.0 14.4 %collective-permute-start.2 = (bf16[128,2048]{1,0:T(8,128)(2,1)S(1)}, bf16[128,2048]{1,0:T(8,128)(2,1)S(1)}, u32[]{:S(2)}, u32[]{:S(2)}) collective-permute-start(bf16[128,2048]{1,0:T(8,128)(2,1)S(1)} %get-tuple-element.61), channel_id=1, source_target_pairs={{0,1},{1,2},{2,3},{3,0},{4,5},{5,6},{6,7},{7,4},{8,9},{9,10},{10,1... | collective-permute-start | bytes 1572872 | tf_op jit(solution)/shard_map/ppermute | solution.py:410
  70.4 13.0 %collective-permute-start.3 = (bf16[128,2048]{1,0:T(8,128)(2,1)S(1)}, bf16[128,2048]{1,0:T(8,128)(2,1)S(1)}, u32[]{:S(2)}, u32[]{:S(2)}) collective-permute-start(bf16[128,2048]{1,0:T(8,128)(2,1)S(1)} %get-tuple-element.62), channel_id=1, source_target_pairs={{0,3},{1,0},{2,1},{3,2},{4,7},{5,4},{6,5},{7,6},{8,11},{9,8},{10,9... | collective-permute-start | bytes 1572872 | tf_op jit(solution)/shard_map/ppermute | solution.py:410
  84.3 8.0 %collective-permute-start.4 = (bf16[64,2048]{1,0:T(8,128)(2,1)S(1)}, bf16[64,2048]{1,0:T(8,128)(2,1)S(1)}, u32[]{:S(2)}, u32[]{:S(2)}) collective-permute-start(bf16[64,2048]{1,0:T(8,128)(2,1)S(1)} %get-tuple-element.72.first_ref), channel_id=1, source_target_pairs={{0,1},{1,2},{2,3},{3,0},{4,5},{5,6},{6,7},{7,4},{8,9},{9,10},{10,1... | collective-permute-start | bytes 786440 | tf_op jit(solution)/shard_map/ppermute | solution.py:410
  85.2 7.1 %collective-permute-start.7 = (bf16[64,2048]{1,0:T(8,128)(2,1)S(1)}, bf16[64,2048]{1,0:T(8,128)(2,1)S(1)}, u32[]{:S(2)}, u32[]{:S(2)}) collective-permute-start(bf16[64,2048]{1,0:T(8,128)(2,1)S(1)} %get-tuple-element.64.second_ref), channel_id=1, source_target_pairs={{0,3},{1,0},{2,1},{3,2},{4,7},{5,4},{6,5},{7,6},{8,11},{9,8},{10,9... | collective-permute-start | bytes 786440 | tf_op jit(solution)/shard_map/ppermute | solution.py:410
  92.3 10.0 %collective-permute-start.8 = (bf16[64,2048]{1,0:T(8,128)(2,1)S(1)}, bf16[64,2048]{1,0:T(8,128)(2,1)S(1)}, u32[]{:S(2)}, u32[]{:S(2)}) collective-permute-start(bf16[64,2048]{1,0:T(8,128)(2,1)S(1)} %collective-permute-done.4.refs_0_), channel_id=1, source_target_pairs={{0,1},{1,2},{2,3},{3,0},{4,5},{5,6},{6,7},{7,4},{8,9},{9,10},{10,1... | collective-permute-start | bytes 786440 | tf_op jit(solution)/shard_map/ppermute | solution.py:410
  92.3 10.0 %collective-permute-start.9 = (bf16[64,2048]{1,0:T(8,128)(2,1)S(1)}, bf16[64,2048]{1,0:T(8,128)(2,1)S(1)}, u32[]{:S(2)}, u32[]{:S(2)}) collective-permute-start(bf16[64,2048]{1,0:T(8,128)(2,1)S(1)} %collective-permute-done.7.refs_3_), channel_id=1, source_target_pairs={{0,3},{1,0},{2,1},{3,2},{4,7},{5,4},{6,5},{7,6},{8,11},{9,8},{10,9... | collective-permute-start | bytes 786440 | tf_op jit(solution)/shard_map/ppermute | solution.py:410
  95.5 28.4 %collective-permute-start.5 = (bf16[64,2048]{1,0:T(8,128)(2,1)S(1)}, bf16[64,2048]{1,0:T(8,128)(2,1)S(1)}, u32[]{:S(2)}, u32[]{:S(2)}) collective-permute-start(bf16[64,2048]{1,0:T(8,128)(2,1)S(1)} %get-tuple-element.64.second_ref), channel_id=1, source_target_pairs={{0,1},{1,2},{2,3},{3,0},{4,5},{5,6},{6,7},{7,4},{8,9},{9,10},{10,1... | collective-permute-start | bytes 786440 | tf_op jit(solution)/shard_map/ppermute | solution.py:410
  95.5 28.4 %collective-permute-start.6 = (bf16[64,2048]{1,0:T(8,128)(2,1)S(1)}, bf16[64,2048]{1,0:T(8,128)(2,1)S(1)}, u32[]{:S(2)}, u32[]{:S(2)}) collective-permute-start(bf16[64,2048]{1,0:T(8,128)(2,1)S(1)} %get-tuple-element.72.first_ref), channel_id=1, source_target_pairs={{0,3},{1,0},{2,1},{3,2},{4,7},{5,4},{6,5},{7,6},{8,11},{9,8},{10,9... | collective-permute-start | bytes 786440 | tf_op jit(solution)/shard_map/ppermute | solution.py:410
  120.6 11.1 %collective-permute-start.10 = (bf16[1024,128]{1,0:T(8,128)(2,1)S(1)}, bf16[1024,128]{1,0:T(8,128)(2,1)S(1)}, u32[]{:S(2)}, u32[]{:S(2)}) collective-permute-start(bf16[1024,128]{1,0:T(8,128)(2,1)S(1)} %get-tuple-element.69), channel_id=1, source_target_pairs={{0,1},{1,2},{2,3},{3,0},{4,5},{5,6},{6,7},{7,4},{8,9},{9,10},{10,1... | collective-permute-start | bytes 786440 | tf_op jit(solution)/shard_map/ppermute | solution.py:410
  122.2 9.6 %collective-permute-start.11 = (bf16[1024,128]{1,0:T(8,128)(2,1)S(1)}, bf16[1024,128]{1,0:T(8,128)(2,1)S(1)}, u32[]{:S(2)}, u32[]{:S(2)}) collective-permute-start(bf16[1024,128]{1,0:T(8,128)(2,1)S(1)} %get-tuple-element.70), channel_id=1, source_target_pairs={{0,3},{1,0},{2,1},{3,2},{4,7},{5,4},{6,5},{7,6},{8,11},{9,8},{10,9... | collective-permute-start | bytes 786440 | tf_op jit(solution)/shard_map/ppermute | solution.py:410
  128.5 10.5 %collective-permute-start.13 = (bf16[1024,128]{1,0:T(8,128)(2,1)S(1)}, bf16[1024,128]{1,0:T(8,128)(2,1)S(1)}, u32[]{:S(2)}, u32[]{:S(2)}) collective-permute-start(bf16[1024,128]{1,0:T(8,128)(2,1)S(1)} %get-tuple-element.73), channel_id=1, source_target_pairs={{0,1},{1,2},{2,3},{3,0},{4,5},{5,6},{6,7},{7,4},{8,9},{9,10},{10,1... | collective-permute-start | bytes 786440 | tf_op jit(solution)/shard_map/ppermute | solution.py:410
  128.8 10.1 %collective-permute-start.14 = (bf16[1024,128]{1,0:T(8,128)(2,1)S(1)}, bf16[1024,128]{1,0:T(8,128)(2,1)S(1)}, u32[]{:S(2)}, u32[]{:S(2)}) collective-permute-start(bf16[1024,128]{1,0:T(8,128)(2,1)S(1)} %get-tuple-element.74), channel_id=1, source_target_pairs={{0,3},{1,0},{2,1},{3,2},{4,7},{5,4},{6,5},{7,6},{8,11},{9,8},{10,9... | collective-permute-start | bytes 786440 | tf_op jit(solution)/shard_map/ppermute | solution.py:410
  131.9 11.4 %collective-permute-start.12 = (bf16[1024,128]{1,0:T(8,128)(2,1)S(1)}, bf16[1024,128]{1,0:T(8,128)(2,1)S(1)}, u32[]{:S(2)}, u32[]{:S(2)}) collective-permute-start(bf16[1024,128]{1,0:T(8,128)(2,1)S(1)} %get-tuple-element.71), channel_id=1, source_target_pairs={{0,1},{1,2},{2,3},{3,0},{4,5},{5,6},{6,7},{7,4},{8,9},{9,10},{10,1... | collective-permute-start | bytes 786440 | tf_op jit(solution)/shard_map/ppermute | solution.py:410
  132.1 11.2 %copy-start.3 = (f32[2048]{0:T(1024)S(1)}, f32[2048]{0:T(1024)}, u32[]{:S(2)}) copy-start(f32[2048]{0:T(1024)} %param.38) | copy-start | bytes 24580
  132.1 11.2 %collective-permute-start.15 = (bf16[1024,128]{1,0:T(8,128)(2,1)S(1)}, bf16[1024,128]{1,0:T(8,128)(2,1)S(1)}, u32[]{:S(2)}, u32[]{:S(2)}) collective-permute-start(bf16[1024,128]{1,0:T(8,128)(2,1)S(1)} %get-tuple-element.75), channel_id=1, source_target_pairs={{0,3},{1,0},{2,1},{3,2},{4,7},{5,4},{6,5},{7,6},{8,11},{9,8},{10,9... | collective-permute-start | bytes 786440 | tf_op jit(solution)/shard_map/ppermute | solution.py:410
Sparse Core Ops, SparseCore 0:
  10.1 103.4 all-gather.1

commit v6 on v5

--- a/solution.py
+++ b/solution.py
@@ -13,6 +13,7 @@
 LANES = 128
 SPANS = 4
 SPAN_PART = 16
+SLICE_HEADS = (0, 0, 1, 1, 2, 2, 3, 4)
 SP = ("sp_0", "sp_1", "sp_2")
 SP_TP = ("sp_0", "sp_1", "sp_2", "tp")
 EPS = 1e-06
@@ -100,6 +101,16 @@
 
 def mm_tn(a, b):
     return lax.dot_general(a, b, (((0,), (0,)), ((), ())), preferred_element_type=F32)
+
+
+def in_two(values):
+    high = values.astype(BF16).astype(F32)
+    return high, values - high
+
+
+def log_rows(high, low):
+    sub = lax.broadcasted_iota(jnp.int32, (16, LANES), 0)
+    return jnp.where(sub == 0, high, jnp.where(sub == 1, low, 0.0)).astype(BF16)
 
 
 def turned_span(place, turn):
@@ -150,33 +161,39 @@
     @pl.when(span == SPANS - 1)
     def _():
         sums = decay_ref[...]
-        high = sums.astype(BF16).astype(F32)
-        low = sums - high
-        sub = lax.broadcasted_iota(jnp.int32, (8, LANES), 0)
-        at = 0
-        for head, count in enumerate((16, 16, 16, 8, 8)):
-            pair = jnp.where(
-                sub == 0,
-                high[head : head + 1, :],
-                jnp.where(sub == 1, low[head : head + 1, :], 0.0),
-            )
-            body = state_ref[at * 8 : (at + count) * 8, :].reshape(count, 8, LANES)
-            ends = jnp.broadcast_to(pair[None], (count, 8, LANES))
-            message_ref[at : at + count] = jnp.concatenate([body, ends], axis=1).astype(BF16)
-            at += count
+        high, low = in_two(sums)
+        for part, head in enumerate(SLICE_HEADS):
+            message_ref[part, 0:64] = state_ref[part * 64 : part * 64 + 64, :].astype(BF16)
+            message_ref[part, 64:80] = log_rows(high[head : head + 1, :], low[head : head + 1, :])
         for copy in copies:
             copy.wait()
 
 
-def prefix_kernel(message_ref, out_ref):
-    devices = message_ref.shape[0]
-    carried = jnp.zeros((8, LANES), F32)
-    for k in range(devices):
-        out_ref[k] = carried.astype(BF16)
-        if k + 1 < devices:
-            piece = message_ref[k].astype(F32)
-            kept = jnp.exp(piece[8:9, :] + piece[9:10, :])
-            carried = carried * kept + piece[0:8, :]
+def plane_kernel(message_ref, out_ref, within_ref, logs_ref):
+    carried = jnp.zeros((64, LANES), F32)
+    logs = jnp.zeros((1, LANES), F32)
+    for k in range(8):
+        within_ref[k] = carried
+        logs_ref[k] = jnp.broadcast_to(logs, (8, LANES))
+        piece = message_ref[k].astype(F32)
+        log = piece[64:65, :] + piece[65:66, :]
+        carried = carried * jnp.exp(log) + piece[0:64, :]
+        logs = logs + log
+    ends = log_rows(*in_two(logs))
+    for k in range(8):
+        out_ref[k, 0:64] = carried.astype(BF16)
+        out_ref[k, 64:80] = ends
+
+
+def prefix_kernel(index_ref, planes_ref, within_ref, logs_ref, out_ref):
+    plane = index_ref[0] // 8
+    carried = jnp.zeros((64, LANES), F32)
+    for k in range(7):
+        piece = planes_ref[k].astype(F32)
+        log = piece[64:65, :] + piece[65:66, :]
+        carried = jnp.where(k < plane, carried * jnp.exp(log) + piece[0:64, :], carried)
+    for k in range(8):
+        out_ref[k] = (carried * jnp.exp(logs_ref[k, 0:1, :]) + within_ref[k]).astype(BF16)
 
 
 def gated(output, gate, scale):
@@ -481,7 +498,7 @@
         out_shape=(
             jax.ShapeDtypeStruct((SPANS, 512, LANES), F32),
             jax.ShapeDtypeStruct((SPANS, 8, LANES), F32),
-            jax.ShapeDtypeStruct((devices, 16, LANES), BF16),
+            jax.ShapeDtypeStruct((8, 80, LANES), BF16),
             *(pltpu.VMEM(x.shape, x.dtype) for x in staged),
         ),
         grid_spec=pltpu.PrefetchScalarGridSpec(
@@ -493,7 +510,7 @@
             ],
             out_specs=[
                 *state_blocks,
-                pl.BlockSpec((devices, 16, LANES), lambda s, i, t: (0, 0, 0)),
+                pl.BlockSpec((8, 80, LANES), lambda s, i, t: (0, 0, 0)),
                 *([pl.BlockSpec(memory_space=pltpu.VMEM)] * len(staged)),
             ],
             scratch_shapes=[
@@ -517,15 +534,30 @@
         ),
     )
 
-    arrived = lax.all_to_all(message, SP, 0, 0, tiled=True)
+    arrived = lax.all_to_all(message, SP[1:], 0, 0, tiled=True)
+    planes, within, logs = pl.pallas_call(
+        plane_kernel,
+        out_shape=(
+            jax.ShapeDtypeStruct((8, 80, LANES), BF16),
+            jax.ShapeDtypeStruct((8, 64, LANES), F32),
+            jax.ShapeDtypeStruct((8, 8, LANES), F32),
+        ),
+        compiler_params=SMALL,
+        name="plane",
+        cost_estimate=pl.CostEstimate(flops=300_000, bytes_accessed=600_000, transcendentals=8_000),
+    )(arrived)
+    planes = lax.all_to_all(planes, SP[0], 0, 0, tiled=True)
+    whole = pl.BlockSpec(memory_space=pltpu.VMEM)
     prefixes = pl.pallas_call(
         prefix_kernel,
-        out_shape=jax.ShapeDtypeStruct((devices, 8, LANES), BF16),
+        out_shape=jax.ShapeDtypeStruct((8, 64, LANES), BF16),
+        in_specs=[pl.BlockSpec(memory_space=pltpu.SMEM), whole, whole, whole],
+        out_specs=whole,
         compiler_params=SMALL,
         name="prefix",
-        cost_estimate=pl.CostEstimate(flops=2_000_000, bytes_accessed=400_000, transcendentals=8_000),
-    )(arrived)
-    prefix = lax.all_to_all(prefixes, SP, 0, 0, tiled=True).reshape(512, LANES)
+        cost_estimate=pl.CostEstimate(flops=300_000, bytes_accessed=600_000, transcendentals=8_000),
+    )(scalars[0], planes, within, logs)
+    prefix = lax.all_to_all(prefixes, SP[1:], 0, 0, tiled=True).reshape(512, LANES)
 
     def finish(first, count, out_shape, out_specs):
         wide, narrow, decays, states = span_blocks(lambda s, i, t: turned_span(first + s, t[0]))
@@ -588,7 +620,6 @@
     far_low, far_high = shifted(below_low, "tp", 1), shifted(above_high, "tp", -1)
 
     ups, downs = 4, 4
-    whole = pl.BlockSpec(memory_space=pltpu.VMEM)
     turned = pltpu.VMEM((width, rows), BF16)
     turned_half = pltpu.VMEM((width // 2, rows), BF16)
     weights = pltpu.VMEM((devices, share, units), BF16)

time: 154 us -> 152 us (0.987)
  blocking collectives: 42.7 us -> 37.4 us
  waiting for transfers between devices: 35.9 us -> 39.5 us
    all_to_all x2 -> x3, blocking collectives: 42.7 us -> 37.4 us  [the longest x1 18.4 us: local(): planes = lax.all_to_all(planes, SP[0], 0, 0, tiled=True)]
    all_gather x1, waiting for transfers between devices: 11.3 us -> 16 us  [local(): lax.all_gather(jnp.concatenate([up_weight, down_weight.T], axis=0), SP, a...]
where the time goes in v6:
time: 152 us; the launch traced here: 150 us
  waiting for transfers between devices  39.5 us (26%)
  blocking collectives  37.4 us (25%)
  Pallas kernels  31.4 us (21%)
  starting transfers between devices  26.4 us (17%)
  between operations  13.5 us (9%)
  other arithmetic  1.69 us (1%)
    ppermute x16, starting transfers between devices, shifted(): lax.ppermute(array, axis, [(k, (k + by) % size) for k in range(size)])  26.4 us
    ppermute x16, waiting for transfers between devices, shifted(): lax.ppermute(array, axis, [(k, (k + by) % size) for k in range(size)])  23.5 us
    all_to_all x1, blocking collectives, local(): planes = lax.all_to_all(planes, SP[0], 0, 0, tiled=True)  18.4 us
    all_gather x1, waiting for transfers between devices, local(): lax.all_gather(jnp.concatenate([up_weight, down_weight.T], axis=0), SP, a...  16 us
    all_to_all x1, blocking collectives, local(): arrived = lax.all_to_all(message, SP[1:], 0, 0, tiled=True)  10.6 us
    all_to_all x1, blocking collectives, local(): lax.all_to_all(prefixes, SP[1:], 0, 0, tiled=True).reshape(512, LANES)  8.49 us
    pallas_call x2, Pallas kernels, finish(): pl.pallas_call(functools.partial(finish_kernel, first=first), out_shape=o...  7.51 us
    pallas_call x1, Pallas kernels, local(): pl.pallas_call(functools.partial(far_mixer_kernel, ups=ups, downs=downs),...  7.05 us
  transfers between devices with their start and end apart: 17, of which 7 were waited for; matrix products, arithmetic and copies ran while one was open for 0% of the time, Pallas kernels for 20%

profile of v6, /device:TPU:32, one launch (start us, length us, event | category | flops | bytes accessed | tf_op | source)
XLA Modules:
  0.0 149.9 jit_solution(4215818859582704968)
XLA Ops:
  6.5 1.7 %pad_maximum_fusion = bf16[64,2048]{1,0:T(8,128)(2,1)} fusion(bf16[32,2048]{1,0:T(8,128)(2,1)} %bitcast.14, bf16[32,2048]{1,0:T(8,128)(2,1)} %param.34), kind=kLoop, calls=%fused_computation | loop fusion | flops 524288 | bytes 524288 | tf_op jit(solution)/shard_map/concatenate | solution.py:467
  8.3 6.2 %states.1 = (f32[4,512,128]{2,1,0:T(8,128)S(1)}, f32[4,8,128]{2,1,0:T(8,128)S(1)}, bf16[8,80,128]{2,1,0:T(8,128)(2,1)S(1)}, f32[4,128,128]{2,1,0:T(8,128)S(1)}, ...) custom-call(s32[1]{0:T(128)} %bitcast.index_ref, ...), custom_call_target="tpu_custom_call" | custom-call | flops 60000000 | bytes 2500000 | tf_op jit(solution)/shard_map/states/pallas_call | solution.py:496
  14.5 10.6 %all_to_all.15.message_ref = bf16[8,80,128]{2,1,0:T(8,128)(2,1)S(1)} all-to-all(bf16[8,80,128]{2,1,0:T(8,128)(2,1)S(1)} %get-tuple-element.59), channel_id=1, replica_groups=mesh['sp_0'=8,'sp_1'=4,'sp_2'=2,'tp'=4] {'sp_1','sp_2'}, dimensions={0} | all-to-all | bytes 327680 | tf_op jit(solution)/shard_map/all_to_all | solution.py:537
  25.1 18.4 %all_to_all.16.planes_ref = bf16[8,80,128]{2,1,0:T(8,128)(2,1)S(1)} all-to-all(bf16[8,80,128]{2,1,0:T(8,128)(2,1)S(1)} %get-tuple-element.60), channel_id=1, replica_groups=mesh['sp_0'=8,'sp_1'=4,'sp_2'=2,'tp'=4] {'sp_0'}, dimensions={0} | all-to-all | bytes 327680 | tf_op jit(solution)/shard_map/all_to_all | solution.py:549
  43.5 8.5 %all_to_all.17 = bf16[8,64,128]{2,1,0:T(8,128)(2,1)S(1)} all-to-all(bf16[8,64,128]{2,1,0:T(8,128)(2,1)S(1)} %prefix.1), channel_id=1, replica_groups=mesh['sp_0'=8,'sp_1'=4,'sp_2'=2,'tp'=4] {'sp_1','sp_2'}, dimensions={0} | all-to-all | bytes 262144 | tf_op jit(solution)/shard_map/all_to_all | solution.py:560
  52.0 1.9 %finish_far.1 = (bf16[64,2048]{1,0:T(8,128)(2,1)S(1)}, bf16[64,2048]{1,0:T(8,128)(2,1)S(1)}) custom-call(s32[1]{0:T(128)} %bitcast.index_ref, s32[1]{0:T(128)} %bitcast.1._.turn_ref, bf16[512,384]{1,0:T(8,128)(2,1)S(1)} %get-tuple-element.44.wq_ref, bf16[512,384]{1,0:T(8,128)(2,1)S(1)} %get-tuple-element.45.wk_ref, ...), custom_call_target="tpu_custom_call" | custom-call | flops 350000000 | bytes 4500000 | tf_op jit(solution)/shard_map/finish_far/pallas_call | solution.py:564
  53.9 1.7 %collective-permute-start = (bf16[64,2048]{1,0:T(8,128)(2,1)S(1)}, bf16[64,2048]{1,0:T(8,128)(2,1)S(1)}, u32[]{:S(2)}, u32[]{:S(2)}) collective-permute-start(bf16[64,2048]{1,0:T(8,128)(2,1)S(1)} %get-tuple-element.65), channel_id=1, source_target_pairs={{0,1},{1,2},{2,3},{3,0},{4,5},{5,6},{6,7},{7,4},{8,9},{9,10},{10,1... | collective-permute-start | bytes 786440 | tf_op jit(solution)/shard_map/ppermute | solution.py:427
  57.2 5.6 %finish.1.minus_ref.plus_ref.own_ref = bf16[3,128,2048]{2,1,0:T(8,128)(2,1)S(1)} custom-call(s32[1]{0:T(128)} %bitcast.index_ref, s32[1]{0:T(128)} %bitcast.1._.turn_ref, bf16[512,384]{1,0:T(8,128)(2,1)S(1)} %get-tuple-element.44.wq_ref, bf16[512,384]{1,0:T(8,128)(2,1)S(1)} %get-tuple-element.45.wk_ref, bf16[512,384]{1,0:T(8,128)(2,1)S(1)} %get-tuple-element.46.wv_ref, ...), custom_call_target="tpu_custom_call" | custom-call | flops 1050000000 | bytes 7500000 | tf_op jit(solution)/shard_map/finish/pallas_call | solution.py:564
  63.4 1.7 %collective-permute-start.2 = (bf16[128,2048]{1,0:T(8,128)(2,1)S(1)}, bf16[128,2048]{1,0:T(8,128)(2,1)S(1)}, u32[]{:S(2)}, u32[]{:S(2)}) collective-permute-start(bf16[128,2048]{1,0:T(8,128)(2,1)S(1)} %get-tuple-element.67), channel_id=1, source_target_pairs={{0,1},{1,2},{2,3},{3,0},{4,5},{5,6},{6,7},{7,4},{8,9},{9,10},{10,1... | collective-permute-start | bytes 1572872 | tf_op jit(solution)/shard_map/ppermute | solution.py:427
  65.0 1.7 %collective-permute-start.3 = (bf16[128,2048]{1,0:T(8,128)(2,1)S(1)}, bf16[128,2048]{1,0:T(8,128)(2,1)S(1)}, u32[]{:S(2)}, u32[]{:S(2)}) collective-permute-start(bf16[128,2048]{1,0:T(8,128)(2,1)S(1)} %get-tuple-element.68), channel_id=1, source_target_pairs={{0,3},{1,0},{2,1},{3,2},{4,7},{5,4},{6,5},{7,6},{8,11},{9,8},{10,9... | collective-permute-start | bytes 1572872 | tf_op jit(solution)/shard_map/ppermute | solution.py:427
  66.7 10.8 %collective-permute-done.2.below_ref = bf16[128,2048]{1,0:T(8,128)(2,1)S(1)} collective-permute-done((bf16[128,2048]{1,0:T(8,128)(2,1)S(1)}, bf16[128,2048]{1,0:T(8,128)(2,1)S(1)}, u32[]{:S(2)}, u32[]{:S(2)}) %collective-permute-start.2) | collective-permute-done | bytes 524320 | tf_op jit(solution)/shard_map/ppermute | solution.py:427
  79.4 2.3 %collective-permute-start.7 = (bf16[64,2048]{1,0:T(8,128)(2,1)S(1)}, bf16[64,2048]{1,0:T(8,128)(2,1)S(1)}, u32[]{:S(2)}, u32[]{:S(2)}) collective-permute-start(bf16[64,2048]{1,0:T(8,128)(2,1)S(1)} %get-tuple-element.70.second_ref), channel_id=1, source_target_pairs={{0,3},{1,0},{2,1},{3,2},{4,7},{5,4},{6,5},{7,6},{8,11},{9,8},{10,9... | collective-permute-start | bytes 786440 | tf_op jit(solution)/shard_map/ppermute | solution.py:427
  81.7 4.5 %collective-permute-done.4.refs_0_ = bf16[64,2048]{1,0:T(8,128)(2,1)S(1)} collective-permute-done((bf16[64,2048]{1,0:T(8,128)(2,1)S(1)}, bf16[64,2048]{1,0:T(8,128)(2,1)S(1)}, u32[]{:S(2)}, u32[]{:S(2)}) %collective-permute-start.4) | collective-permute-done | bytes 262176 | tf_op jit(solution)/shard_map/ppermute | solution.py:427
  86.2 3.2 %collective-permute-start.9 = (bf16[64,2048]{1,0:T(8,128)(2,1)S(1)}, bf16[64,2048]{1,0:T(8,128)(2,1)S(1)}, u32[]{:S(2)}, u32[]{:S(2)}) collective-permute-start(bf16[64,2048]{1,0:T(8,128)(2,1)S(1)} %collective-permute-done.7.refs_3_), channel_id=1, source_target_pairs={{0,3},{1,0},{2,1},{3,2},{4,7},{5,4},{6,5},{7,6},{8,11},{9,8},{10,9... | collective-permute-start | bytes 786440 | tf_op jit(solution)/shard_map/ppermute | solution.py:427
  89.4 3.2 %collective-permute-start.6 = (bf16[64,2048]{1,0:T(8,128)(2,1)S(1)}, bf16[64,2048]{1,0:T(8,128)(2,1)S(1)}, u32[]{:S(2)}, u32[]{:S(2)}) collective-permute-start(bf16[64,2048]{1,0:T(8,128)(2,1)S(1)} %get-tuple-element.78.first_ref), channel_id=1, source_target_pairs={{0,3},{1,0},{2,1},{3,2},{4,7},{5,4},{6,5},{7,6},{8,11},{9,8},{10,9... | collective-permute-start | bytes 786440 | tf_op jit(solution)/shard_map/ppermute | solution.py:427
  92.7 3.3 %collective-permute-done.8.refs_0_ = bf16[64,2048]{1,0:T(8,128)(2,1)S(1)} collective-permute-done((bf16[64,2048]{1,0:T(8,128)(2,1)S(1)}, bf16[64,2048]{1,0:T(8,128)(2,1)S(1)}, u32[]{:S(2)}, u32[]{:S(2)}) %collective-permute-start.8) | collective-permute-done | bytes 262176 | tf_op jit(solution)/shard_map/ppermute | solution.py:427
  95.9 16.0 %all-gather.2.cloned.1.call-done = bf16[4096,2048]{1,0:T(8,128)(2,1)} async-done(((bf16[64,2048]{1,0:T(8,128)(2,1)}), bf16[4096,2048]{1,0:T(8,128)(2,1)}) %all-gather.2.cloned.1.call-update) | async-done | bytes 16777232 | tf_op jit(solution)/shard_map/all_gather | solution.py:466
  112.0 7.1 %mixer_far.1 = (bf16[64,32,2048]{2,1,0:T(8,128)(2,1)S(1)}, bf16[64,32,2048]{2,1,0:T(8,128)(2,1)S(1)}, bf16[1024,128]{1,0:T(8,128)(2,1)S(1)}, bf16[1024,128]{1,0:T(8,128)(2,1)S(1)}) custom-call(bf16[64,2048]{1,0:T(8,128)(2,1)S(1)} %collective-permute-done.8.refs_0_, bf16[64,2048]{1,0:T(8,128)(2,1)S(1)} %collective-permute-done.9.refs_1_, ...), custom_call_target="tpu_custom_call" | custom-call | flops 2147483648 | bytes 20000000 | tf_op jit(solution)/shard_map/mixer_far/pallas_call | solution.py:629
  120.6 1.8 %collective-permute-start.11 = (bf16[1024,128]{1,0:T(8,128)(2,1)S(1)}, bf16[1024,128]{1,0:T(8,128)(2,1)S(1)}, u32[]{:S(2)}, u32[]{:S(2)}) collective-permute-start(bf16[1024,128]{1,0:T(8,128)(2,1)S(1)} %get-tuple-element.76), channel_id=1, source_target_pairs={{0,3},{1,0},{2,1},{3,2},{4,7},{5,4},{6,5},{7,6},{8,11},{9,8},{10,9... | collective-permute-start | bytes 786440 | tf_op jit(solution)/shard_map/ppermute | solution.py:427
  122.4 4.5 %mixer_near.1 = (bf16[1024,128]{1,0:T(8,128)(2,1)S(1)}, bf16[1024,128]{1,0:T(8,128)(2,1)S(1)}, bf16[1024,128]{1,0:T(8,128)(2,1)S(1)}, bf16[1024,128]{1,0:T(8,128)(2,1)S(1)}) custom-call(bf16[64,2048]{1,0:T(8,128)(2,1)S(1)} %collective-permute-done.4.refs_0_, bf16[64,2048]{1,0:T(8,128)(2,1)S(1)} %collective-permute-done.5.refs_1_, ...), custom_call_target="tpu_custom_call" | custom-call | flops 4294967296 | bytes 2000000 | tf_op jit(solution)/shard_map/mixer_near/pallas_call | solution.py:642
  127.2 3.0 %collective-permute-start.14 = (bf16[1024,128]{1,0:T(8,128)(2,1)S(1)}, bf16[1024,128]{1,0:T(8,128)(2,1)S(1)}, u32[]{:S(2)}, u32[]{:S(2)}) collective-permute-start(bf16[1024,128]{1,0:T(8,128)(2,1)S(1)} %get-tuple-element.80), channel_id=1, source_target_pairs={{0,3},{1,0},{2,1},{3,2},{4,7},{5,4},{6,5},{7,6},{8,11},{9,8},{10,9... | collective-permute-start | bytes 786440 | tf_op jit(solution)/shard_map/ppermute | solution.py:427
  130.5 3.2 %collective-permute-start.15 = (bf16[1024,128]{1,0:T(8,128)(2,1)S(1)}, bf16[1024,128]{1,0:T(8,128)(2,1)S(1)}, u32[]{:S(2)}, u32[]{:S(2)}) collective-permute-start(bf16[1024,128]{1,0:T(8,128)(2,1)S(1)} %get-tuple-element.81), channel_id=1, source_target_pairs={{0,3},{1,0},{2,1},{3,2},{4,7},{5,4},{6,5},{7,6},{8,11},{9,8},{10,9... | collective-permute-start | bytes 786440 | tf_op jit(solution)/shard_map/ppermute | solution.py:427
  133.6 3.5 %mixer_own.1.own_ref = bf16[2048,128]{1,0:T(8,128)(2,1)S(1)} custom-call(bf16[64,2048]{1,0:T(8,128)(2,1)S(1)} %get-tuple-element.78.first_ref, bf16[64,2048]{1,0:T(8,128)(2,1)S(1)} %get-tuple-element.70.second_ref, bf16[64,32,2048]{2,1,0:T(8,128)(2,1)S(1)} %get-tuple-element.71.refs_4_.up_ref, bf16[64,32,2048]{2,1,0:T(8,128)(2,1)S(1)} %get-tuple-element.72.refs_5_.down_ref), custom_call_target="tpu_custom_call" | custom-call | flops 2147483648 | bytes 2000000 | tf_op jit(solution)/shard_map/mixer_own/pallas_call | solution.py:666
  137.3 4.3 %collective-permute-done.12.below_low_ref = bf16[1024,128]{1,0:T(8,128)(2,1)S(1)} collective-permute-done((bf16[1024,128]{1,0:T(8,128)(2,1)S(1)}, bf16[1024,128]{1,0:T(8,128)(2,1)S(1)}, u32[]{:S(2)}, u32[]{:S(2)}) %collective-permute-start.12) | collective-permute-done | bytes 262176 | tf_op jit(solution)/shard_map/ppermute | solution.py:427
  (35 shorter events, 8.0 us)
Async XLA Ops:
  6.5 105.5 %all-gather.2.cloned.1.call-start = ((), (), s32[]{:S(2)}) async-start(), calls=%async_computation.3 | async-start | bytes 17039360 | tf_op jit(solution)/shard_map/all_gather | solution.py:466
  52.0 25.5 %copy-start = (bf16[128,2048]{1,0:T(8,128)(2,1)S(1)}, bf16[128,2048]{1,0:T(8,128)(2,1)}, u32[]{:S(2)}) copy-start(bf16[128,2048]{1,0:T(8,128)(2,1)} %residual_ref.1) | copy-start | bytes 1572868
  52.0 25.5 %copy-start.1 = (f32[2048]{0:T(1024)S(1)}, f32[2048]{0:T(1024)}, u32[]{:S(2)}) copy-start(f32[2048]{0:T(1024)} %param.36) | copy-start | bytes 24580
  52.0 25.5 %copy-start.2 = (f32[2048]{0:T(1024)S(1)}, f32[2048]{0:T(1024)}, u32[]{:S(2)}) copy-start(f32[2048]{0:T(1024)} %param.37) | copy-start | bytes 24580
  53.9 9.3 %collective-permute-start = (bf16[64,2048]{1,0:T(8,128)(2,1)S(1)}, bf16[64,2048]{1,0:T(8,128)(2,1)S(1)}, u32[]{:S(2)}, u32[]{:S(2)}) collective-permute-start(bf16[64,2048]{1,0:T(8,128)(2,1)S(1)} %get-tuple-element.65), channel_id=1, source_target_pairs={{0,1},{1,2},{2,3},{3,0},{4,5},{5,6},{6,7},{7,4},{8,9},{9,10},{10,1... | collective-permute-start | bytes 786440 | tf_op jit(solution)/shard_map/ppermute | solution.py:427
  55.6 7.6 %collective-permute-start.1 = (bf16[64,2048]{1,0:T(8,128)(2,1)S(1)}, bf16[64,2048]{1,0:T(8,128)(2,1)S(1)}, u32[]{:S(2)}, u32[]{:S(2)}) collective-permute-start(bf16[64,2048]{1,0:T(8,128)(2,1)S(1)} %get-tuple-element.66), channel_id=1, source_target_pairs={{0,3},{1,0},{2,1},{3,2},{4,7},{5,4},{6,5},{7,6},{8,11},{9,8},{10,9... | collective-permute-start | bytes 786440 | tf_op jit(solution)/shard_map/ppermute | solution.py:427
  63.4 14.1 %collective-permute-start.2 = (bf16[128,2048]{1,0:T(8,128)(2,1)S(1)}, bf16[128,2048]{1,0:T(8,128)(2,1)S(1)}, u32[]{:S(2)}, u32[]{:S(2)}) collective-permute-start(bf16[128,2048]{1,0:T(8,128)(2,1)S(1)} %get-tuple-element.67), channel_id=1, source_target_pairs={{0,1},{1,2},{2,3},{3,0},{4,5},{5,6},{6,7},{7,4},{8,9},{9,10},{10,1... | collective-permute-start | bytes 1572872 | tf_op jit(solution)/shard_map/ppermute | solution.py:427
  65.0 12.5 %collective-permute-start.3 = (bf16[128,2048]{1,0:T(8,128)(2,1)S(1)}, bf16[128,2048]{1,0:T(8,128)(2,1)S(1)}, u32[]{:S(2)}, u32[]{:S(2)}) collective-permute-start(bf16[128,2048]{1,0:T(8,128)(2,1)S(1)} %get-tuple-element.68), channel_id=1, source_target_pairs={{0,3},{1,0},{2,1},{3,2},{4,7},{5,4},{6,5},{7,6},{8,11},{9,8},{10,9... | collective-permute-start | bytes 1572872 | tf_op jit(solution)/shard_map/ppermute | solution.py:427
  78.4 7.8 %collective-permute-start.4 = (bf16[64,2048]{1,0:T(8,128)(2,1)S(1)}, bf16[64,2048]{1,0:T(8,128)(2,1)S(1)}, u32[]{:S(2)}, u32[]{:S(2)}) collective-permute-start(bf16[64,2048]{1,0:T(8,128)(2,1)S(1)} %get-tuple-element.78.first_ref), channel_id=1, source_target_pairs={{0,1},{1,2},{2,3},{3,0},{4,5},{5,6},{6,7},{7,4},{8,9},{9,10},{10,1... | collective-permute-start | bytes 786440 | tf_op jit(solution)/shard_map/ppermute | solution.py:427
  79.4 6.8 %collective-permute-start.7 = (bf16[64,2048]{1,0:T(8,128)(2,1)S(1)}, bf16[64,2048]{1,0:T(8,128)(2,1)S(1)}, u32[]{:S(2)}, u32[]{:S(2)}) collective-permute-start(bf16[64,2048]{1,0:T(8,128)(2,1)S(1)} %get-tuple-element.70.second_ref), channel_id=1, source_target_pairs={{0,3},{1,0},{2,1},{3,2},{4,7},{5,4},{6,5},{7,6},{8,11},{9,8},{10,9... | collective-permute-start | bytes 786440 | tf_op jit(solution)/shard_map/ppermute | solution.py:427
  86.2 9.8 %collective-permute-start.8 = (bf16[64,2048]{1,0:T(8,128)(2,1)S(1)}, bf16[64,2048]{1,0:T(8,128)(2,1)S(1)}, u32[]{:S(2)}, u32[]{:S(2)}) collective-permute-start(bf16[64,2048]{1,0:T(8,128)(2,1)S(1)} %collective-permute-done.4.refs_0_), channel_id=1, source_target_pairs={{0,1},{1,2},{2,3},{3,0},{4,5},{5,6},{6,7},{7,4},{8,9},{9,10},{10,1... | collective-permute-start | bytes 786440 | tf_op jit(solution)/shard_map/ppermute | solution.py:427
  86.2 9.7 %collective-permute-start.9 = (bf16[64,2048]{1,0:T(8,128)(2,1)S(1)}, bf16[64,2048]{1,0:T(8,128)(2,1)S(1)}, u32[]{:S(2)}, u32[]{:S(2)}) collective-permute-start(bf16[64,2048]{1,0:T(8,128)(2,1)S(1)} %collective-permute-done.7.refs_3_), channel_id=1, source_target_pairs={{0,3},{1,0},{2,1},{3,2},{4,7},{5,4},{6,5},{7,6},{8,11},{9,8},{10,9... | collective-permute-start | bytes 786440 | tf_op jit(solution)/shard_map/ppermute | solution.py:427
  89.4 32.9 %collective-permute-start.5 = (bf16[64,2048]{1,0:T(8,128)(2,1)S(1)}, bf16[64,2048]{1,0:T(8,128)(2,1)S(1)}, u32[]{:S(2)}, u32[]{:S(2)}) collective-permute-start(bf16[64,2048]{1,0:T(8,128)(2,1)S(1)} %get-tuple-element.70.second_ref), channel_id=1, source_target_pairs={{0,1},{1,2},{2,3},{3,0},{4,5},{5,6},{6,7},{7,4},{8,9},{9,10},{10,1... | collective-permute-start | bytes 786440 | tf_op jit(solution)/shard_map/ppermute | solution.py:427
  89.4 32.9 %collective-permute-start.6 = (bf16[64,2048]{1,0:T(8,128)(2,1)S(1)}, bf16[64,2048]{1,0:T(8,128)(2,1)S(1)}, u32[]{:S(2)}, u32[]{:S(2)}) collective-permute-start(bf16[64,2048]{1,0:T(8,128)(2,1)S(1)} %get-tuple-element.78.first_ref), channel_id=1, source_target_pairs={{0,3},{1,0},{2,1},{3,2},{4,7},{5,4},{6,5},{7,6},{8,11},{9,8},{10,9... | collective-permute-start | bytes 786440 | tf_op jit(solution)/shard_map/ppermute | solution.py:427
  119.1 11.1 %collective-permute-start.10 = (bf16[1024,128]{1,0:T(8,128)(2,1)S(1)}, bf16[1024,128]{1,0:T(8,128)(2,1)S(1)}, u32[]{:S(2)}, u32[]{:S(2)}) collective-permute-start(bf16[1024,128]{1,0:T(8,128)(2,1)S(1)} %get-tuple-element.75), channel_id=1, source_target_pairs={{0,1},{1,2},{2,3},{3,0},{4,5},{5,6},{6,7},{7,4},{8,9},{9,10},{10,1... | collective-permute-start | bytes 786440 | tf_op jit(solution)/shard_map/ppermute | solution.py:427
  120.6 9.6 %collective-permute-start.11 = (bf16[1024,128]{1,0:T(8,128)(2,1)S(1)}, bf16[1024,128]{1,0:T(8,128)(2,1)S(1)}, u32[]{:S(2)}, u32[]{:S(2)}) collective-permute-start(bf16[1024,128]{1,0:T(8,128)(2,1)S(1)} %get-tuple-element.76), channel_id=1, source_target_pairs={{0,3},{1,0},{2,1},{3,2},{4,7},{5,4},{6,5},{7,6},{8,11},{9,8},{10,9... | collective-permute-start | bytes 786440 | tf_op jit(solution)/shard_map/ppermute | solution.py:427
  126.9 10.5 %collective-permute-start.13 = (bf16[1024,128]{1,0:T(8,128)(2,1)S(1)}, bf16[1024,128]{1,0:T(8,128)(2,1)S(1)}, u32[]{:S(2)}, u32[]{:S(2)}) collective-permute-start(bf16[1024,128]{1,0:T(8,128)(2,1)S(1)} %get-tuple-element.79), channel_id=1, source_target_pairs={{0,1},{1,2},{2,3},{3,0},{4,5},{5,6},{6,7},{7,4},{8,9},{9,10},{10,1... | collective-permute-start | bytes 786440 | tf_op jit(solution)/shard_map/ppermute | solution.py:427
  127.2 10.1 %collective-permute-start.14 = (bf16[1024,128]{1,0:T(8,128)(2,1)S(1)}, bf16[1024,128]{1,0:T(8,128)(2,1)S(1)}, u32[]{:S(2)}, u32[]{:S(2)}) collective-permute-start(bf16[1024,128]{1,0:T(8,128)(2,1)S(1)} %get-tuple-element.80), channel_id=1, source_target_pairs={{0,3},{1,0},{2,1},{3,2},{4,7},{5,4},{6,5},{7,6},{8,11},{9,8},{10,9... | collective-permute-start | bytes 786440 | tf_op jit(solution)/shard_map/ppermute | solution.py:427
  130.3 11.4 %collective-permute-start.12 = (bf16[1024,128]{1,0:T(8,128)(2,1)S(1)}, bf16[1024,128]{1,0:T(8,128)(2,1)S(1)}, u32[]{:S(2)}, u32[]{:S(2)}) collective-permute-start(bf16[1024,128]{1,0:T(8,128)(2,1)S(1)} %get-tuple-element.77), channel_id=1, source_target_pairs={{0,1},{1,2},{2,3},{3,0},{4,5},{5,6},{6,7},{7,4},{8,9},{9,10},{10,1... | collective-permute-start | bytes 786440 | tf_op jit(solution)/shard_map/ppermute | solution.py:427
  130.5 11.2 %copy-start.3 = (f32[2048]{0:T(1024)S(1)}, f32[2048]{0:T(1024)}, u32[]{:S(2)}) copy-start(f32[2048]{0:T(1024)} %param.38) | copy-start | bytes 24580
  130.5 11.2 %collective-permute-start.15 = (bf16[1024,128]{1,0:T(8,128)(2,1)S(1)}, bf16[1024,128]{1,0:T(8,128)(2,1)S(1)}, u32[]{:S(2)}, u32[]{:S(2)}) collective-permute-start(bf16[1024,128]{1,0:T(8,128)(2,1)S(1)} %get-tuple-element.81), channel_id=1, source_target_pairs={{0,3},{1,0},{2,1},{3,2},{4,7},{5,4},{6,5},{7,6},{8,11},{9,8},{10,9... | collective-permute-start | bytes 786440 | tf_op jit(solution)/shard_map/ppermute | solution.py:427
Sparse Core Ops, SparseCore 0:
  10.1 101.8 all-gather.1

commit v7 on v6

--- a/solution.py
+++ b/solution.py
@@ -317,8 +317,10 @@
             (slice(half, 2 * half), below_high_ref, above_high_ref),
         )
     ]
-    lowered = jnp.concatenate(lowered, axis=0).T
-    out_ref[...] = (updated_ref[...].astype(F32) + rms(lowered, gain_ref[...])).astype(BF16)
+    lowered = jnp.concatenate(lowered, axis=0)
+    scale = lax.rsqrt(jnp.mean(lowered * lowered, axis=0, keepdims=True) + EPS)
+    scaled = (lowered * scale).astype(BF16).T.astype(F32)
+    out_ref[...] = (updated_ref[...].astype(F32) + scaled * gain_ref[...]).astype(BF16)
 
 
 def up_block(x_ref, up_ref, at, block):
@@ -334,17 +336,18 @@
 
 def far_mixer_kernel(*refs, ups, downs):
     halves, refs = refs[:2], refs[2:]
-    both_ref, up_ref, down_ref, low_ref, high_ref, x_ref, hidden_ref, sems = refs
+    both_ref, up_ref, down_ref, low_ref, high_ref, x_ref, hidden_ref, total_ref, sems = refs
     devices, share, units = up_ref.shape
     half = halves[0].shape[0]
-    block = units // ups
+    band = devices // ups
+    block = band * share
     group = devices // downs
     lines = group * share
 
     def up_copy(k):
-        at = pl.multiple_of(k * block, block)
+        at = k * band
         return pltpu.make_async_copy(
-            both_ref.at[:, 0, :, pl.ds(at, block)], up_ref.at[:, :, pl.ds(at, block)], sems.at[k]
+            both_ref.at[pl.ds(at, band), 0], up_ref.at[pl.ds(at, band)], sems.at[k]
         )
 
     def down_copy(k):
@@ -360,11 +363,13 @@
     for k, ref in enumerate(halves):
         x_ref[k * half : (k + 1) * half] = ref[...]
 
-    @pl.loop(0, ups)
-    def _(k):
+    for k in range(ups):
         up_copy(k).wait()
-        at = pl.multiple_of(k * block, block)
-        hidden_ref[pl.ds(at, block), :] = up_block(x_ref, up_ref, at, block)
+        weight = up_ref[k * band : (k + 1) * band].reshape(block, units)
+        part = mm(x_ref[:, k * block : (k + 1) * block], weight)
+        total_ref[...] = part if k == 0 else total_ref[...] + part
+    rectified = jnp.maximum(total_ref[...], 0.0)
+    hidden_ref[...] = (rectified * rectified).astype(BF16).T
 
     def lower(k, far_ref, base):
         down_copy(k).wait()
@@ -631,7 +636,9 @@
         out_shape=(weights, weights, turned_half, turned_half),
         in_specs=[*([whole] * 2), pl.BlockSpec(memory_space=pltpu.HBM)],
         out_specs=[whole] * 4,
-        scratch_shapes=[*scratch_half, pltpu.SemaphoreType.DMA((ups + downs,))],
+        scratch_shapes=[
+            *scratch_half, pltpu.VMEM((rows, units), F32), pltpu.SemaphoreType.DMA((ups + downs,)),
+        ],
         compiler_params=SMALL,
         name="mixer_far",
         cost_estimate=pl.CostEstimate(

time: 152 us -> 152 us (level)
  no operation moved by 1% of the time
where the time goes in v7:
time: 152 us; the launch traced here: 150 us
  waiting for transfers between devices  39.5 us (26%)
  blocking collectives  37.4 us (25%)
  Pallas kernels  31.3 us (21%)
  starting transfers between devices  26.4 us (17%)
  between operations  13.5 us (9%)
  other arithmetic  1.69 us (1%)
    ppermute x16, starting transfers between devices, shifted(): lax.ppermute(array, axis, [(k, (k + by) % size) for k in range(size)])  26.4 us
    ppermute x16, waiting for transfers between devices, shifted(): lax.ppermute(array, axis, [(k, (k + by) % size) for k in range(size)])  23.5 us
    all_to_all x1, blocking collectives, local(): planes = lax.all_to_all(planes, SP[0], 0, 0, tiled=True)  18.4 us
    all_gather x1, waiting for transfers between devices, local(): lax.all_gather(jnp.concatenate([up_weight, down_weight.T], axis=0), SP, a...  16 us
    all_to_all x1, blocking collectives, local(): arrived = lax.all_to_all(message, SP[1:], 0, 0, tiled=True)  10.6 us
    all_to_all x1, blocking collectives, local(): lax.all_to_all(prefixes, SP[1:], 0, 0, tiled=True).reshape(512, LANES)  8.49 us
    pallas_call x2, Pallas kernels, finish(): pl.pallas_call(functools.partial(finish_kernel, first=first), out_shape=o...  7.51 us
    pallas_call x1, Pallas kernels, local(): pl.pallas_call(functools.partial(far_mixer_kernel, ups=ups, downs=downs),...  6.98 us
  transfers between devices with their start and end apart: 17, of which 7 were waited for; matrix products, arithmetic and copies ran while one was open for 0% of the time, Pallas kernels for 20%

profile of v7, /device:TPU:32, one launch (start us, length us, event | category | flops | bytes accessed | tf_op | source)
XLA Modules:
  0.0 149.8 jit_solution(18150894923366676614)
XLA Ops:
  6.5 1.7 %pad_maximum_fusion = bf16[64,2048]{1,0:T(8,128)(2,1)} fusion(bf16[32,2048]{1,0:T(8,128)(2,1)} %bitcast.14, bf16[32,2048]{1,0:T(8,128)(2,1)} %param.34), kind=kLoop, calls=%fused_computation | loop fusion | flops 524288 | bytes 524288 | tf_op jit(solution)/shard_map/concatenate | solution.py:472
  8.3 6.2 %states.1 = (f32[4,512,128]{2,1,0:T(8,128)S(1)}, f32[4,8,128]{2,1,0:T(8,128)S(1)}, bf16[8,80,128]{2,1,0:T(8,128)(2,1)S(1)}, f32[4,128,128]{2,1,0:T(8,128)S(1)}, ...) custom-call(s32[1]{0:T(128)} %bitcast.index_ref, ...), custom_call_target="tpu_custom_call" | custom-call | flops 60000000 | bytes 2500000 | tf_op jit(solution)/shard_map/states/pallas_call | solution.py:501
  14.5 10.6 %all_to_all.15.message_ref = bf16[8,80,128]{2,1,0:T(8,128)(2,1)S(1)} all-to-all(bf16[8,80,128]{2,1,0:T(8,128)(2,1)S(1)} %get-tuple-element.59), channel_id=1, replica_groups=mesh['sp_0'=8,'sp_1'=4,'sp_2'=2,'tp'=4] {'sp_1','sp_2'}, dimensions={0} | all-to-all | bytes 327680 | tf_op jit(solution)/shard_map/all_to_all | solution.py:542
  25.1 18.4 %all_to_all.16.planes_ref = bf16[8,80,128]{2,1,0:T(8,128)(2,1)S(1)} all-to-all(bf16[8,80,128]{2,1,0:T(8,128)(2,1)S(1)} %get-tuple-element.60), channel_id=1, replica_groups=mesh['sp_0'=8,'sp_1'=4,'sp_2'=2,'tp'=4] {'sp_0'}, dimensions={0} | all-to-all | bytes 327680 | tf_op jit(solution)/shard_map/all_to_all | solution.py:554
  43.5 8.5 %all_to_all.17 = bf16[8,64,128]{2,1,0:T(8,128)(2,1)S(1)} all-to-all(bf16[8,64,128]{2,1,0:T(8,128)(2,1)S(1)} %prefix.1), channel_id=1, replica_groups=mesh['sp_0'=8,'sp_1'=4,'sp_2'=2,'tp'=4] {'sp_1','sp_2'}, dimensions={0} | all-to-all | bytes 262144 | tf_op jit(solution)/shard_map/all_to_all | solution.py:565
  52.0 1.9 %finish_far.1 = (bf16[64,2048]{1,0:T(8,128)(2,1)S(1)}, bf16[64,2048]{1,0:T(8,128)(2,1)S(1)}) custom-call(s32[1]{0:T(128)} %bitcast.index_ref, s32[1]{0:T(128)} %bitcast.1._.turn_ref, bf16[512,384]{1,0:T(8,128)(2,1)S(1)} %get-tuple-element.44.wq_ref, bf16[512,384]{1,0:T(8,128)(2,1)S(1)} %get-tuple-element.45.wk_ref, ...), custom_call_target="tpu_custom_call" | custom-call | flops 350000000 | bytes 4500000 | tf_op jit(solution)/shard_map/finish_far/pallas_call | solution.py:569
  53.9 1.7 %collective-permute-start = (bf16[64,2048]{1,0:T(8,128)(2,1)S(1)}, bf16[64,2048]{1,0:T(8,128)(2,1)S(1)}, u32[]{:S(2)}, u32[]{:S(2)}) collective-permute-start(bf16[64,2048]{1,0:T(8,128)(2,1)S(1)} %get-tuple-element.65), channel_id=1, source_target_pairs={{0,1},{1,2},{2,3},{3,0},{4,5},{5,6},{6,7},{7,4},{8,9},{9,10},{10,1... | collective-permute-start | bytes 786440 | tf_op jit(solution)/shard_map/ppermute | solution.py:432
  57.2 5.6 %finish.1.minus_ref.plus_ref.own_ref = bf16[3,128,2048]{2,1,0:T(8,128)(2,1)S(1)} custom-call(s32[1]{0:T(128)} %bitcast.index_ref, s32[1]{0:T(128)} %bitcast.1._.turn_ref, bf16[512,384]{1,0:T(8,128)(2,1)S(1)} %get-tuple-element.44.wq_ref, bf16[512,384]{1,0:T(8,128)(2,1)S(1)} %get-tuple-element.45.wk_ref, bf16[512,384]{1,0:T(8,128)(2,1)S(1)} %get-tuple-element.46.wv_ref, ...), custom_call_target="tpu_custom_call" | custom-call | flops 1050000000 | bytes 7500000 | tf_op jit(solution)/shard_map/finish/pallas_call | solution.py:569
  63.4 1.7 %collective-permute-start.2 = (bf16[128,2048]{1,0:T(8,128)(2,1)S(1)}, bf16[128,2048]{1,0:T(8,128)(2,1)S(1)}, u32[]{:S(2)}, u32[]{:S(2)}) collective-permute-start(bf16[128,2048]{1,0:T(8,128)(2,1)S(1)} %get-tuple-element.67), channel_id=1, source_target_pairs={{0,1},{1,2},{2,3},{3,0},{4,5},{5,6},{6,7},{7,4},{8,9},{9,10},{10,1... | collective-permute-start | bytes 1572872 | tf_op jit(solution)/shard_map/ppermute | solution.py:432
  65.0 1.7 %collective-permute-start.3 = (bf16[128,2048]{1,0:T(8,128)(2,1)S(1)}, bf16[128,2048]{1,0:T(8,128)(2,1)S(1)}, u32[]{:S(2)}, u32[]{:S(2)}) collective-permute-start(bf16[128,2048]{1,0:T(8,128)(2,1)S(1)} %get-tuple-element.68), channel_id=1, source_target_pairs={{0,3},{1,0},{2,1},{3,2},{4,7},{5,4},{6,5},{7,6},{8,11},{9,8},{10,9... | collective-permute-start | bytes 1572872 | tf_op jit(solution)/shard_map/ppermute | solution.py:432
  66.7 10.8 %collective-permute-done.2.below_ref = bf16[128,2048]{1,0:T(8,128)(2,1)S(1)} collective-permute-done((bf16[128,2048]{1,0:T(8,128)(2,1)S(1)}, bf16[128,2048]{1,0:T(8,128)(2,1)S(1)}, u32[]{:S(2)}, u32[]{:S(2)}) %collective-permute-start.2) | collective-permute-done | bytes 524320 | tf_op jit(solution)/shard_map/ppermute | solution.py:432
  79.4 2.3 %collective-permute-start.7 = (bf16[64,2048]{1,0:T(8,128)(2,1)S(1)}, bf16[64,2048]{1,0:T(8,128)(2,1)S(1)}, u32[]{:S(2)}, u32[]{:S(2)}) collective-permute-start(bf16[64,2048]{1,0:T(8,128)(2,1)S(1)} %get-tuple-element.70.second_ref), channel_id=1, source_target_pairs={{0,3},{1,0},{2,1},{3,2},{4,7},{5,4},{6,5},{7,6},{8,11},{9,8},{10,9... | collective-permute-start | bytes 786440 | tf_op jit(solution)/shard_map/ppermute | solution.py:432
  81.7 4.5 %collective-permute-done.4.refs_0_ = bf16[64,2048]{1,0:T(8,128)(2,1)S(1)} collective-permute-done((bf16[64,2048]{1,0:T(8,128)(2,1)S(1)}, bf16[64,2048]{1,0:T(8,128)(2,1)S(1)}, u32[]{:S(2)}, u32[]{:S(2)}) %collective-permute-start.4) | collective-permute-done | bytes 262176 | tf_op jit(solution)/shard_map/ppermute | solution.py:432
  86.2 3.2 %collective-permute-start.9 = (bf16[64,2048]{1,0:T(8,128)(2,1)S(1)}, bf16[64,2048]{1,0:T(8,128)(2,1)S(1)}, u32[]{:S(2)}, u32[]{:S(2)}) collective-permute-start(bf16[64,2048]{1,0:T(8,128)(2,1)S(1)} %collective-permute-done.7.refs_3_), channel_id=1, source_target_pairs={{0,3},{1,0},{2,1},{3,2},{4,7},{5,4},{6,5},{7,6},{8,11},{9,8},{10,9... | collective-permute-start | bytes 786440 | tf_op jit(solution)/shard_map/ppermute | solution.py:432
  89.4 3.2 %collective-permute-start.6 = (bf16[64,2048]{1,0:T(8,128)(2,1)S(1)}, bf16[64,2048]{1,0:T(8,128)(2,1)S(1)}, u32[]{:S(2)}, u32[]{:S(2)}) collective-permute-start(bf16[64,2048]{1,0:T(8,128)(2,1)S(1)} %get-tuple-element.78.first_ref), channel_id=1, source_target_pairs={{0,3},{1,0},{2,1},{3,2},{4,7},{5,4},{6,5},{7,6},{8,11},{9,8},{10,9... | collective-permute-start | bytes 786440 | tf_op jit(solution)/shard_map/ppermute | solution.py:432
  92.7 3.3 %collective-permute-done.8.refs_0_ = bf16[64,2048]{1,0:T(8,128)(2,1)S(1)} collective-permute-done((bf16[64,2048]{1,0:T(8,128)(2,1)S(1)}, bf16[64,2048]{1,0:T(8,128)(2,1)S(1)}, u32[]{:S(2)}, u32[]{:S(2)}) %collective-permute-start.8) | collective-permute-done | bytes 262176 | tf_op jit(solution)/shard_map/ppermute | solution.py:432
  95.9 16.0 %all-gather.2.cloned.1.call-done = bf16[4096,2048]{1,0:T(8,128)(2,1)} async-done(((bf16[64,2048]{1,0:T(8,128)(2,1)}), bf16[4096,2048]{1,0:T(8,128)(2,1)}) %all-gather.2.cloned.1.call-update) | async-done | bytes 16777232 | tf_op jit(solution)/shard_map/all_gather | solution.py:471
  112.0 7.0 %mixer_far.1 = (bf16[64,32,2048]{2,1,0:T(8,128)(2,1)S(1)}, bf16[64,32,2048]{2,1,0:T(8,128)(2,1)S(1)}, bf16[1024,128]{1,0:T(8,128)(2,1)S(1)}, bf16[1024,128]{1,0:T(8,128)(2,1)S(1)}) custom-call(bf16[64,2048]{1,0:T(8,128)(2,1)S(1)} %collective-permute-done.8.refs_0_, bf16[64,2048]{1,0:T(8,128)(2,1)S(1)} %collective-permute-done.9.refs_1_, ...), custom_call_target="tpu_custom_call" | custom-call | flops 2147483648 | bytes 20000000 | tf_op jit(solution)/shard_map/mixer_far/pallas_call | solution.py:634
  120.5 1.8 %collective-permute-start.11 = (bf16[1024,128]{1,0:T(8,128)(2,1)S(1)}, bf16[1024,128]{1,0:T(8,128)(2,1)S(1)}, u32[]{:S(2)}, u32[]{:S(2)}) collective-permute-start(bf16[1024,128]{1,0:T(8,128)(2,1)S(1)} %get-tuple-element.76), channel_id=1, source_target_pairs={{0,3},{1,0},{2,1},{3,2},{4,7},{5,4},{6,5},{7,6},{8,11},{9,8},{10,9... | collective-permute-start | bytes 786440 | tf_op jit(solution)/shard_map/ppermute | solution.py:432
  122.3 4.5 %mixer_near.1 = (bf16[1024,128]{1,0:T(8,128)(2,1)S(1)}, bf16[1024,128]{1,0:T(8,128)(2,1)S(1)}, bf16[1024,128]{1,0:T(8,128)(2,1)S(1)}, bf16[1024,128]{1,0:T(8,128)(2,1)S(1)}) custom-call(bf16[64,2048]{1,0:T(8,128)(2,1)S(1)} %collective-permute-done.4.refs_0_, bf16[64,2048]{1,0:T(8,128)(2,1)S(1)} %collective-permute-done.5.refs_1_, ...), custom_call_target="tpu_custom_call" | custom-call | flops 4294967296 | bytes 2000000 | tf_op jit(solution)/shard_map/mixer_near/pallas_call | solution.py:649
  127.2 3.0 %collective-permute-start.14 = (bf16[1024,128]{1,0:T(8,128)(2,1)S(1)}, bf16[1024,128]{1,0:T(8,128)(2,1)S(1)}, u32[]{:S(2)}, u32[]{:S(2)}) collective-permute-start(bf16[1024,128]{1,0:T(8,128)(2,1)S(1)} %get-tuple-element.80), channel_id=1, source_target_pairs={{0,3},{1,0},{2,1},{3,2},{4,7},{5,4},{6,5},{7,6},{8,11},{9,8},{10,9... | collective-permute-start | bytes 786440 | tf_op jit(solution)/shard_map/ppermute | solution.py:432
  130.4 3.1 %collective-permute-start.15 = (bf16[1024,128]{1,0:T(8,128)(2,1)S(1)}, bf16[1024,128]{1,0:T(8,128)(2,1)S(1)}, u32[]{:S(2)}, u32[]{:S(2)}) collective-permute-start(bf16[1024,128]{1,0:T(8,128)(2,1)S(1)} %get-tuple-element.81), channel_id=1, source_target_pairs={{0,3},{1,0},{2,1},{3,2},{4,7},{5,4},{6,5},{7,6},{8,11},{9,8},{10,9... | collective-permute-start | bytes 786440 | tf_op jit(solution)/shard_map/ppermute | solution.py:432
  133.6 3.5 %mixer_own.1.own_ref = bf16[2048,128]{1,0:T(8,128)(2,1)S(1)} custom-call(bf16[64,2048]{1,0:T(8,128)(2,1)S(1)} %get-tuple-element.78.first_ref, bf16[64,2048]{1,0:T(8,128)(2,1)S(1)} %get-tuple-element.70.second_ref, bf16[64,32,2048]{2,1,0:T(8,128)(2,1)S(1)} %get-tuple-element.71.refs_4_.up_ref, bf16[64,32,2048]{2,1,0:T(8,128)(2,1)S(1)} %get-tuple-element.72.refs_5_.down_ref), custom_call_target="tpu_custom_call" | custom-call | flops 2147483648 | bytes 2000000 | tf_op jit(solution)/shard_map/mixer_own/pallas_call | solution.py:673
  137.3 4.3 %collective-permute-done.12.below_low_ref = bf16[1024,128]{1,0:T(8,128)(2,1)S(1)} collective-permute-done((bf16[1024,128]{1,0:T(8,128)(2,1)S(1)}, bf16[1024,128]{1,0:T(8,128)(2,1)S(1)}, u32[]{:S(2)}, u32[]{:S(2)}) %collective-permute-start.12) | collective-permute-done | bytes 262176 | tf_op jit(solution)/shard_map/ppermute | solution.py:432
  (35 shorter events, 7.9 us)
Async XLA Ops:
  6.5 105.5 %all-gather.2.cloned.1.call-start = ((), (), s32[]{:S(2)}) async-start(), calls=%async_computation.3 | async-start | bytes 17039360 | tf_op jit(solution)/shard_map/all_gather | solution.py:471
  52.0 25.5 %copy-start = (bf16[128,2048]{1,0:T(8,128)(2,1)S(1)}, bf16[128,2048]{1,0:T(8,128)(2,1)}, u32[]{:S(2)}) copy-start(bf16[128,2048]{1,0:T(8,128)(2,1)} %residual_ref.1) | copy-start | bytes 1572868
  52.0 25.5 %copy-start.1 = (f32[2048]{0:T(1024)S(1)}, f32[2048]{0:T(1024)}, u32[]{:S(2)}) copy-start(f32[2048]{0:T(1024)} %param.36) | copy-start | bytes 24580
  52.0 25.5 %copy-start.2 = (f32[2048]{0:T(1024)S(1)}, f32[2048]{0:T(1024)}, u32[]{:S(2)}) copy-start(f32[2048]{0:T(1024)} %param.37) | copy-start | bytes 24580
  53.9 9.3 %collective-permute-start = (bf16[64,2048]{1,0:T(8,128)(2,1)S(1)}, bf16[64,2048]{1,0:T(8,128)(2,1)S(1)}, u32[]{:S(2)}, u32[]{:S(2)}) collective-permute-start(bf16[64,2048]{1,0:T(8,128)(2,1)S(1)} %get-tuple-element.65), channel_id=1, source_target_pairs={{0,1},{1,2},{2,3},{3,0},{4,5},{5,6},{6,7},{7,4},{8,9},{9,10},{10,1... | collective-permute-start | bytes 786440 | tf_op jit(solution)/shard_map/ppermute | solution.py:432
  55.6 7.6 %collective-permute-start.1 = (bf16[64,2048]{1,0:T(8,128)(2,1)S(1)}, bf16[64,2048]{1,0:T(8,128)(2,1)S(1)}, u32[]{:S(2)}, u32[]{:S(2)}) collective-permute-start(bf16[64,2048]{1,0:T(8,128)(2,1)S(1)} %get-tuple-element.66), channel_id=1, source_target_pairs={{0,3},{1,0},{2,1},{3,2},{4,7},{5,4},{6,5},{7,6},{8,11},{9,8},{10,9... | collective-permute-start | bytes 786440 | tf_op jit(solution)/shard_map/ppermute | solution.py:432
  63.4 14.1 %collective-permute-start.2 = (bf16[128,2048]{1,0:T(8,128)(2,1)S(1)}, bf16[128,2048]{1,0:T(8,128)(2,1)S(1)}, u32[]{:S(2)}, u32[]{:S(2)}) collective-permute-start(bf16[128,2048]{1,0:T(8,128)(2,1)S(1)} %get-tuple-element.67), channel_id=1, source_target_pairs={{0,1},{1,2},{2,3},{3,0},{4,5},{5,6},{6,7},{7,4},{8,9},{9,10},{10,1... | collective-permute-start | bytes 1572872 | tf_op jit(solution)/shard_map/ppermute | solution.py:432
  65.0 12.5 %collective-permute-start.3 = (bf16[128,2048]{1,0:T(8,128)(2,1)S(1)}, bf16[128,2048]{1,0:T(8,128)(2,1)S(1)}, u32[]{:S(2)}, u32[]{:S(2)}) collective-permute-start(bf16[128,2048]{1,0:T(8,128)(2,1)S(1)} %get-tuple-element.68), channel_id=1, source_target_pairs={{0,3},{1,0},{2,1},{3,2},{4,7},{5,4},{6,5},{7,6},{8,11},{9,8},{10,9... | collective-permute-start | bytes 1572872 | tf_op jit(solution)/shard_map/ppermute | solution.py:432
  78.4 7.8 %collective-permute-start.4 = (bf16[64,2048]{1,0:T(8,128)(2,1)S(1)}, bf16[64,2048]{1,0:T(8,128)(2,1)S(1)}, u32[]{:S(2)}, u32[]{:S(2)}) collective-permute-start(bf16[64,2048]{1,0:T(8,128)(2,1)S(1)} %get-tuple-element.78.first_ref), channel_id=1, source_target_pairs={{0,1},{1,2},{2,3},{3,0},{4,5},{5,6},{6,7},{7,4},{8,9},{9,10},{10,1... | collective-permute-start | bytes 786440 | tf_op jit(solution)/shard_map/ppermute | solution.py:432
  79.4 6.8 %collective-permute-start.7 = (bf16[64,2048]{1,0:T(8,128)(2,1)S(1)}, bf16[64,2048]{1,0:T(8,128)(2,1)S(1)}, u32[]{:S(2)}, u32[]{:S(2)}) collective-permute-start(bf16[64,2048]{1,0:T(8,128)(2,1)S(1)} %get-tuple-element.70.second_ref), channel_id=1, source_target_pairs={{0,3},{1,0},{2,1},{3,2},{4,7},{5,4},{6,5},{7,6},{8,11},{9,8},{10,9... | collective-permute-start | bytes 786440 | tf_op jit(solution)/shard_map/ppermute | solution.py:432
  86.2 9.8 %collective-permute-start.8 = (bf16[64,2048]{1,0:T(8,128)(2,1)S(1)}, bf16[64,2048]{1,0:T(8,128)(2,1)S(1)}, u32[]{:S(2)}, u32[]{:S(2)}) collective-permute-start(bf16[64,2048]{1,0:T(8,128)(2,1)S(1)} %collective-permute-done.4.refs_0_), channel_id=1, source_target_pairs={{0,1},{1,2},{2,3},{3,0},{4,5},{5,6},{6,7},{7,4},{8,9},{9,10},{10,1... | collective-permute-start | bytes 786440 | tf_op jit(solution)/shard_map/ppermute | solution.py:432
  86.2 9.7 %collective-permute-start.9 = (bf16[64,2048]{1,0:T(8,128)(2,1)S(1)}, bf16[64,2048]{1,0:T(8,128)(2,1)S(1)}, u32[]{:S(2)}, u32[]{:S(2)}) collective-permute-start(bf16[64,2048]{1,0:T(8,128)(2,1)S(1)} %collective-permute-done.7.refs_3_), channel_id=1, source_target_pairs={{0,3},{1,0},{2,1},{3,2},{4,7},{5,4},{6,5},{7,6},{8,11},{9,8},{10,9... | collective-permute-start | bytes 786440 | tf_op jit(solution)/shard_map/ppermute | solution.py:432
  89.4 32.9 %collective-permute-start.5 = (bf16[64,2048]{1,0:T(8,128)(2,1)S(1)}, bf16[64,2048]{1,0:T(8,128)(2,1)S(1)}, u32[]{:S(2)}, u32[]{:S(2)}) collective-permute-start(bf16[64,2048]{1,0:T(8,128)(2,1)S(1)} %get-tuple-element.70.second_ref), channel_id=1, source_target_pairs={{0,1},{1,2},{2,3},{3,0},{4,5},{5,6},{6,7},{7,4},{8,9},{9,10},{10,1... | collective-permute-start | bytes 786440 | tf_op jit(solution)/shard_map/ppermute | solution.py:432
  89.4 32.9 %collective-permute-start.6 = (bf16[64,2048]{1,0:T(8,128)(2,1)S(1)}, bf16[64,2048]{1,0:T(8,128)(2,1)S(1)}, u32[]{:S(2)}, u32[]{:S(2)}) collective-permute-start(bf16[64,2048]{1,0:T(8,128)(2,1)S(1)} %get-tuple-element.78.first_ref), channel_id=1, source_target_pairs={{0,3},{1,0},{2,1},{3,2},{4,7},{5,4},{6,5},{7,6},{8,11},{9,8},{10,9... | collective-permute-start | bytes 786440 | tf_op jit(solution)/shard_map/ppermute | solution.py:432
  119.0 11.1 %collective-permute-start.10 = (bf16[1024,128]{1,0:T(8,128)(2,1)S(1)}, bf16[1024,128]{1,0:T(8,128)(2,1)S(1)}, u32[]{:S(2)}, u32[]{:S(2)}) collective-permute-start(bf16[1024,128]{1,0:T(8,128)(2,1)S(1)} %get-tuple-element.75), channel_id=1, source_target_pairs={{0,1},{1,2},{2,3},{3,0},{4,5},{5,6},{6,7},{7,4},{8,9},{9,10},{10,1... | collective-permute-start | bytes 786440 | tf_op jit(solution)/shard_map/ppermute | solution.py:432
  120.5 9.6 %collective-permute-start.11 = (bf16[1024,128]{1,0:T(8,128)(2,1)S(1)}, bf16[1024,128]{1,0:T(8,128)(2,1)S(1)}, u32[]{:S(2)}, u32[]{:S(2)}) collective-permute-start(bf16[1024,128]{1,0:T(8,128)(2,1)S(1)} %get-tuple-element.76), channel_id=1, source_target_pairs={{0,3},{1,0},{2,1},{3,2},{4,7},{5,4},{6,5},{7,6},{8,11},{9,8},{10,9... | collective-permute-start | bytes 786440 | tf_op jit(solution)/shard_map/ppermute | solution.py:432
  126.8 10.5 %collective-permute-start.13 = (bf16[1024,128]{1,0:T(8,128)(2,1)S(1)}, bf16[1024,128]{1,0:T(8,128)(2,1)S(1)}, u32[]{:S(2)}, u32[]{:S(2)}) collective-permute-start(bf16[1024,128]{1,0:T(8,128)(2,1)S(1)} %get-tuple-element.79), channel_id=1, source_target_pairs={{0,1},{1,2},{2,3},{3,0},{4,5},{5,6},{6,7},{7,4},{8,9},{9,10},{10,1... | collective-permute-start | bytes 786440 | tf_op jit(solution)/shard_map/ppermute | solution.py:432
  127.2 10.1 %collective-permute-start.14 = (bf16[1024,128]{1,0:T(8,128)(2,1)S(1)}, bf16[1024,128]{1,0:T(8,128)(2,1)S(1)}, u32[]{:S(2)}, u32[]{:S(2)}) collective-permute-start(bf16[1024,128]{1,0:T(8,128)(2,1)S(1)} %get-tuple-element.80), channel_id=1, source_target_pairs={{0,3},{1,0},{2,1},{3,2},{4,7},{5,4},{6,5},{7,6},{8,11},{9,8},{10,9... | collective-permute-start | bytes 786440 | tf_op jit(solution)/shard_map/ppermute | solution.py:432
  130.2 11.4 %collective-permute-start.12 = (bf16[1024,128]{1,0:T(8,128)(2,1)S(1)}, bf16[1024,128]{1,0:T(8,128)(2,1)S(1)}, u32[]{:S(2)}, u32[]{:S(2)}) collective-permute-start(bf16[1024,128]{1,0:T(8,128)(2,1)S(1)} %get-tuple-element.77), channel_id=1, source_target_pairs={{0,1},{1,2},{2,3},{3,0},{4,5},{5,6},{6,7},{7,4},{8,9},{9,10},{10,1... | collective-permute-start | bytes 786440 | tf_op jit(solution)/shard_map/ppermute | solution.py:432
  130.4 11.2 %copy-start.3 = (f32[2048]{0:T(1024)S(1)}, f32[2048]{0:T(1024)}, u32[]{:S(2)}) copy-start(f32[2048]{0:T(1024)} %param.38) | copy-start | bytes 24580
  130.4 11.2 %collective-permute-start.15 = (bf16[1024,128]{1,0:T(8,128)(2,1)S(1)}, bf16[1024,128]{1,0:T(8,128)(2,1)S(1)}, u32[]{:S(2)}, u32[]{:S(2)}) collective-permute-start(bf16[1024,128]{1,0:T(8,128)(2,1)S(1)} %get-tuple-element.81), channel_id=1, source_target_pairs={{0,3},{1,0},{2,1},{3,2},{4,7},{5,4},{6,5},{7,6},{8,11},{9,8},{10,9... | collective-permute-start | bytes 786440 | tf_op jit(solution)/shard_map/ppermute | solution.py:432
Sparse Core Ops, SparseCore 0:
  10.1 101.8 all-gather.1

commit v8 on v6

--- a/solution.py
+++ b/solution.py
@@ -109,7 +109,7 @@
 
 
 def log_rows(high, low):
-    sub = lax.broadcasted_iota(jnp.int32, (16, LANES), 0)
+    sub = lax.broadcasted_iota(jnp.int32, (8, LANES), 0)
     return jnp.where(sub == 0, high, jnp.where(sub == 1, low, 0.0)).astype(BF16)
 
 
@@ -164,7 +164,7 @@
         high, low = in_two(sums)
         for part, head in enumerate(SLICE_HEADS):
             message_ref[part, 0:64] = state_ref[part * 64 : part * 64 + 64, :].astype(BF16)
-            message_ref[part, 64:80] = log_rows(high[head : head + 1, :], low[head : head + 1, :])
+            message_ref[part, 64:72] = log_rows(high[head : head + 1, :], low[head : head + 1, :])
         for copy in copies:
             copy.wait()
 
@@ -182,7 +182,7 @@
     ends = log_rows(*in_two(logs))
     for k in range(8):
         out_ref[k, 0:64] = carried.astype(BF16)
-        out_ref[k, 64:80] = ends
+        out_ref[k, 64:72] = ends
 
 
 def prefix_kernel(index_ref, planes_ref, within_ref, logs_ref, out_ref):
@@ -498,7 +498,7 @@
         out_shape=(
             jax.ShapeDtypeStruct((SPANS, 512, LANES), F32),
             jax.ShapeDtypeStruct((SPANS, 8, LANES), F32),
-            jax.ShapeDtypeStruct((8, 80, LANES), BF16),
+            jax.ShapeDtypeStruct((8, 72, LANES), BF16),
             *(pltpu.VMEM(x.shape, x.dtype) for x in staged),
         ),
         grid_spec=pltpu.PrefetchScalarGridSpec(
@@ -510,7 +510,7 @@
             ],
             out_specs=[
                 *state_blocks,
-                pl.BlockSpec((8, 80, LANES), lambda s, i, t: (0, 0, 0)),
+                pl.BlockSpec((8, 72, LANES), lambda s, i, t: (0, 0, 0)),
                 *([pl.BlockSpec(memory_space=pltpu.VMEM)] * len(staged)),
             ],
             scratch_shapes=[
@@ -538,7 +538,7 @@
     planes, within, logs = pl.pallas_call(
         plane_kernel,
         out_shape=(
-            jax.ShapeDtypeStruct((8, 80, LANES), BF16),
+            jax.ShapeDtypeStruct((8, 72, LANES), BF16),
             jax.ShapeDtypeStruct((8, 64, LANES), F32),
             jax.ShapeDtypeStruct((8, 8, LANES), F32),
         ),

time: 152 us -> 152 us (level)
  no operation moved by 1% of the time
where the time goes in v8:
time: 152 us; the launch traced here: 150 us
  waiting for transfers between devices  39.9 us (26%)
  blocking collectives  36.6 us (24%)
  Pallas kernels  31.4 us (21%)
  starting transfers between devices  26.4 us (17%)
  between operations  13.5 us (9%)
  other arithmetic  1.69 us (1%)
    ppermute x16, starting transfers between devices, shifted(): lax.ppermute(array, axis, [(k, (k + by) % size) for k in range(size)])  26.4 us
    ppermute x16, waiting for transfers between devices, shifted(): lax.ppermute(array, axis, [(k, (k + by) % size) for k in range(size)])  23.5 us
    all_to_all x1, blocking collectives, local(): planes = lax.all_to_all(planes, SP[0], 0, 0, tiled=True)  17.7 us
    all_gather x1, waiting for transfers between devices, local(): lax.all_gather(jnp.concatenate([up_weight, down_weight.T], axis=0), SP, a...  16.4 us
    all_to_all x1, blocking collectives, local(): arrived = lax.all_to_all(message, SP[1:], 0, 0, tiled=True)  10.4 us
    all_to_all x1, blocking collectives, local(): lax.all_to_all(prefixes, SP[1:], 0, 0, tiled=True).reshape(512, LANES)  8.49 us
    pallas_call x2, Pallas kernels, finish(): pl.pallas_call(functools.partial(finish_kernel, first=first), out_shape=o...  7.51 us
    pallas_call x1, Pallas kernels, local(): pl.pallas_call(functools.partial(far_mixer_kernel, ups=ups, downs=downs),...  7.04 us
  transfers between devices with their start and end apart: 17, of which 7 were waited for; matrix products, arithmetic and copies ran while one was open for 0% of the time, Pallas kernels for 20%

profile of v8, /device:TPU:32, one launch (start us, length us, event | category | flops | bytes accessed | tf_op | source)
XLA Modules:
  0.0 149.5 jit_solution(3099980760436865594)
XLA Ops:
  6.5 1.7 %pad_maximum_fusion = bf16[64,2048]{1,0:T(8,128)(2,1)} fusion(bf16[32,2048]{1,0:T(8,128)(2,1)} %bitcast.14, bf16[32,2048]{1,0:T(8,128)(2,1)} %param.34), kind=kLoop, calls=%fused_computation | loop fusion | flops 524288 | bytes 524288 | tf_op jit(solution)/shard_map/concatenate | solution.py:467
  8.3 6.2 %states.1 = (f32[4,512,128]{2,1,0:T(8,128)S(1)}, f32[4,8,128]{2,1,0:T(8,128)S(1)}, bf16[8,72,128]{2,1,0:T(8,128)(2,1)S(1)}, f32[4,128,128]{2,1,0:T(8,128)S(1)}, ...) custom-call(s32[1]{0:T(128)} %bitcast.index_ref, ...), custom_call_target="tpu_custom_call" | custom-call | flops 60000000 | bytes 2500000 | tf_op jit(solution)/shard_map/states/pallas_call | solution.py:496
  14.5 10.4 %all_to_all.15.message_ref = bf16[8,72,128]{2,1,0:T(8,128)(2,1)S(1)} all-to-all(bf16[8,72,128]{2,1,0:T(8,128)(2,1)S(1)} %get-tuple-element.59), channel_id=1, replica_groups=mesh['sp_0'=8,'sp_1'=4,'sp_2'=2,'tp'=4] {'sp_1','sp_2'}, dimensions={0} | all-to-all | bytes 294912 | tf_op jit(solution)/shard_map/all_to_all | solution.py:537
  24.9 17.7 %all_to_all.16.planes_ref = bf16[8,72,128]{2,1,0:T(8,128)(2,1)S(1)} all-to-all(bf16[8,72,128]{2,1,0:T(8,128)(2,1)S(1)} %get-tuple-element.60), channel_id=1, replica_groups=mesh['sp_0'=8,'sp_1'=4,'sp_2'=2,'tp'=4] {'sp_0'}, dimensions={0} | all-to-all | bytes 294912 | tf_op jit(solution)/shard_map/all_to_all | solution.py:549
  42.7 8.5 %all_to_all.17 = bf16[8,64,128]{2,1,0:T(8,128)(2,1)S(1)} all-to-all(bf16[8,64,128]{2,1,0:T(8,128)(2,1)S(1)} %prefix.1), channel_id=1, replica_groups=mesh['sp_0'=8,'sp_1'=4,'sp_2'=2,'tp'=4] {'sp_1','sp_2'}, dimensions={0} | all-to-all | bytes 262144 | tf_op jit(solution)/shard_map/all_to_all | solution.py:560
  51.2 1.9 %finish_far.1 = (bf16[64,2048]{1,0:T(8,128)(2,1)S(1)}, bf16[64,2048]{1,0:T(8,128)(2,1)S(1)}) custom-call(s32[1]{0:T(128)} %bitcast.index_ref, s32[1]{0:T(128)} %bitcast.1._.turn_ref, bf16[512,384]{1,0:T(8,128)(2,1)S(1)} %get-tuple-element.44.wq_ref, bf16[512,384]{1,0:T(8,128)(2,1)S(1)} %get-tuple-element.45.wk_ref, ...), custom_call_target="tpu_custom_call" | custom-call | flops 350000000 | bytes 4500000 | tf_op jit(solution)/shard_map/finish_far/pallas_call | solution.py:564
  53.1 1.7 %collective-permute-start = (bf16[64,2048]{1,0:T(8,128)(2,1)S(1)}, bf16[64,2048]{1,0:T(8,128)(2,1)S(1)}, u32[]{:S(2)}, u32[]{:S(2)}) collective-permute-start(bf16[64,2048]{1,0:T(8,128)(2,1)S(1)} %get-tuple-element.65), channel_id=1, source_target_pairs={{0,1},{1,2},{2,3},{3,0},{4,5},{5,6},{6,7},{7,4},{8,9},{9,10},{10,1... | collective-permute-start | bytes 786440 | tf_op jit(solution)/shard_map/ppermute | solution.py:427
  54.8 1.7 %collective-permute-start.1 = (bf16[64,2048]{1,0:T(8,128)(2,1)S(1)}, bf16[64,2048]{1,0:T(8,128)(2,1)S(1)}, u32[]{:S(2)}, u32[]{:S(2)}) collective-permute-start(bf16[64,2048]{1,0:T(8,128)(2,1)S(1)} %get-tuple-element.66), channel_id=1, source_target_pairs={{0,3},{1,0},{2,1},{3,2},{4,7},{5,4},{6,5},{7,6},{8,11},{9,8},{10,9... | collective-permute-start | bytes 786440 | tf_op jit(solution)/shard_map/ppermute | solution.py:427
  56.4 5.6 %finish.1.minus_ref.plus_ref.own_ref = bf16[3,128,2048]{2,1,0:T(8,128)(2,1)S(1)} custom-call(s32[1]{0:T(128)} %bitcast.index_ref, s32[1]{0:T(128)} %bitcast.1._.turn_ref, bf16[512,384]{1,0:T(8,128)(2,1)S(1)} %get-tuple-element.44.wq_ref, bf16[512,384]{1,0:T(8,128)(2,1)S(1)} %get-tuple-element.45.wk_ref, bf16[512,384]{1,0:T(8,128)(2,1)S(1)} %get-tuple-element.46.wv_ref, ...), custom_call_target="tpu_custom_call" | custom-call | flops 1050000000 | bytes 7500000 | tf_op jit(solution)/shard_map/finish/pallas_call | solution.py:564
  64.3 1.7 %collective-permute-start.3 = (bf16[128,2048]{1,0:T(8,128)(2,1)S(1)}, bf16[128,2048]{1,0:T(8,128)(2,1)S(1)}, u32[]{:S(2)}, u32[]{:S(2)}) collective-permute-start(bf16[128,2048]{1,0:T(8,128)(2,1)S(1)} %get-tuple-element.68), channel_id=1, source_target_pairs={{0,3},{1,0},{2,1},{3,2},{4,7},{5,4},{6,5},{7,6},{8,11},{9,8},{10,9... | collective-permute-start | bytes 1572872 | tf_op jit(solution)/shard_map/ppermute | solution.py:427
  66.0 10.8 %collective-permute-done.2.below_ref = bf16[128,2048]{1,0:T(8,128)(2,1)S(1)} collective-permute-done((bf16[128,2048]{1,0:T(8,128)(2,1)S(1)}, bf16[128,2048]{1,0:T(8,128)(2,1)S(1)}, u32[]{:S(2)}, u32[]{:S(2)}) %collective-permute-start.2) | collective-permute-done | bytes 524320 | tf_op jit(solution)/shard_map/ppermute | solution.py:427
  78.7 2.3 %collective-permute-start.7 = (bf16[64,2048]{1,0:T(8,128)(2,1)S(1)}, bf16[64,2048]{1,0:T(8,128)(2,1)S(1)}, u32[]{:S(2)}, u32[]{:S(2)}) collective-permute-start(bf16[64,2048]{1,0:T(8,128)(2,1)S(1)} %get-tuple-element.70.second_ref), channel_id=1, source_target_pairs={{0,3},{1,0},{2,1},{3,2},{4,7},{5,4},{6,5},{7,6},{8,11},{9,8},{10,9... | collective-permute-start | bytes 786440 | tf_op jit(solution)/shard_map/ppermute | solution.py:427
  81.0 4.5 %collective-permute-done.4.refs_0_ = bf16[64,2048]{1,0:T(8,128)(2,1)S(1)} collective-permute-done((bf16[64,2048]{1,0:T(8,128)(2,1)S(1)}, bf16[64,2048]{1,0:T(8,128)(2,1)S(1)}, u32[]{:S(2)}, u32[]{:S(2)}) %collective-permute-start.4) | collective-permute-done | bytes 262176 | tf_op jit(solution)/shard_map/ppermute | solution.py:427
  85.5 3.2 %collective-permute-start.9 = (bf16[64,2048]{1,0:T(8,128)(2,1)S(1)}, bf16[64,2048]{1,0:T(8,128)(2,1)S(1)}, u32[]{:S(2)}, u32[]{:S(2)}) collective-permute-start(bf16[64,2048]{1,0:T(8,128)(2,1)S(1)} %collective-permute-done.7.refs_3_), channel_id=1, source_target_pairs={{0,3},{1,0},{2,1},{3,2},{4,7},{5,4},{6,5},{7,6},{8,11},{9,8},{10,9... | collective-permute-start | bytes 786440 | tf_op jit(solution)/shard_map/ppermute | solution.py:427
  88.7 3.2 %collective-permute-start.6 = (bf16[64,2048]{1,0:T(8,128)(2,1)S(1)}, bf16[64,2048]{1,0:T(8,128)(2,1)S(1)}, u32[]{:S(2)}, u32[]{:S(2)}) collective-permute-start(bf16[64,2048]{1,0:T(8,128)(2,1)S(1)} %get-tuple-element.78.first_ref), channel_id=1, source_target_pairs={{0,3},{1,0},{2,1},{3,2},{4,7},{5,4},{6,5},{7,6},{8,11},{9,8},{10,9... | collective-permute-start | bytes 786440 | tf_op jit(solution)/shard_map/ppermute | solution.py:427
  91.9 3.3 %collective-permute-done.8.refs_0_ = bf16[64,2048]{1,0:T(8,128)(2,1)S(1)} collective-permute-done((bf16[64,2048]{1,0:T(8,128)(2,1)S(1)}, bf16[64,2048]{1,0:T(8,128)(2,1)S(1)}, u32[]{:S(2)}, u32[]{:S(2)}) %collective-permute-start.8) | collective-permute-done | bytes 262176 | tf_op jit(solution)/shard_map/ppermute | solution.py:427
  95.2 16.4 %all-gather.2.cloned.1.call-done = bf16[4096,2048]{1,0:T(8,128)(2,1)} async-done(((bf16[64,2048]{1,0:T(8,128)(2,1)}), bf16[4096,2048]{1,0:T(8,128)(2,1)}) %all-gather.2.cloned.1.call-update) | async-done | bytes 16777232 | tf_op jit(solution)/shard_map/all_gather | solution.py:466
  111.6 7.0 %mixer_far.1 = (bf16[64,32,2048]{2,1,0:T(8,128)(2,1)S(1)}, bf16[64,32,2048]{2,1,0:T(8,128)(2,1)S(1)}, bf16[1024,128]{1,0:T(8,128)(2,1)S(1)}, bf16[1024,128]{1,0:T(8,128)(2,1)S(1)}) custom-call(bf16[64,2048]{1,0:T(8,128)(2,1)S(1)} %collective-permute-done.8.refs_0_, bf16[64,2048]{1,0:T(8,128)(2,1)S(1)} %collective-permute-done.9.refs_1_, ...), custom_call_target="tpu_custom_call" | custom-call | flops 2147483648 | bytes 20000000 | tf_op jit(solution)/shard_map/mixer_far/pallas_call | solution.py:629
  120.2 1.8 %collective-permute-start.11 = (bf16[1024,128]{1,0:T(8,128)(2,1)S(1)}, bf16[1024,128]{1,0:T(8,128)(2,1)S(1)}, u32[]{:S(2)}, u32[]{:S(2)}) collective-permute-start(bf16[1024,128]{1,0:T(8,128)(2,1)S(1)} %get-tuple-element.76), channel_id=1, source_target_pairs={{0,3},{1,0},{2,1},{3,2},{4,7},{5,4},{6,5},{7,6},{8,11},{9,8},{10,9... | collective-permute-start | bytes 786440 | tf_op jit(solution)/shard_map/ppermute | solution.py:427
  122.0 4.5 %mixer_near.1 = (bf16[1024,128]{1,0:T(8,128)(2,1)S(1)}, bf16[1024,128]{1,0:T(8,128)(2,1)S(1)}, bf16[1024,128]{1,0:T(8,128)(2,1)S(1)}, bf16[1024,128]{1,0:T(8,128)(2,1)S(1)}) custom-call(bf16[64,2048]{1,0:T(8,128)(2,1)S(1)} %collective-permute-done.4.refs_0_, bf16[64,2048]{1,0:T(8,128)(2,1)S(1)} %collective-permute-done.5.refs_1_, ...), custom_call_target="tpu_custom_call" | custom-call | flops 4294967296 | bytes 2000000 | tf_op jit(solution)/shard_map/mixer_near/pallas_call | solution.py:642
  126.8 3.0 %collective-permute-start.14 = (bf16[1024,128]{1,0:T(8,128)(2,1)S(1)}, bf16[1024,128]{1,0:T(8,128)(2,1)S(1)}, u32[]{:S(2)}, u32[]{:S(2)}) collective-permute-start(bf16[1024,128]{1,0:T(8,128)(2,1)S(1)} %get-tuple-element.80), channel_id=1, source_target_pairs={{0,3},{1,0},{2,1},{3,2},{4,7},{5,4},{6,5},{7,6},{8,11},{9,8},{10,9... | collective-permute-start | bytes 786440 | tf_op jit(solution)/shard_map/ppermute | solution.py:427
  130.1 3.1 %collective-permute-start.15 = (bf16[1024,128]{1,0:T(8,128)(2,1)S(1)}, bf16[1024,128]{1,0:T(8,128)(2,1)S(1)}, u32[]{:S(2)}, u32[]{:S(2)}) collective-permute-start(bf16[1024,128]{1,0:T(8,128)(2,1)S(1)} %get-tuple-element.81), channel_id=1, source_target_pairs={{0,3},{1,0},{2,1},{3,2},{4,7},{5,4},{6,5},{7,6},{8,11},{9,8},{10,9... | collective-permute-start | bytes 786440 | tf_op jit(solution)/shard_map/ppermute | solution.py:427
  133.2 3.5 %mixer_own.1.own_ref = bf16[2048,128]{1,0:T(8,128)(2,1)S(1)} custom-call(bf16[64,2048]{1,0:T(8,128)(2,1)S(1)} %get-tuple-element.78.first_ref, bf16[64,2048]{1,0:T(8,128)(2,1)S(1)} %get-tuple-element.70.second_ref, bf16[64,32,2048]{2,1,0:T(8,128)(2,1)S(1)} %get-tuple-element.71.refs_4_.up_ref, bf16[64,32,2048]{2,1,0:T(8,128)(2,1)S(1)} %get-tuple-element.72.refs_5_.down_ref), custom_call_target="tpu_custom_call" | custom-call | flops 2147483648 | bytes 2000000 | tf_op jit(solution)/shard_map/mixer_own/pallas_call | solution.py:666
  136.9 4.3 %collective-permute-done.12.below_low_ref = bf16[1024,128]{1,0:T(8,128)(2,1)S(1)} collective-permute-done((bf16[1024,128]{1,0:T(8,128)(2,1)S(1)}, bf16[1024,128]{1,0:T(8,128)(2,1)S(1)}, u32[]{:S(2)}, u32[]{:S(2)}) %collective-permute-start.12) | collective-permute-done | bytes 262176 | tf_op jit(solution)/shard_map/ppermute | solution.py:427
  (35 shorter events, 8.1 us)
Async XLA Ops:
  6.5 105.1 %all-gather.2.cloned.1.call-start = ((), (), s32[]{:S(2)}) async-start(), calls=%async_computation.3 | async-start | bytes 17039360 | tf_op jit(solution)/shard_map/all_gather | solution.py:466
  51.2 25.6 %copy-start = (bf16[128,2048]{1,0:T(8,128)(2,1)S(1)}, bf16[128,2048]{1,0:T(8,128)(2,1)}, u32[]{:S(2)}) copy-start(bf16[128,2048]{1,0:T(8,128)(2,1)} %residual_ref.1) | copy-start | bytes 1572868
  51.2 25.6 %copy-start.1 = (f32[2048]{0:T(1024)S(1)}, f32[2048]{0:T(1024)}, u32[]{:S(2)}) copy-start(f32[2048]{0:T(1024)} %param.36) | copy-start | bytes 24580
  51.2 25.6 %copy-start.2 = (f32[2048]{0:T(1024)S(1)}, f32[2048]{0:T(1024)}, u32[]{:S(2)}) copy-start(f32[2048]{0:T(1024)} %param.37) | copy-start | bytes 24580
  53.1 9.4 %collective-permute-start = (bf16[64,2048]{1,0:T(8,128)(2,1)S(1)}, bf16[64,2048]{1,0:T(8,128)(2,1)S(1)}, u32[]{:S(2)}, u32[]{:S(2)}) collective-permute-start(bf16[64,2048]{1,0:T(8,128)(2,1)S(1)} %get-tuple-element.65), channel_id=1, source_target_pairs={{0,1},{1,2},{2,3},{3,0},{4,5},{5,6},{6,7},{7,4},{8,9},{9,10},{10,1... | collective-permute-start | bytes 786440 | tf_op jit(solution)/shard_map/ppermute | solution.py:427
  54.8 7.7 %collective-permute-start.1 = (bf16[64,2048]{1,0:T(8,128)(2,1)S(1)}, bf16[64,2048]{1,0:T(8,128)(2,1)S(1)}, u32[]{:S(2)}, u32[]{:S(2)}) collective-permute-start(bf16[64,2048]{1,0:T(8,128)(2,1)S(1)} %get-tuple-element.66), channel_id=1, source_target_pairs={{0,3},{1,0},{2,1},{3,2},{4,7},{5,4},{6,5},{7,6},{8,11},{9,8},{10,9... | collective-permute-start | bytes 786440 | tf_op jit(solution)/shard_map/ppermute | solution.py:427
  62.7 14.1 %collective-permute-start.2 = (bf16[128,2048]{1,0:T(8,128)(2,1)S(1)}, bf16[128,2048]{1,0:T(8,128)(2,1)S(1)}, u32[]{:S(2)}, u32[]{:S(2)}) collective-permute-start(bf16[128,2048]{1,0:T(8,128)(2,1)S(1)} %get-tuple-element.67), channel_id=1, source_target_pairs={{0,1},{1,2},{2,3},{3,0},{4,5},{5,6},{6,7},{7,4},{8,9},{9,10},{10,1... | collective-permute-start | bytes 1572872 | tf_op jit(solution)/shard_map/ppermute | solution.py:427
  64.3 12.5 %collective-permute-start.3 = (bf16[128,2048]{1,0:T(8,128)(2,1)S(1)}, bf16[128,2048]{1,0:T(8,128)(2,1)S(1)}, u32[]{:S(2)}, u32[]{:S(2)}) collective-permute-start(bf16[128,2048]{1,0:T(8,128)(2,1)S(1)} %get-tuple-element.68), channel_id=1, source_target_pairs={{0,3},{1,0},{2,1},{3,2},{4,7},{5,4},{6,5},{7,6},{8,11},{9,8},{10,9... | collective-permute-start | bytes 1572872 | tf_op jit(solution)/shard_map/ppermute | solution.py:427
  77.7 7.8 %collective-permute-start.4 = (bf16[64,2048]{1,0:T(8,128)(2,1)S(1)}, bf16[64,2048]{1,0:T(8,128)(2,1)S(1)}, u32[]{:S(2)}, u32[]{:S(2)}) collective-permute-start(bf16[64,2048]{1,0:T(8,128)(2,1)S(1)} %get-tuple-element.78.first_ref), channel_id=1, source_target_pairs={{0,1},{1,2},{2,3},{3,0},{4,5},{5,6},{6,7},{7,4},{8,9},{9,10},{10,1... | collective-permute-start | bytes 786440 | tf_op jit(solution)/shard_map/ppermute | solution.py:427
  78.7 6.7 %collective-permute-start.7 = (bf16[64,2048]{1,0:T(8,128)(2,1)S(1)}, bf16[64,2048]{1,0:T(8,128)(2,1)S(1)}, u32[]{:S(2)}, u32[]{:S(2)}) collective-permute-start(bf16[64,2048]{1,0:T(8,128)(2,1)S(1)} %get-tuple-element.70.second_ref), channel_id=1, source_target_pairs={{0,3},{1,0},{2,1},{3,2},{4,7},{5,4},{6,5},{7,6},{8,11},{9,8},{10,9... | collective-permute-start | bytes 786440 | tf_op jit(solution)/shard_map/ppermute | solution.py:427
  85.5 9.8 %collective-permute-start.8 = (bf16[64,2048]{1,0:T(8,128)(2,1)S(1)}, bf16[64,2048]{1,0:T(8,128)(2,1)S(1)}, u32[]{:S(2)}, u32[]{:S(2)}) collective-permute-start(bf16[64,2048]{1,0:T(8,128)(2,1)S(1)} %collective-permute-done.4.refs_0_), channel_id=1, source_target_pairs={{0,1},{1,2},{2,3},{3,0},{4,5},{5,6},{6,7},{7,4},{8,9},{9,10},{10,1... | collective-permute-start | bytes 786440 | tf_op jit(solution)/shard_map/ppermute | solution.py:427
  85.5 9.7 %collective-permute-start.9 = (bf16[64,2048]{1,0:T(8,128)(2,1)S(1)}, bf16[64,2048]{1,0:T(8,128)(2,1)S(1)}, u32[]{:S(2)}, u32[]{:S(2)}) collective-permute-start(bf16[64,2048]{1,0:T(8,128)(2,1)S(1)} %collective-permute-done.7.refs_3_), channel_id=1, source_target_pairs={{0,3},{1,0},{2,1},{3,2},{4,7},{5,4},{6,5},{7,6},{8,11},{9,8},{10,9... | collective-permute-start | bytes 786440 | tf_op jit(solution)/shard_map/ppermute | solution.py:427
  88.7 33.3 %collective-permute-start.5 = (bf16[64,2048]{1,0:T(8,128)(2,1)S(1)}, bf16[64,2048]{1,0:T(8,128)(2,1)S(1)}, u32[]{:S(2)}, u32[]{:S(2)}) collective-permute-start(bf16[64,2048]{1,0:T(8,128)(2,1)S(1)} %get-tuple-element.70.second_ref), channel_id=1, source_target_pairs={{0,1},{1,2},{2,3},{3,0},{4,5},{5,6},{6,7},{7,4},{8,9},{9,10},{10,1... | collective-permute-start | bytes 786440 | tf_op jit(solution)/shard_map/ppermute | solution.py:427
  88.7 33.3 %collective-permute-start.6 = (bf16[64,2048]{1,0:T(8,128)(2,1)S(1)}, bf16[64,2048]{1,0:T(8,128)(2,1)S(1)}, u32[]{:S(2)}, u32[]{:S(2)}) collective-permute-start(bf16[64,2048]{1,0:T(8,128)(2,1)S(1)} %get-tuple-element.78.first_ref), channel_id=1, source_target_pairs={{0,3},{1,0},{2,1},{3,2},{4,7},{5,4},{6,5},{7,6},{8,11},{9,8},{10,9... | collective-permute-start | bytes 786440 | tf_op jit(solution)/shard_map/ppermute | solution.py:427
  118.6 11.1 %collective-permute-start.10 = (bf16[1024,128]{1,0:T(8,128)(2,1)S(1)}, bf16[1024,128]{1,0:T(8,128)(2,1)S(1)}, u32[]{:S(2)}, u32[]{:S(2)}) collective-permute-start(bf16[1024,128]{1,0:T(8,128)(2,1)S(1)} %get-tuple-element.75), channel_id=1, source_target_pairs={{0,1},{1,2},{2,3},{3,0},{4,5},{5,6},{6,7},{7,4},{8,9},{9,10},{10,1... | collective-permute-start | bytes 786440 | tf_op jit(solution)/shard_map/ppermute | solution.py:427
  120.2 9.6 %collective-permute-start.11 = (bf16[1024,128]{1,0:T(8,128)(2,1)S(1)}, bf16[1024,128]{1,0:T(8,128)(2,1)S(1)}, u32[]{:S(2)}, u32[]{:S(2)}) collective-permute-start(bf16[1024,128]{1,0:T(8,128)(2,1)S(1)} %get-tuple-element.76), channel_id=1, source_target_pairs={{0,3},{1,0},{2,1},{3,2},{4,7},{5,4},{6,5},{7,6},{8,11},{9,8},{10,9... | collective-permute-start | bytes 786440 | tf_op jit(solution)/shard_map/ppermute | solution.py:427
  126.5 10.5 %collective-permute-start.13 = (bf16[1024,128]{1,0:T(8,128)(2,1)S(1)}, bf16[1024,128]{1,0:T(8,128)(2,1)S(1)}, u32[]{:S(2)}, u32[]{:S(2)}) collective-permute-start(bf16[1024,128]{1,0:T(8,128)(2,1)S(1)} %get-tuple-element.79), channel_id=1, source_target_pairs={{0,1},{1,2},{2,3},{3,0},{4,5},{5,6},{6,7},{7,4},{8,9},{9,10},{10,1... | collective-permute-start | bytes 786440 | tf_op jit(solution)/shard_map/ppermute | solution.py:427
  126.8 10.1 %collective-permute-start.14 = (bf16[1024,128]{1,0:T(8,128)(2,1)S(1)}, bf16[1024,128]{1,0:T(8,128)(2,1)S(1)}, u32[]{:S(2)}, u32[]{:S(2)}) collective-permute-start(bf16[1024,128]{1,0:T(8,128)(2,1)S(1)} %get-tuple-element.80), channel_id=1, source_target_pairs={{0,3},{1,0},{2,1},{3,2},{4,7},{5,4},{6,5},{7,6},{8,11},{9,8},{10,9... | collective-permute-start | bytes 786440 | tf_op jit(solution)/shard_map/ppermute | solution.py:427
  129.9 11.4 %collective-permute-start.12 = (bf16[1024,128]{1,0:T(8,128)(2,1)S(1)}, bf16[1024,128]{1,0:T(8,128)(2,1)S(1)}, u32[]{:S(2)}, u32[]{:S(2)}) collective-permute-start(bf16[1024,128]{1,0:T(8,128)(2,1)S(1)} %get-tuple-element.77), channel_id=1, source_target_pairs={{0,1},{1,2},{2,3},{3,0},{4,5},{5,6},{6,7},{7,4},{8,9},{9,10},{10,1... | collective-permute-start | bytes 786440 | tf_op jit(solution)/shard_map/ppermute | solution.py:427
  130.1 11.2 %copy-start.3 = (f32[2048]{0:T(1024)S(1)}, f32[2048]{0:T(1024)}, u32[]{:S(2)}) copy-start(f32[2048]{0:T(1024)} %param.38) | copy-start | bytes 24580
  130.1 11.2 %collective-permute-start.15 = (bf16[1024,128]{1,0:T(8,128)(2,1)S(1)}, bf16[1024,128]{1,0:T(8,128)(2,1)S(1)}, u32[]{:S(2)}, u32[]{:S(2)}) collective-permute-start(bf16[1024,128]{1,0:T(8,128)(2,1)S(1)} %get-tuple-element.81), channel_id=1, source_target_pairs={{0,3},{1,0},{2,1},{3,2},{4,7},{5,4},{6,5},{7,6},{8,11},{9,8},{10,9... | collective-permute-start | bytes 786440 | tf_op jit(solution)/shard_map/ppermute | solution.py:427
Sparse Core Ops, SparseCore 0:
  10.1 101.4 all-gather.1
